TPU v7x, 512 devices: a whole 4x4x16 slice. The times are simulated.
512 devices in a mesh: ep: 32 (over z, core), tp: 16 (over y, x).
Axes of the slice: x: 4, y: 4, z: 16, core: 2. Of those that a mesh axis runs over, the one named last changes fastest.
Arguments:
- token_rows: bfloat16 [768, 2048], P('ep', 'tp'), may hold values from -6 to 6
- prior_state: float32 [768, 64, 2048], P('ep', None, 'tp'), may hold values from -4 to 4
- first_gain: bfloat16 [2048], replicated, may hold values from 0.099609375 to 1.8984375
- w_recept: bfloat16 [2048, 2048], P(None, 'tp'), may hold values from -0.125 to 0.125
- w_key: bfloat16 [2048, 2048], P(None, 'tp'), may hold values from -0.125 to 0.125
- w_value: bfloat16 [2048, 2048], P(None, 'tp'), may hold values from -0.125 to 0.125
- decay_down: bfloat16 [2048, 96], P('tp'), may hold values from -0.125 to 0.125
- decay_up: bfloat16 [96, 2048], P(None, 'tp'), may hold values from -0.625 to 0.625
- decay_base: float32 [2048], P('tp'), may hold values from -4 to 3
- iclr_down: bfloat16 [2048, 96], P('tp'), may hold values from -0.125 to 0.125
- iclr_up: bfloat16 [96, 2048], P(None, 'tp'), may hold values from -0.625 to 0.625
- iclr_base: float32 [2048], P('tp'), may hold values from -4 to 4
- key_scale: bfloat16 [2048], P('tp'), may hold values from 0.29882812 to 1.5
- key_mix: bfloat16 [2048], P('tp'), may hold values from 0 to 2
- head_gain: bfloat16 [2048], P('tp'), may hold values from 0.099609375 to 1.8984375
- w_out: bfloat16 [2048, 2048], P(None, 'tp'), may hold values from -0.125 to 0.125
- second_gain: bfloat16 [2048], replicated, may hold values from 0.099609375 to 1.8984375
- routes: int32 [768, 4], P('ep'), may hold values from 0 to 31, all different within a row; in each aligned block of 24 rows (0 to 23, 24 to 47, ...) at most 4 rows name the same one
- route_weights: float32 [768, 4], P('ep'), may hold values from 0.2 to 1
- exp_gate: bfloat16 [32, 2048, 2048], P('ep', None, 'tp'), may hold values from -0.125 to 0.125
- exp_up: bfloat16 [32, 2048, 2048], P('ep', None, 'tp'), may hold values from -0.125 to 0.125
- exp_down: bfloat16 [32, 2048, 2048], P('ep', 'tp'), may hold values from -0.125 to 0.125
- dense_gate: bfloat16 [2048, 512], P(None, 'tp'), may hold values from -0.125 to 0.125
- dense_up: bfloat16 [2048, 512], P(None, 'tp'), may hold values from -0.125 to 0.125
- dense_down: bfloat16 [512, 2048], P('tp'), may hold values from -0.25 to 0.25
- dense_mix: bfloat16 [2048], replicated, may hold values from -0.125 to 0.125
Outputs:
- layer_out: bfloat16 [768, 2048], P('ep', 'tp')
- next_state: float32 [768, 64, 2048], P('ep', None, 'tp')
Inputs may be any that keep to these rules, and one draw needn't show every extreme that they name: `routes`: each row names 4 different experts. Among the rows of one index of ep no expert is named by more than 4 rows, and in every draw some expert is named by exactly 4 of them.
All inputs are finite; a program needn't handle non-finite values.
Results may differ from a plain program's by a relative error of at most 0.018.
Values may be sent and summed in bfloat16 or wider, within the bound.
No kernel may reach another device: no remote copies, remote signals or barrier semaphores. Data moves between devices by JAX's collectives and lax.ppermute only.
A program may use at most 64 MiB of HBM per device.

v0:
```python
import jax
import jax.numpy as jnp
from jax import lax
from jax.sharding import PartitionSpec as P

HEAD = 64


norm_eps = 1e-06
head_eps = 0.00064
key_eps = 1e-06


def laid_out(pieces, dim):
    pieces = jnp.moveaxis(pieces, 0, dim)
    shape = pieces.shape
    return pieces.reshape(*shape[:dim], shape[dim] * shape[dim + 1], *shape[dim + 2 :])


def sent_to_all(value, axis):
    count = lax.axis_size(axis)
    return lax.all_to_all(
        jnp.broadcast_to(value[None], (count, *value.shape)), axis, 0, 0, tiled=True
    )


def collect(value, axis, dim):
    return laid_out(sent_to_all(value, axis), dim)


def over_copies(value, axis):
    everything = sent_to_all(value, axis)
    return jnp.sum(everything, axis=0)


def together(arrays, axis):
    ends = [0]
    for a in arrays:
        ends.append(ends[-1] + a.size)
    total = over_copies(jnp.concatenate([a.ravel() for a in arrays]), axis)
    return tuple((total[b:e].reshape(a.shape) for a, b, e in zip(arrays, ends, ends[1:])))


def split_up(value, dim, count):
    before, after = (value.shape[:dim], value.shape[dim + 1 :])
    return jnp.moveaxis(value.reshape(*before, count, -1, *after), dim, 0)


def sum_at_owner(value, axis, dim):
    pieces = split_up(value, dim, lax.axis_size(axis))
    arrived = lax.all_to_all(pieces, axis, split_axis=0, concat_axis=0, tiled=True)
    return arrived.astype(jnp.float32).sum(axis=0)


def product(left, right):
    return jnp.dot(left, right, preferred_element_type=jnp.float32)


def scale_rows(values, mean_square, gain):
    return (values * lax.rsqrt(mean_square + norm_eps) * gain.astype(jnp.float32)).astype(
        jnp.bfloat16
    )


def first_norm_rows(token_rows, gain):
    own_width = token_rows.shape[1]
    start = lax.axis_index("tp") * own_width
    gathered = collect(token_rows, "tp", 1)
    values = gathered.astype(jnp.float32)
    full_rows = scale_rows(values, jnp.mean(values * values, axis=1, keepdims=True), gain)
    own_cols = lax.dynamic_slice_in_dim(full_rows, start, own_width, 1)
    return (full_rows, own_cols)


def second_norm_rows(residual, gain):
    own_width = residual.shape[1]
    start = lax.axis_index("tp") * own_width
    gathered = collect(residual, "tp", 1)
    values = gathered.astype(jnp.float32)
    full_rows = scale_rows(values, jnp.mean(values * values, axis=1, keepdims=True), gain)
    own_cols = lax.dynamic_slice_in_dim(full_rows, start, own_width, 1)
    return (full_rows, own_cols)


def local(
    token_rows,
    prior_state,
    first_gain,
    w_recept,
    w_key,
    w_value,
    decay_down,
    decay_up,
    decay_base,
    iclr_down,
    iclr_up,
    iclr_base,
    key_scale,
    key_mix,
    head_gain,
    w_out,
    second_gain,
    routes,
    route_weights,
    exp_gate,
    exp_up,
    exp_down,
    dense_gate,
    dense_up,
    dense_down,
    dense_mix,
):
    seq_count, own_width = token_rows.shape
    heads_dev = own_width // HEAD
    first_full, first_own = first_norm_rows(token_rows, first_gain)
    decay_low, rate_low = together(
        (product(first_own, decay_down), product(first_own, iclr_down)), "tp"
    )
    decay_act = jnp.tanh(decay_low).astype(jnp.bfloat16)
    rate_act = rate_low.astype(jnp.bfloat16)
    recept = product(first_full, w_recept).astype(jnp.bfloat16)
    key_rows = product(first_full, w_key).astype(jnp.bfloat16)
    value_rows = product(first_full, w_value).astype(jnp.bfloat16)
    decay_rate = jnp.exp(
        -jnp.exp(-jax.nn.softplus(-(decay_base + product(decay_act, decay_up))) - 0.5)
    )
    iclr_rate = jax.nn.sigmoid(iclr_base + product(rate_act, iclr_up))
    key_float = key_rows.astype(jnp.float32)
    scaled = (key_float * key_scale.astype(jnp.float32)).reshape(seq_count, heads_dev, HEAD)
    removal = scaled * lax.rsqrt(jnp.sum(scaled * scaled, axis=-1, keepdims=True) + key_eps)
    written = (key_float * (1.0 + (iclr_rate - 1.0) * key_mix.astype(jnp.float32))).reshape(
        seq_count, heads_dev, HEAD
    )
    state_grid = prior_state.reshape(seq_count, HEAD, heads_dev, HEAD)
    recall = jnp.sum(state_grid * removal[:, None], axis=-1)
    scaled_removal = removal * iclr_rate.reshape(seq_count, heads_dev, HEAD)
    value_cols = jnp.transpose(
        value_rows.astype(jnp.float32).reshape(seq_count, heads_dev, HEAD), (0, 2, 1)
    )
    state_grid = (
        state_grid * decay_rate.reshape(seq_count, 1, heads_dev, HEAD)
        - recall[..., None] * scaled_removal[:, None]
        + value_cols[..., None] * written[:, None]
    )
    read = jnp.sum(
        state_grid * recept.astype(jnp.float32).reshape(seq_count, 1, heads_dev, HEAD), axis=-1
    )
    read = jnp.transpose(read, (0, 2, 1))
    centered = read - jnp.mean(read, axis=-1, keepdims=True)
    variance = jnp.mean(centered * centered, axis=-1, keepdims=True)
    head_out = (
        centered
        * lax.rsqrt(variance + head_eps)
        * head_gain.astype(jnp.float32).reshape(heads_dev, HEAD)
    )
    head_out = head_out.reshape(seq_count, own_width).astype(jnp.bfloat16)
    heads_all = collect(head_out, "tp", 1)
    mixer_out = product(heads_all, w_out).astype(jnp.bfloat16)
    residual = (token_rows.astype(jnp.float32) + mixer_out.astype(jnp.float32)).astype(jnp.bfloat16)
    second_full, second_own = second_norm_rows(residual, second_gain)
    dense_hidden = (
        jax.nn.silu(product(second_full, dense_gate)) * product(second_full, dense_up)
    ).astype(jnp.bfloat16)
    dense_out = sum_at_owner(product(dense_hidden, dense_down).astype(jnp.bfloat16), "tp", 1)
    mix_gate = jax.nn.sigmoid(product(second_full, dense_mix[:, None])[:, 0])
    group_count = lax.axis_size("ep")
    local_experts = exp_gate.shape[0]
    experts = local_experts * group_count
    top_count = routes.shape[1]
    capacity = max(2, 3 * seq_count * top_count // (2 * experts))
    assign_count = seq_count * top_count
    flat_ids = routes.reshape(assign_count)
    onehot = (flat_ids[:, None] == jnp.arange(experts, dtype=jnp.int32)[None, :]).astype(
        jnp.float32
    )
    earlier = (jnp.arange(assign_count)[:, None] > jnp.arange(assign_count)[None, :]).astype(
        jnp.float32
    )
    before = jnp.dot(earlier, onehot, precision=lax.Precision.HIGHEST)
    ranking = jnp.sum(before * onehot, axis=1).astype(jnp.int32)
    slot_index = flat_ids * capacity + ranking
    slot_total = experts * capacity
    slot_onehot = (jnp.arange(slot_total, dtype=jnp.int32)[:, None] == slot_index[None, :]).astype(
        jnp.bfloat16
    )
    repeated = jnp.repeat(second_own, top_count, axis=0)
    outgoing = product(slot_onehot, repeated).astype(jnp.bfloat16)
    outgoing = outgoing.reshape(group_count, local_experts, capacity, second_own.shape[1])
    arrived = lax.all_to_all(outgoing, "ep", split_axis=0, concat_axis=0, tiled=True)
    arrived = collect(arrived, "tp", 3)
    gate_act = jnp.einsum("secd,edf->secf", arrived, exp_gate, preferred_element_type=jnp.float32)
    up_act = jnp.einsum("secd,edf->secf", arrived, exp_up, preferred_element_type=jnp.float32)
    hidden = (jax.nn.silu(gate_act) * up_act).astype(jnp.bfloat16)
    partial_value = jnp.einsum(
        "secf,efd->secd", hidden, exp_down, preferred_element_type=jnp.float32
    ).astype(jnp.bfloat16)
    partial_value = lax.optimization_barrier(partial_value)
    summed = sum_at_owner(partial_value.astype(jnp.float32).astype(jnp.bfloat16), "tp", 3).astype(
        jnp.bfloat16
    )
    returned = lax.all_to_all(summed, "ep", split_axis=0, concat_axis=0, tiled=True)
    returned = returned.reshape(slot_total, own_width)
    picked = jnp.take(returned, slot_index, axis=0).astype(jnp.float32)
    weighted = picked * route_weights.reshape(assign_count)[:, None]
    routed = jnp.sum(weighted.reshape(seq_count, top_count, own_width), axis=1)
    layer_out = residual.astype(jnp.float32) + routed + mix_gate[:, None] * dense_out
    return (layer_out.astype(jnp.bfloat16), state_grid.reshape(seq_count, HEAD, own_width))


def solution(mesh):
    in_specs = (
        P("ep", "tp"),
        P("ep", None, "tp"),
        P(),
        P(None, "tp"),
        P(None, "tp"),
        P(None, "tp"),
        P("tp", None),
        P(None, "tp"),
        P("tp"),
        P("tp", None),
        P(None, "tp"),
        P("tp"),
        P("tp"),
        P("tp"),
        P("tp"),
        P(None, "tp"),
        P(),
        P("ep", None),
        P("ep", None),
        P("ep", None, "tp"),
        P("ep", None, "tp"),
        P("ep", "tp", None),
        P(None, "tp"),
        P(None, "tp"),
        P("tp", None),
        P(),
    )
    out_specs = (P("ep", "tp"), P("ep", None, "tp"))
    return jax.shard_map(local, mesh=mesh, in_specs=in_specs, out_specs=out_specs, check_vma=False)
```

profile of v0, /device:TPU:1, one launch (start us, length us, event | category | flops | bytes accessed | tf_op | source)
XLA Modules:
  0.0 167.7 jit_solution(7866539967462157941)
XLA Ops:
  0.7 1.4 broadcast_in_dim.21
  2.1 7.6 %all-to-all-start = ((bf16[16,24,128]{2,1,0:T(8,128)(2,1)}), bf16[16,24,128]{2,1,0:T(8,128)(2,1)S(1)}, u32[]{:S(2)}, u32[]{:S(2)}) async-start(bf16[16,24,128]{2,1,0:T(8,128)(2,1)} %broadcast_in_dim.21), calls=%async_computation | async-start | bytes 196608 | tf_op jit(solution)/shard_map/all_to_all | solution.py:22
  9.7 1.3 convert_bitcast_fusion.2
  11.0 2.3 %reshape.267 = f32[24,64,2,64]{3,2,1,0:T(2,128)S(1)} reshape(f32[24,64,128]{2,1,0:T(8,128)} %param.27) | data formatting | bytes 1572864 | tf_op jit(solution)/shard_map/reshape | solution.py:134
  13.4 0.6 reshape.287
  14.1 0.6 reshape.274
  14.7 1.7 all-to-all-done
  16.6 0.2 fusion.13
  16.9 0.2 broadcast_multiply_fusion.1
  17.3 0.1 fusion.59
  17.5 0.1 fusion.61
  17.7 0.9 broadcast_in_dim.22
  18.6 5.0 %all-to-all-start.1 = ((f32[16,1,4608]{2,1,0:T(1,128)}), f32[16,1,4608]{2,1,0:T(1,128)S(1)}, u32[]{:S(2)}, u32[]{:S(2)}) async-start(f32[16,1,4608]{2,1,0:T(1,128)} %broadcast_in_dim.22), calls=%async_computation.1 | async-start | bytes 589824 | tf_op jit(solution)/shard_map/all_to_all | solution.py:22
  23.9 1.2 fusion.12
  25.2 0.3 copy.93
  25.5 5.9 %all-to-all-done.1 = f32[16,1,4608]{2,1,0:T(1,128)S(1)} async-done(((f32[16,1,4608]{2,1,0:T(1,128)}), f32[16,1,4608]{2,1,0:T(1,128)S(1)}, u32[]{:S(2)}, u32[]{:S(2)}) %all-to-all-start.1) | async-done | bytes 294944 | tf_op jit(solution)/shard_map/all_to_all | solution.py:22
  31.4 0.2 reduce_sum.114
  31.7 0.1 multiply_multiply_fusion
  32.3 0.2 fusion.50
  32.5 1.7 %multiply_reduce_fusion.1 = f32[24,64,2]{2,1,0:T(8,128)S(1)} fusion(f32[24,64,2,64]{3,2,1,0:T(2,128)S(1)} %reshape.267, f32[24,2,64]{2,1,0:T(2,128)S(1)} %get-tuple-element.3), kind=kLoop, calls=%fused_computation.5 | loop fusion | flops 390144 | bytes 811008 | tf_op jit(solution)/shard_map/reduce_sum | solution.py:135
  34.2 0.9 copy-done.1
  35.1 6.6 %multiply_reduce_fusion = f32[24,64,2]{2,1,0:T(8,128)} fusion(f32[24,64,2,64]{3,2,1,0:T(2,128)S(1)} %reshape.267, f32[24,2,64]{2,1,0:T(2,128)S(1)} %reshape.286, f32[24,2,64]{2,1,0:T(2,128)S(1)} %mul.301, f32[24,64,2]{2,1,0:T(8,128)S(1)} %copy.93, f32[24,2,64]{2,1,0:T(2,128)S(1)} %get-tuple-element.2, f32[24,64,2]{2,1,0:T(8,128)S(1)} %multiply_reduce_fusion.1, ...), kind=kLoop, calls=%fused_computation.4 | loop fusion | flops 1373184 | bytes 872448 | tf_op jit(solution)/shard_map/reduce_sum | solution.py:145
  41.7 1.4 copy.94
  43.2 0.2 multiply_reduce_fusion.3
  43.6 0.7 broadcast_in_dim.23
  44.3 3.5 %all-to-all-start.2 = ((bf16[16,24,128]{2,1,0:T(8,128)(2,1)}), bf16[16,24,128]{2,1,0:T(8,128)(2,1)S(1)}, u32[]{:S(2)}, u32[]{:S(2)}) async-start(bf16[16,24,128]{2,1,0:T(8,128)(2,1)} %broadcast_in_dim.23), calls=%async_computation.2 | async-start | bytes 196608 | tf_op jit(solution)/shard_map/all_to_all | solution.py:22
  47.8 0.2 fusion.17
  48.0 6.4 %all-to-all-done.2 = bf16[16,24,128]{2,1,0:T(8,128)(2,1)S(1)} async-done(((bf16[16,24,128]{2,1,0:T(8,128)(2,1)}), bf16[16,24,128]{2,1,0:T(8,128)(2,1)S(1)}, u32[]{:S(2)}, u32[]{:S(2)}) %all-to-all-start.2) | async-done | bytes 98336 | tf_op jit(solution)/shard_map/all_to_all | solution.py:22
  54.4 0.2 fusion.16
  54.6 0.7 broadcast_in_dim.25
  55.3 3.5 %all-to-all-start.3 = ((bf16[16,24,128]{2,1,0:T(8,128)(2,1)}), bf16[16,24,128]{2,1,0:T(8,128)(2,1)S(1)}, u32[]{:S(2)}, u32[]{:S(2)}) async-start(bf16[16,24,128]{2,1,0:T(8,128)(2,1)} %broadcast_in_dim.25), calls=%async_computation.3 | async-start | bytes 196608 | tf_op jit(solution)/shard_map/all_to_all | solution.py:22
  58.8 6.6 %all-to-all-done.3 = bf16[16,24,128]{2,1,0:T(8,128)(2,1)S(1)} async-done(((bf16[16,24,128]{2,1,0:T(8,128)(2,1)}), bf16[16,24,128]{2,1,0:T(8,128)(2,1)S(1)}, u32[]{:S(2)}, u32[]{:S(2)}) %all-to-all-start.3) | async-done | bytes 98336 | tf_op jit(solution)/shard_map/all_to_all | solution.py:22
  65.6 0.6 copy-done.29
  66.3 0.1 convolution_convert_fusion.2
  66.4 31.9 %all_to_all.46 = bf16[32,1,4,128]{3,2,1,0:T(4,128)(2,1)S(1)} all-to-all(bf16[32,1,4,128]{3,2,1,0:T(4,128)(2,1)S(1)} %bitcast.158), channel_id=1, replica_groups=mesh['ep'=32,'tp'=16] {'ep'}, dimensions={0} | all-to-all | bytes 65536 | tf_op jit(solution)/shard_map/all_to_all | solution.py:189
  98.4 0.9 broadcast_in_dim.28
  99.3 3.7 %all-to-all-start.5 = ((bf16[16,32,1,4,128]{4,1,3,2,0:T(8,128)(2,1)}), bf16[16,32,1,4,128]{4,1,3,2,0:T(8,128)(2,1)S(1)}, u32[]{:S(2)}, u32[]{:S(2)}) async-start(bf16[16,32,1,4,128]{4,1,3,2,0:T(8,128)(2,1)} %broadcast_in_dim.28), calls=%async_computation.5 | async-start | bytes 1048576 | tf_op jit(solution)/shard_map/all_to_all | solution.py:22
  103.1 0.6 mul.327
  103.9 9.6 %all-to-all-done.5 = bf16[16,32,1,4,128]{4,1,3,2,0:T(8,128)(2,1)S(1)} async-done(((bf16[16,32,1,4,128]{4,1,3,2,0:T(8,128)(2,1)}), bf16[16,32,1,4,128]{4,1,3,2,0:T(8,128)(2,1)S(1)}, u32[]{:S(2)}, u32[]{:S(2)}) %all-to-all-start.5) | async-done | bytes 524320 | tf_op jit(solution)/shard_map/all_to_all | solution.py:22
  113.5 0.3 copy.103
  113.8 0.2 reshape.277
  114.0 0.9 convolution_bitcast_fusion.1
  115.0 1.4 fusion
  116.4 0.9 bitcast_bitcast_fusion
  117.3 3.8 %all-to-all-start.6 = ((bf16[16,32,1,4,128]{4,1,3,2,0:T(8,128)(2,1)}), bf16[16,32,1,4,128]{4,1,3,2,0:T(8,128)(2,1)S(1)}, u32[]{:S(2)}, u32[]{:S(2)}) async-start(bf16[16,32,1,4,128]{4,1,3,2,0:T(8,128)(2,1)} %bitcast_bitcast_fusion), calls=%async_computation.6 | async-start | bytes 1048576 | tf_op jit(solution)/shard_map/all_to_all | solution.py:51
  121.1 0.7 copy.108
  121.9 0.6 reshape.301
  122.5 0.6 pad_clamp_fusion
  123.1 1.9 %mul.297 = f32[24,64,2,64]{3,2,1,0:T(2,128)S(1)} broadcast(f32[24,64,2]{2,1,0:T(8,128)S(1)} %copy.93), dimensions={0,1,2} | broadcast | bytes 798720 | tf_op jit(solution)/shard_map/mul | solution.py:143
  125.0 1.8 %mul.348 = f32[24,64,128]{2,1,0:T(8,128)} reshape(f32[24,64,2,64]{3,2,1,0:T(2,128)S(1)} %mul.297) | data formatting | bytes 1572864 | tf_op jit(solution)/shard_map/mul | solution.py:143
  126.8 1.9 %mul.293 = f32[24,64,2,64]{3,2,1,0:T(2,128)S(1)} broadcast(f32[24,64,2]{2,1,0:T(8,128)S(1)} %copy-done.2), dimensions={0,1,2} | broadcast | bytes 798720 | tf_op jit(solution)/shard_map/mul | solution.py:142
  128.7 1.8 %mul.342 = f32[24,64,128]{2,1,0:T(8,128)} reshape(f32[24,64,2,64]{3,2,1,0:T(2,128)S(1)} %mul.293) | data formatting | bytes 1572864 | tf_op jit(solution)/shard_map/mul | solution.py:142
  130.5 1.1 fusion.69
  131.6 1.3 fusion.1
  133.0 0.6 copy.131
  133.6 6.4 %all-to-all-start.8 = ((bf16[16,24,128]{2,1,0:T(8,128)(2,1)}), bf16[16,24,128]{2,1,0:T(8,128)(2,1)S(1)}, u32[]{:S(2)}, u32[]{:S(2)}) async-start(bf16[16,24,128]{2,1,0:T(8,128)(2,1)} %bitcast.154), calls=%async_computation.8 | async-start | bytes 196608 | tf_op jit(solution)/shard_map/all_to_all | solution.py:51
  140.1 2.4 %multiply_add_fusion = f32[24,64,128]{2,1,0:T(8,128)} fusion(f32[24,64,128]{2,1,0:T(8,128)S(1)} %copy-done.4, f32[24,64,128]{2,1,0:T(8,128)} %mul.342, f32[24,64,128]{2,1,0:T(8,128)S(1)} %copy-done.3, f32[24,128]{1,0:T(8,128)S(1)} %get-tuple-element.5, f32[24,128]{1,0:T(8,128)S(1)} %get-tuple-element.4, f32[24,128]{1,0:T(8,128)S(1)} %copy-done.13), kind=kLoop, calls=%fused_computation.39 | loop fusion | flops 983040 | bytes 3182592 | tf_op jit(solution)/shard_map/add | solution.py:141
  142.6 0.6 copy.106
  143.2 3.5 %all-to-all-done.8 = bf16[16,24,128]{2,1,0:T(8,128)(2,1)S(1)} async-done(((bf16[16,24,128]{2,1,0:T(8,128)(2,1)}), bf16[16,24,128]{2,1,0:T(8,128)(2,1)S(1)}, u32[]{:S(2)}, u32[]{:S(2)}) %all-to-all-start.8) | async-done | bytes 98336 | tf_op jit(solution)/shard_map/all_to_all | solution.py:51
  146.7 7.1 %all-to-all-start.7 = ((bf16[32,1,4,128]{3,2,1,0:T(4,128)(2,1)}), bf16[32,1,4,128]{3,2,1,0:T(4,128)(2,1)S(1)}, u32[]{:S(2)}, u32[]{:S(2)}) async-start(bf16[32,1,4,128]{3,2,1,0:T(4,128)(2,1)} %copy.106), calls=%async_computation.7 | async-start | bytes 65536 | tf_op jit(solution)/shard_map/all_to_all | solution.py:201
  153.9 0.2 fusion.21
  154.1 11.9 %all-to-all-done.7 = bf16[32,1,4,128]{3,2,1,0:T(4,128)(2,1)S(1)} async-done(((bf16[32,1,4,128]{3,2,1,0:T(4,128)(2,1)}), bf16[32,1,4,128]{3,2,1,0:T(4,128)(2,1)S(1)}, u32[]{:S(2)}, u32[]{:S(2)}) %all-to-all-start.7) | async-done | bytes 32800 | tf_op jit(solution)/shard_map/all_to_all | solution.py:201
  166.1 0.8 gather_fusion
  167.0 0.7 add_convert_fusion
  (128 shorter events, 2.9 us)
Async XLA Ops:
  0.6 114.3 %copy-start = (bf16[1,128,2048]{2,1,0:T(8,128)(2,1)S(1)}, bf16[1,128,2048]{2,1,0:T(8,128)(2,1)}, u32[]{:S(2)}) copy-start(bf16[1,128,2048]{2,1,0:T(8,128)(2,1)} %param.47) | copy-start | bytes 1572868
  0.6 12.7 %copy-start.24 = (bf16[2048]{0:T(1024)(128)(2,1)S(1)}, bf16[2048]{0:T(1024)(128)(2,1)}, u32[]{:S(2)}) copy-start(bf16[2048]{0:T(1024)(128)(2,1)} %param.28) | copy-start | bytes 12292
  0.7 12.7 %copy-start.34 = (bf16[128]{0:T(256)(128)(2,1)S(1)}, bf16[128]{0:T(256)(128)(2,1)}, u32[]{:S(2)}) copy-start(bf16[128]{0:T(256)(128)(2,1)} %param.38) | copy-start | bytes 772
  0.7 12.7 %copy-start.35 = (bf16[128]{0:T(256)(128)(2,1)S(1)}, bf16[128]{0:T(256)(128)(2,1)}, u32[]{:S(2)}) copy-start(bf16[128]{0:T(256)(128)(2,1)} %param.39) | copy-start | bytes 772
  0.7 12.7 %copy-start.36 = (bf16[128]{0:T(256)(128)(2,1)S(1)}, bf16[128]{0:T(256)(128)(2,1)}, u32[]{:S(2)}) copy-start(bf16[128]{0:T(256)(128)(2,1)} %param.40) | copy-start | bytes 772
  0.7 13.3 %copy-start.20 = (s32[24,4]{0,1:T(4,128)S(1)}, s32[24,4]{0,1:T(4,128)}, u32[]{:S(2)}) copy-start(s32[24,4]{0,1:T(4,128)} %param.43) | copy-start | bytes 1156
  0.7 15.9 %copy-start.7 = (bf16[2048,128]{1,0:T(8,128)(2,1)S(1)}, bf16[2048,128]{1,0:T(8,128)(2,1)}, u32[]{:S(2)}) copy-start(bf16[2048,128]{1,0:T(8,128)(2,1)} %param.29) | copy-start | bytes 1572868
  2.1 14.2 %all-to-all-start = ((bf16[16,24,128]{2,1,0:T(8,128)(2,1)}), bf16[16,24,128]{2,1,0:T(8,128)(2,1)S(1)}, u32[]{:S(2)}, u32[]{:S(2)}) async-start(bf16[16,24,128]{2,1,0:T(8,128)(2,1)} %broadcast_in_dim.21), calls=%async_computation | async-start | bytes 196608 | tf_op jit(solution)/shard_map/all_to_all | solution.py:22
  11.0 5.8 %copy-start.9 = (bf16[2048,128]{1,0:T(8,128)(2,1)S(1)}, bf16[2048,128]{1,0:T(8,128)(2,1)}, u32[]{:S(2)}) copy-start(bf16[2048,128]{1,0:T(8,128)(2,1)} %param.30) | copy-start | bytes 1572868
  11.0 6.2 %copy-start.17 = (bf16[128,96]{0,1:T(8,128)(2,1)S(1)}, bf16[128,96]{0,1:T(8,128)(2,1)}, u32[]{:S(2)}) copy-start(bf16[128,96]{0,1:T(8,128)(2,1)} %param.35) | copy-start | bytes 73732
  11.0 6.5 %copy-start.18 = (bf16[128,96]{0,1:T(8,128)(2,1)S(1)}, bf16[128,96]{0,1:T(8,128)(2,1)}, u32[]{:S(2)}) copy-start(bf16[128,96]{0,1:T(8,128)(2,1)} %param.32) | copy-start | bytes 73732
  17.0 14.7 %copy-start.19 = (bf16[96,128]{1,0:T(8,128)(2,1)S(1)}, bf16[96,128]{1,0:T(8,128)(2,1)}, u32[]{:S(2)}) copy-start(bf16[96,128]{1,0:T(8,128)(2,1)} %param.36) | copy-start | bytes 73732
  17.1 14.7 %copy-start.28 = (f32[128]{0:T(128)S(1)}, f32[128]{0:T(128)}, u32[]{:S(2)}) copy-start(f32[128]{0:T(128)} %param.37) | copy-start | bytes 1540
  17.7 14.5 %copy-start.33 = (bf16[96,128]{1,0:T(8,128)(2,1)S(1)}, bf16[96,128]{1,0:T(8,128)(2,1)}, u32[]{:S(2)}) copy-start(bf16[96,128]{1,0:T(8,128)(2,1)} %param.33) | copy-start | bytes 73732
  17.7 14.5 %copy-start.37 = (f32[128]{0:T(128)S(1)}, f32[128]{0:T(128)}, u32[]{:S(2)}) copy-start(f32[128]{0:T(128)} %param.34) | copy-start | bytes 1540
  18.6 12.8 %all-to-all-start.1 = ((f32[16,1,4608]{2,1,0:T(1,128)}), f32[16,1,4608]{2,1,0:T(1,128)S(1)}, u32[]{:S(2)}, u32[]{:S(2)}) async-start(f32[16,1,4608]{2,1,0:T(1,128)} %broadcast_in_dim.22), calls=%async_computation.1 | async-start | bytes 589824 | tf_op jit(solution)/shard_map/all_to_all | solution.py:22
  32.4 1.8 %copy-start.12 = (f32[24,128]{1,0:T(8,128)}, f32[24,128]{1,0:T(8,128)S(1)}, u32[]{:S(2)}) copy-start(f32[24,128]{1,0:T(8,128)S(1)} %fusion.50) | copy-start | bytes 36868
  34.2 0.9 copy-start.1
  35.1 8.3 %copy-start.27 = (f32[2,64]{1,0:T(2,128)S(1)}, f32[2,64]{1,0:T(2,128)}, u32[]{:S(2)}) copy-start(f32[2,64]{1,0:T(2,128)} %reshape.287) | copy-start | bytes 1540
  35.1 12.7 %copy-start.31 = (s32[96]{0:T(128)S(1)}, s32[96]{0:T(128)}, u32[]{:S(2)}) copy-start(s32[96]{0:T(128)} %reshape.274) | copy-start | bytes 1156
  35.1 19.3 %copy-start.8 = (bf16[2048,128]{1,0:T(8,128)(2,1)S(1)}, bf16[2048,128]{1,0:T(8,128)(2,1)}, u32[]{:S(2)}) copy-start(bf16[2048,128]{1,0:T(8,128)(2,1)} %param.41) | copy-start | bytes 1572868
  35.1 19.3 %copy-start.16 = (bf16[24,128]{1,0:T(8,128)(2,1)S(1)}, bf16[24,128]{1,0:T(8,128)(2,1)}, u32[]{:S(2)}) copy-start(bf16[24,128]{1,0:T(8,128)(2,1)} %param.26) | copy-start | bytes 18436
  41.7 24.4 %copy-start.15 = (f32[2048]{0:T(1024)S(1)}, f32[2048]{0:T(1024)}, u32[]{:S(2)}) copy-start(f32[2048]{0:T(1024)} %get-tuple-element.7) | copy-start | bytes 24580
  44.3 10.1 %all-to-all-start.2 = ((bf16[16,24,128]{2,1,0:T(8,128)(2,1)}), bf16[16,24,128]{2,1,0:T(8,128)(2,1)S(1)}, u32[]{:S(2)}, u32[]{:S(2)}) async-start(bf16[16,24,128]{2,1,0:T(8,128)(2,1)} %broadcast_in_dim.23), calls=%async_computation.2 | async-start | bytes 196608 | tf_op jit(solution)/shard_map/all_to_all | solution.py:22
  47.8 55.2 %copy-start.21 = (s32[24,4]{0,1:T(4,128)S(1)}, s32[24,4]{0,1:T(4,128)}, u32[]{:S(2)}) copy-start(s32[24,4]{0,1:T(4,128)} %param.43) | copy-start | bytes 1156
  48.0 55.0 %copy-start.38 = (f32[96]{0:T(128)}, f32[96]{0:T(128)S(1)}, u32[]{:S(2)}) copy-start(f32[96]{0:T(128)S(1)} %fusion.17) | copy-start | bytes 1156
  55.3 10.1 %all-to-all-start.3 = ((bf16[16,24,128]{2,1,0:T(8,128)(2,1)}), bf16[16,24,128]{2,1,0:T(8,128)(2,1)S(1)}, u32[]{:S(2)}, u32[]{:S(2)}) async-start(bf16[16,24,128]{2,1,0:T(8,128)(2,1)} %broadcast_in_dim.25), calls=%async_computation.3 | async-start | bytes 196608 | tf_op jit(solution)/shard_map/all_to_all | solution.py:22
  65.4 33.9 %copy-start.5 = (bf16[16,24,128]{2,1,0:T(8,128)(2,1)}, bf16[16,24,128]{2,1,0:T(8,128)(2,1)S(1)}, u32[]{:S(2)}) copy-start(bf16[16,24,128]{2,1,0:T(8,128)(2,1)S(1)} %all-to-all-done.3) | copy-start | bytes 294916
  65.6 0.6 copy-start.29
  99.3 14.8 %copy-start.10 = (bf16[1,2048,128]{2,1,0:T(8,128)(2,1)S(1)}, bf16[1,2048,128]{2,1,0:T(8,128)(2,1)}, u32[]{:S(2)}) copy-start(bf16[1,2048,128]{2,1,0:T(8,128)(2,1)} %param.45) | copy-start | bytes 1572868
  99.3 14.2 %all-to-all-start.5 = ((bf16[16,32,1,4,128]{4,1,3,2,0:T(8,128)(2,1)}), bf16[16,32,1,4,128]{4,1,3,2,0:T(8,128)(2,1)S(1)}, u32[]{:S(2)}, u32[]{:S(2)}) async-start(bf16[16,32,1,4,128]{4,1,3,2,0:T(8,128)(2,1)} %broadcast_in_dim.28), calls=%async_computation.5 | async-start | bytes 1048576 | tf_op jit(solution)/shard_map/all_to_all | solution.py:22
  113.5 1.5 copy-start.11
  116.3 4.8 %copy-start.32 = (s32[96,1]{0,1:T(1,128)S(1)}, s32[96,1]{0,1:T(1,128)}, u32[]{:S(2)}) copy-start(s32[96,1]{0,1:T(1,128)} %mul.327) | copy-start | bytes 1156
  116.4 4.8 %copy-start.39 = (f32[96]{0:T(128)S(1)}, f32[96]{0:T(128)}, u32[]{:S(2)}) copy-start(f32[96]{0:T(128)} %copy-done.38) | copy-start | bytes 1156
  116.4 4.8 %copy-start.26 = (f32[24,4]{0,1:T(4,128)S(1)}, f32[24,4]{0,1:T(4,128)}, u32[]{:S(2)}) copy-start(f32[24,4]{0,1:T(4,128)} %param.44) | copy-start | bytes 1156
  116.4 5.5 %copy-start.25 = (bf16[2048]{0:T(1024)(128)(2,1)S(1)}, bf16[2048]{0:T(1024)(128)(2,1)}, u32[]{:S(2)}) copy-start(bf16[2048]{0:T(1024)(128)(2,1)} %param.51) | copy-start | bytes 12292
  117.3 16.3 %all-to-all-start.6 = ((bf16[16,32,1,4,128]{4,1,3,2,0:T(8,128)(2,1)}), bf16[16,32,1,4,128]{4,1,3,2,0:T(8,128)(2,1)S(1)}, u32[]{:S(2)}, u32[]{:S(2)}) async-start(bf16[16,32,1,4,128]{4,1,3,2,0:T(8,128)(2,1)} %bitcast_bitcast_fusion), calls=%async_computation.6 | async-start | bytes 1048576 | tf_op jit(solution)/shard_map/all_to_all | solution.py:51
  125.0 1.8 %copy-start.2 = (f32[24,64,2]{2,1,0:T(8,128)S(1)}, f32[24,64,2]{2,1,0:T(8,128)}, u32[]{:S(2)}) copy-start(f32[24,64,2]{2,1,0:T(8,128)} %copy-done.1) | copy-start | bytes 36868
  128.7 11.3 %copy-start.3 = (f32[24,64,128]{2,1,0:T(8,128)S(1)}, f32[24,64,128]{2,1,0:T(8,128)}, u32[]{:S(2)}) copy-start(f32[24,64,128]{2,1,0:T(8,128)} %param.27) | copy-start | bytes 2359300
  128.7 11.3 %copy-start.13 = (f32[24,128]{1,0:T(8,128)S(1)}, f32[24,128]{1,0:T(8,128)}, u32[]{:S(2)}) copy-start(f32[24,128]{1,0:T(8,128)} %copy-done.12) | copy-start | bytes 36868
  130.5 9.6 %copy-start.4 = (f32[24,64,128]{2,1,0:T(8,128)S(1)}, f32[24,64,128]{2,1,0:T(8,128)}, u32[]{:S(2)}) copy-start(f32[24,64,128]{2,1,0:T(8,128)} %mul.348) | copy-start | bytes 2359300
  133.6 13.1 %all-to-all-start.8 = ((bf16[16,24,128]{2,1,0:T(8,128)(2,1)}), bf16[16,24,128]{2,1,0:T(8,128)(2,1)S(1)}, u32[]{:S(2)}, u32[]{:S(2)}) async-start(bf16[16,24,128]{2,1,0:T(8,128)(2,1)} %bitcast.154), calls=%async_computation.8 | async-start | bytes 196608 | tf_op jit(solution)/shard_map/all_to_all | solution.py:51
  140.1 13.8 %copy-start.6 = (bf16[16,24,128]{2,1,0:T(8,128)(2,1)S(1)}, bf16[16,24,128]{2,1,0:T(8,128)(2,1)}, u32[]{:S(2)}) copy-start(bf16[16,24,128]{2,1,0:T(8,128)(2,1)} %copy-done.5) | copy-start | bytes 294916
  140.1 13.8 %copy-start.22 = (bf16[2048,1]{0,1:T(2,128)(2,1)S(1)}, bf16[2048,1]{0,1:T(2,128)(2,1)}, u32[]{:S(2)}) copy-start(bf16[2048,1]{0,1:T(2,128)(2,1)} %reshape.301) | copy-start | bytes 12292
  140.1 13.8 %copy-start.23 = (f32[16,128]{1,0:T(8,128)S(1)}, f32[16,128]{1,0:T(8,128)}, u32[]{:S(2)}) copy-start(f32[16,128]{1,0:T(8,128)} %get-tuple-element.6) | copy-start | bytes 24580
  140.1 13.8 %copy-start.30 = (f32[24]{0:T(128)S(1)}, f32[24]{0:T(128)}, u32[]{:S(2)}) copy-start(f32[24]{0:T(128)} %copy-done.29) | copy-start | bytes 292
  140.1 26.8 %copy-start.14 = (f32[24,4]{1,0:T(8,128)S(1)}, f32[24,4]{1,0:T(8,128)}, u32[]{:S(2)}) copy-start(f32[24,4]{1,0:T(8,128)} %copy.108) | copy-start | bytes 1156
  146.7 19.4 %all-to-all-start.7 = ((bf16[32,1,4,128]{3,2,1,0:T(4,128)(2,1)}), bf16[32,1,4,128]{3,2,1,0:T(4,128)(2,1)S(1)}, u32[]{:S(2)}, u32[]{:S(2)}) async-start(bf16[32,1,4,128]{3,2,1,0:T(4,128)(2,1)} %copy.106), calls=%async_computation.7 | async-start | bytes 65536 | tf_op jit(solution)/shard_map/all_to_all | solution.py:201
where the time goes:
time: 169 us; the launch traced here: 168 us
  waiting for transfers between devices  45.6 us (27%)
  starting transfers between devices  40.6 us (24%)
  blocking collectives  31.9 us (19%)
  local copies, waits for them, and re-layouts  25.8 us (15%)
  other arithmetic  14.7 us (9%)
  matrix products  7.63 us (5%)
    all_to_all x1, blocking collectives, local(): lax.all_to_all(outgoing, 'ep', split_axis=0, concat_axis=0, tiled=True)  31.9 us
    all_to_all x5, waiting for transfers between devices, sent_to_all(): lax.all_to_all(jnp.broadcast_to(value[None], (count, *value.shape)), axis...  30.2 us
    all_to_all x5, starting transfers between devices, sent_to_all(): lax.all_to_all(jnp.broadcast_to(value[None], (count, *value.shape)), axis...  23.3 us
    all_to_all x1, waiting for transfers between devices, local(): lax.all_to_all(summed, 'ep', split_axis=0, concat_axis=0, tiled=True)  11.9 us
    all_to_all x2, starting transfers between devices, sum_at_owner(): lax.all_to_all(pieces, axis, split_axis=0, concat_axis=0, tiled=True)  10.2 us
    all_to_all x1, starting transfers between devices, local(): lax.all_to_all(summed, 'ep', split_axis=0, concat_axis=0, tiled=True)  7.12 us
    reduce_sum x1, other arithmetic, local(): jnp.sum(state_grid * recept.astype(jnp.float32).reshape(seq_count, 1, hea...  6.56 us
    dot_general x12, matrix products, product(): return jnp.dot(left, right, preferred_element_type=jnp.float32)  5.19 us
  transfers between devices with their start and end apart: 8, of which 7 were waited for; matrix products, arithmetic and copies ran while one was open for 14% of the time, Pallas kernels for 0%

commit v1 on v0

v1 whole, which is shorter than its diff:
```python
import jax
import jax.numpy as jnp
from jax import lax
from jax.experimental import pallas as pl
from jax.experimental.pallas import tpu as pltpu
from jax.sharding import PartitionSpec as P


HEAD = 64
f32 = jnp.float32
bf16 = jnp.bfloat16

norm_eps = 1e-06
head_eps = 0.00064
key_eps = 1e-06


def dot(a, b):
    return jnp.dot(a, b, preferred_element_type=f32)


def split_dot(a, b):
    high = a.astype(bf16)
    low = (a - high.astype(f32)).astype(bf16)
    return dot(high, b) + dot(low, b)


def call(kernel, outs, *args, **kwargs):
    params = pltpu.CompilerParams(vmem_limit_bytes=12 << 20)
    return pl.pallas_call(kernel, out_shape=outs, compiler_params=params, **kwargs)(*args)


def shape(dims, dtype):
    return jax.ShapeDtypeStruct(dims, dtype)


def head_sum(x):
    first = lax.broadcasted_iota(jnp.int32, x.shape, 1) < HEAD
    left = jnp.sum(jnp.where(first, x, 0.0), axis=1, keepdims=True)
    right = jnp.sum(jnp.where(first, 0.0, x), axis=1, keepdims=True)
    return jnp.where(first, left, right)


def same_head():
    rows = lax.broadcasted_iota(jnp.int32, (2 * HEAD, 2 * HEAD), 0) // HEAD
    cols = lax.broadcasted_iota(jnp.int32, (2 * HEAD, 2 * HEAD), 1) // HEAD
    return jnp.where(rows == cols, 1.0, 0.0).astype(bf16)


def own_channel():
    rows = lax.broadcasted_iota(jnp.int32, (HEAD, 2 * HEAD), 0)
    cols = lax.broadcasted_iota(jnp.int32, (HEAD, 2 * HEAD), 1) % HEAD
    return rows == cols


def dot_t(a, b):
    return lax.dot_general(a, b, (((1,), (1,)), ((), ())), preferred_element_type=f32)


def message_kernel(place, tokens, gain, decay_down, iclr_down, out):
    rows = lax.broadcasted_iota(jnp.int32, gain.shape, 0)
    own = jnp.sum(jnp.where(rows == place[0], gain[...].astype(f32), 0.0), axis=0, keepdims=True)
    scaled = (tokens[...].astype(f32) * own).astype(bf16)
    count, seqs, width = out.shape
    rank = decay_down.shape[0]
    pad = jnp.zeros((seqs, width // 3 - rank), f32)
    whole = jnp.concatenate(
        [
            tokens[...].astype(f32),
            dot_t(scaled, decay_down[...]),
            pad,
            dot_t(scaled, iclr_down[...]),
            pad,
        ],
        axis=1,
    ).astype(bf16)
    for p in range(count):
        out[p] = whole


def slot_table(routes, slots):
    top, seqs = routes.shape
    expert = lax.broadcasted_iota(jnp.int32, (slots, seqs), 0) // 4
    matches = [routes[k : k + 1, :] == expert for k in range(top)]
    chosen = jnp.where(matches[0], 1.0, 0.0)
    for match in matches[1:]:
        chosen = chosen + jnp.where(match, 1.0, 0.0)
    earlier = lax.broadcasted_iota(jnp.int32, (seqs, seqs), 0) < lax.broadcasted_iota(
        jnp.int32, (seqs, seqs), 1
    )
    before = dot(chosen.astype(bf16), jnp.where(earlier, 1.0, 0.0).astype(bf16))
    place = (lax.broadcasted_iota(jnp.int32, (slots, seqs), 0) % 4).astype(f32)
    return matches, jnp.where(before == place, chosen, 0.0)


def routing_kernel(routes, hit_out):
    _, hit = slot_table(routes, hit_out.shape[0])
    hit_out[...] = hit.astype(bf16)


def weights_kernel(routes, weights, out):
    matches, hit = slot_table(routes, out.shape[0])
    total = jnp.zeros(out.shape, f32)
    for k, match in enumerate(matches):
        total = total + jnp.where(match, weights[k : k + 1, :], 0.0)
    out[...] = total * hit


def mixer_in_kernel(
    arrived,
    state,
    gain,
    w_recept,
    w_key,
    w_value,
    decay_up,
    decay_base,
    iclr_up,
    iclr_base,
    key_scale,
    key_mix,
    head_gain,
    heads_out,
    vectors_out,
):
    count, seqs, width = arrived.shape
    piece = width // 3
    rank = decay_up.shape[0]
    tokens = [arrived[p, :, :piece].astype(f32) for p in range(count)]
    squares = tokens[0] * tokens[0]
    for x in tokens[1:]:
        squares = squares + x * x
    scale = lax.rsqrt(
        jnp.sum(squares, axis=1, keepdims=True) * (1.0 / (count * piece)) + norm_eps
    )
    first = jnp.concatenate(
        [
            (x * scale * gain[p : p + 1, :].astype(f32)).astype(bf16)
            for p, x in enumerate(tokens)
        ],
        axis=1,
    )
    low = arrived[0, :, piece:].astype(f32)
    for p in range(1, count):
        low = low + arrived[p, :, piece:].astype(f32)
    low = low * scale
    decay_act = jnp.tanh(low[:, :rank]).astype(bf16)
    rate_act = low[:, piece : piece + rank].astype(bf16)
    recept = dot(first, w_recept[...]).astype(bf16).astype(f32)
    key = dot(first, w_key[...]).astype(bf16).astype(f32)
    value = dot(first, w_value[...]).astype(bf16).astype(f32)
    decay_pre = -(decay_base[...] + dot(decay_act, decay_up[...]))
    softplus = jnp.maximum(decay_pre, 0.0) + jnp.log1p(jnp.exp(-jnp.abs(decay_pre)))
    decay = jnp.exp(-jnp.exp(-softplus - 0.5))
    rate = jax.nn.sigmoid(iclr_base[...] + dot(rate_act, iclr_up[...]))
    scaled = key * key_scale[...].astype(f32)
    removal = scaled * lax.rsqrt(head_sum(scaled * scaled) + key_eps)
    written = key * (1.0 + (rate - 1.0) * key_mix[...].astype(f32))
    scaled_removal = removal * rate
    together = same_head()
    own = own_channel()

    def against(weights):
        grid = state[...] * weights[:, None, :]
        spread = split_dot(grid.reshape(seqs * HEAD, piece), together)
        return jnp.sum(jnp.where(own, spread.reshape(seqs, HEAD, piece), 0.0), axis=1)

    recall = against(removal)
    read = (
        against(decay * recept)
        - recall * head_sum(scaled_removal * recept)
        + value * head_sum(written * recept)
    )
    centered = read - head_sum(read) * (1.0 / HEAD)
    variance = head_sum(centered * centered) * (1.0 / HEAD)
    head_out = (centered * lax.rsqrt(variance + head_eps) * head_gain[...].astype(f32)).astype(bf16)
    for p in range(count):
        heads_out[p] = head_out
    for i, v in enumerate((removal, decay, scaled_removal, value, written)):
        vectors_out[i] = v


def state_kernel(state, vectors, out):
    seqs, _, width = state.shape
    removal, decay, scaled_removal, value, written = (
        vectors[i][:, None, :] for i in range(5)
    )
    together = same_head()
    grid = state[...]
    recall = split_dot((grid * removal).reshape(seqs * HEAD, width), together)
    spread = jnp.where(own_channel(), value, 0.0).astype(bf16).reshape(seqs * HEAD, width)
    values = dot(spread, together)
    out[...] = (
        grid * decay
        - recall.reshape(seqs, HEAD, width) * scaled_removal
        + values.reshape(seqs, HEAD, width) * written
    )


def dispatch_kernel(heads, w_out, tokens, hit, residual_out, outgoing):
    count = heads.shape[0]
    rows = jnp.concatenate([heads[p] for p in range(count)], axis=1)
    mixed = dot(rows, w_out[...]).astype(bf16).astype(f32)
    residual = (tokens[...].astype(f32) + mixed).astype(bf16)
    residual_out[...] = residual
    outgoing[...] = dot(hit[...], residual).astype(bf16)


def spread_kernel(arrived, residual, out):
    slots = arrived.shape[0]
    for p in range(out.shape[0]):
        out[p, :slots] = arrived[...]
        out[p, slots:] = residual[...]


def expert_kernel(
    arrived, gain, gate, up, down, dense_gate, dense_up, dense_down, out, dense_rows_out
):
    count, rows, piece = arrived.shape
    slots = rows - dense_rows_out.shape[0]
    pieces = [arrived[p].astype(f32) for p in range(count)]
    squares = pieces[0] * pieces[0]
    for x in pieces[1:]:
        squares = squares + x * x
    scale = lax.rsqrt(
        jnp.sum(squares, axis=1, keepdims=True) * (1.0 / (count * piece)) + norm_eps
    )
    normed = [
        (x * scale * gain[p : p + 1, :].astype(f32)).astype(bf16) for p, x in enumerate(pieces)
    ]
    second = jnp.concatenate(normed, axis=1)
    routed, dense = second[:slots], second[slots:]
    hidden = (jax.nn.silu(dot(routed, gate[...])) * dot(routed, up[...])).astype(bf16)
    dense_hidden = (
        jax.nn.silu(dot_t(dense, dense_gate[...])) * dot_t(dense, dense_up[...])
    ).astype(bf16)
    for p in range(count):
        cols = slice(p * piece, (p + 1) * piece)
        out[p, :slots] = dot(hidden, down[:, cols]).astype(bf16)
        out[p, slots:] = dot(dense_hidden, dense_down[:, cols]).astype(bf16)
    dense_rows_out[...] = dense


def mix_kernel(rows, weights, out):
    count, width = weights.shape
    mix = jnp.zeros(out.shape, f32)
    for p in range(count):
        mix = mix + rows[:, p * width : (p + 1) * width].astype(f32) * weights[
            p : p + 1, :
        ].astype(f32)
    mix = jax.nn.sigmoid(jnp.sum(mix, axis=1, keepdims=True))
    out[...] = jnp.broadcast_to(mix, out.shape)


def total_kernel(partial, expert_out, dense_out):
    count = partial.shape[0]
    slots = expert_out.shape[0]
    total = partial[0].astype(f32)
    for p in range(1, count):
        total = total + partial[p].astype(f32)
    expert_out[...] = total[:slots].astype(bf16)
    dense_out[...] = total[slots:]


def base_kernel(residual, mix, dense, out):
    out[...] = residual[...].astype(f32) + mix[...] * dense[...]


def final_kernel(returned, weights, base, out):
    high = weights[...].astype(bf16)
    rest = weights[...] - high.astype(f32)
    middle = rest.astype(bf16)
    low = (rest - middle.astype(f32)).astype(bf16)
    values = returned[...]
    total = base[...]
    for part in (low, middle, high):
        total = total + lax.dot_general(
            part, values, (((0,), (0,)), ((), ())), preferred_element_type=f32
        )
    out[...] = total.astype(bf16)


def exchange(value, axis):
    return lax.all_to_all(value, axis, 0, 0, tiled=True)


def near(dims, dtype):
    return pltpu.VMEM(dims, dtype)


def held(*values):
    return [pltpu.with_memory_space_constraint(v, pltpu.VMEM) for v in values]


def local(
    token_rows,
    prior_state,
    first_gain,
    w_recept,
    w_key,
    w_value,
    decay_down,
    decay_up,
    decay_base,
    iclr_down,
    iclr_up,
    iclr_base,
    key_scale,
    key_mix,
    head_gain,
    w_out,
    second_gain,
    routes,
    route_weights,
    exp_gate,
    exp_up,
    exp_down,
    dense_gate,
    dense_up,
    dense_down,
    dense_mix,
):
    seqs, width = token_rows.shape
    count = lax.axis_size("tp")
    groups = lax.axis_size("ep")
    slots = groups * 4
    rows = slots + seqs
    place = lax.axis_index("tp").reshape(1).astype(jnp.int32)
    row = lambda v: v.reshape(1, width)
    pieces = lambda v: v.reshape(count, width)
    in_smem = pl.BlockSpec(memory_space=pltpu.SMEM)
    in_vmem = pl.BlockSpec(memory_space=pltpu.VMEM)
    message = call(
        message_kernel,
        near((count, seqs, 3 * width), bf16),
        place,
        *held(token_rows, pieces(first_gain), decay_down.T, iclr_down.T),
        in_specs=[in_smem] + [in_vmem] * 4,
    )
    arrived = exchange(message, "tp")
    hit = call(routing_kernel, near((slots, seqs), bf16), *held(routes.T))
    heads, vectors = call(
        mixer_in_kernel,
        (near((count, seqs, width), bf16), near((5, seqs, width), f32)),
        *held(
            arrived,
            prior_state,
            pieces(first_gain),
            w_recept,
            w_key,
            w_value,
            decay_up,
            row(decay_base),
            iclr_up,
            row(iclr_base),
            row(key_scale),
            row(key_mix),
            row(head_gain),
        ),
    )
    heads_all = exchange(heads, "tp")
    block = 8
    next_state = call(
        state_kernel,
        shape(prior_state.shape, f32),
        prior_state,
        vectors,
        grid=(seqs // block,),
        in_specs=[
            pl.BlockSpec((block, HEAD, width), lambda i: (i, 0, 0)),
            pl.BlockSpec((5, block, width), lambda i: (0, i, 0)),
        ],
        out_specs=pl.BlockSpec((block, HEAD, width), lambda i: (i, 0, 0)),
    )
    residual, outgoing = call(
        dispatch_kernel,
        (near((seqs, width), bf16), shape((slots, width), bf16)),
        *held(heads_all, w_out, token_rows, hit),
    )
    sent = exchange(outgoing.reshape(groups, 4, width), "ep").reshape(slots, width)
    slot_weights = call(weights_kernel, near((slots, seqs), f32), *held(routes.T, route_weights.T))
    gathered = exchange(
        call(spread_kernel, shape((count, rows, width), bf16), *held(sent, residual)), "tp"
    )
    partial, dense_rows = call(
        expert_kernel,
        (shape((count, rows, width), bf16), near((seqs, count * width), bf16)),
        *held(
            gathered,
            pieces(second_gain),
            exp_gate[0],
            exp_up[0],
            exp_down[0],
            dense_gate.T,
            dense_up.T,
            dense_down,
        ),
    )
    mix = call(mix_kernel, near((seqs, width), f32), *held(dense_rows, pieces(dense_mix)))
    expert_out, dense_out = call(
        total_kernel,
        (shape((slots, width), bf16), near((seqs, width), f32)),
        *held(exchange(partial, "tp")),
    )
    base = call(base_kernel, near((seqs, width), f32), *held(residual, mix, dense_out))
    returned = exchange(expert_out.reshape(groups, 4, width), "ep")
    layer_out = call(
        final_kernel,
        shape((seqs, width), bf16),
        *held(returned.reshape(slots, width), slot_weights, base),
    )
    return (layer_out, next_state)


def solution(mesh):
    in_specs = (
        P("ep", "tp"),
        P("ep", None, "tp"),
        P(),
        P(None, "tp"),
        P(None, "tp"),
        P(None, "tp"),
        P("tp", None),
        P(None, "tp"),
        P("tp"),
        P("tp", None),
        P(None, "tp"),
        P("tp"),
        P("tp"),
        P("tp"),
        P("tp"),
        P(None, "tp"),
        P(),
        P("ep", None),
        P("ep", None),
        P("ep", None, "tp"),
        P("ep", None, "tp"),
        P("ep", "tp", None),
        P(None, "tp"),
        P(None, "tp"),
        P("tp", None),
        P(),
    )
    out_specs = (P("ep", "tp"), P("ep", None, "tp"))
    return jax.shard_map(local, mesh=mesh, in_specs=in_specs, out_specs=out_specs, check_vma=False)
```

time: 169 us -> 117 us (0.69)
  blocking collectives: 31.9 us -> 72.9 us
  starting transfers between devices: 40.6 us -> 11.1 us
  waiting for transfers between devices: 45.6 us -> 16.2 us
  local copies, waits for them, and re-layouts: 25.8 us -> 7.42 us
  other arithmetic: 14.7 us -> 0 us
  matrix products: 7.63 us -> 0 us
  Pallas kernels: 0 us -> 7.35 us
    all_to_all x1 -> x4, blocking collectives: 31.9 us -> 72.9 us  [exchange(): return lax.all_to_all(value, axis, 0, 0, tiled=True)]
    all_to_all x8 -> x2, starting transfers between devices: 40.6 us -> 11.1 us  [exchange(): return lax.all_to_all(value, axis, 0, 0, tiled=True)]
    all_to_all x8 -> x2, waiting for transfers between devices: 45.6 us -> 16.2 us  [exchange(): return lax.all_to_all(value, axis, 0, 0, tiled=True)]
    reduce_sum x11 -> x0, other arithmetic: 9.3 us -> none  [the longest x1 6.56 us: local(): jnp.sum(state_grid * recept.astype(jnp.float32).reshape(seq_count, 1, hea...]
    mul x12 -> x0, local copies, waits for them, and re-layouts: 9.08 us -> none  [the longest x3 3.74 us: local(): value_cols[..., None] * written[:, None]]
    dot_general x15 -> x0, matrix products: 7.63 us -> none  [the longest x12 5.19 us: product(): return jnp.dot(left, right, preferred_element_type=jnp.float32)]
    pallas_call x0 -> x12, Pallas kernels: none -> 7.35 us  [call(): pl.pallas_call(kernel, out_shape=outs, compiler_params=params, **kwargs)]
    broadcast_in_dim x7 -> x0, local copies, waits for them, and re-layouts: 4.54 us -> none  [the longest x6 4.53 us: sent_to_all(): jnp.broadcast_to(value[None], (count, *value.shape))]
  transfers between devices with their start and end apart: 8 -> 2, of which waited for: 7 -> 2; matrix products, arithmetic and copies ran while one was open for 14% -> 0% of each run, Pallas kernels for 0% -> 2%
where the time goes in v1:
time: 117 us; the launch traced here: 116 us
  blocking collectives  72.9 us (62%)
  waiting for transfers between devices  16.2 us (14%)
  starting transfers between devices  11.1 us (9%)
  local copies, waits for them, and re-layouts  7.42 us (6%)
  Pallas kernels  7.35 us (6%)
    all_to_all x4, blocking collectives, exchange(): return lax.all_to_all(value, axis, 0, 0, tiled=True)  72.9 us
    all_to_all x2, waiting for transfers between devices, exchange(): return lax.all_to_all(value, axis, 0, 0, tiled=True)  16.2 us
    all_to_all x2, starting transfers between devices, exchange(): return lax.all_to_all(value, axis, 0, 0, tiled=True)  11.1 us
    unnamed x56, local copies, waits for them, and re-layouts  7.42 us
    pallas_call x12, Pallas kernels, call(): pl.pallas_call(kernel, out_shape=outs, compiler_params=params, **kwargs)  7.35 us
  transfers between devices with their start and end apart: 2, of which 2 were waited for; matrix products, arithmetic and copies ran while one was open for 0% of the time, Pallas kernels for 2%

profile of v1, /device:TPU:1, one launch (start us, length us, event | category | flops | bytes accessed | tf_op | source)
XLA Modules:
  0.0 115.9 jit_solution(10377405312582774467)
XLA Ops:
  0.6 0.0 copy-start
  0.6 0.0 copy-start.13
  0.7 0.8 copy-done.13
  1.4 0.0 copy-start.15
  1.4 0.7 copy-done.15
  2.1 0.0 copy-start.16
  2.1 0.7 copy-done.16
  2.9 0.0 copy-start.17
  2.9 0.7 copy-done.17
  3.6 0.2 shard_map.257
  3.7 0.0 copy-start.11
  3.8 0.0 copy-start.12
  3.8 0.0 copy-start.26
  3.8 0.0 copy-start.27
  3.8 15.2 %all_to_all.30.arrived = bf16[16,24,384]{2,1,0:T(8,128)(2,1)S(1)} all-to-all(bf16[16,24,384]{2,1,0:T(8,128)(2,1)S(1)} %shard_map.257), channel_id=1, replica_groups=mesh['ep'=32,'tp'=16] {'tp'}, dimensions={0} | all-to-all | bytes 589824 | tf_op jit(solution)/shard_map/all_to_all | solution.py:284
  19.0 0.0 copy-start.18
  19.0 0.0 copy-start.23
  19.0 0.0 copy-start.24
  19.0 0.0 copy-done
  19.0 0.0 copy-done.11
  19.0 0.0 copy-done.12
  19.1 0.0 copy-done.26
  19.1 0.0 copy-done.27
  19.1 0.6 copy-done.18
  19.7 0.0 copy-done.23
  19.7 0.0 copy-done.24
  19.7 0.0 copy-done.25
  19.7 1.0 copy-done.1
  20.8 1.0 copy-done.2
  21.8 1.0 copy-done.3
  22.8 1.9 %shard_map.258 = (bf16[16,24,128]{2,1,0:T(8,128)(2,1)}, f32[5,24,128]{2,1,0:T(8,128)S(1)}) custom-call(bf16[16,24,384]{2,1,0:T(8,128)(2,1)S(1)} %all_to_all.30.arrived, f32[24,64,128]{2,1,0:T(8,128)S(1)} %copy-done, bf16[16,128]{1,0:T(8,128)(2,1)S(1)} %bitcast.33, bf16[2048,128]{1,0:T(8,128)(2,1)S(1)} %copy-done.1, bf16[2048,128]{1,0:T(8,128)(2,1)S(1)} %copy-done.2, ...), custom_call_target="tpu_custom_call" | custom-call | tf_op jit(solution)/shard_map/pallas_call | solution.py:30
  24.7 3.6 %all-to-all-start.1 = ((bf16[16,24,128]{2,1,0:T(8,128)(2,1)}), bf16[16,24,128]{2,1,0:T(8,128)(2,1)S(1)}, u32[]{:S(2)}, u32[]{:S(2)}) async-start(bf16[16,24,128]{2,1,0:T(8,128)(2,1)} %get-tuple-element.10), calls=%async_computation.1 | async-start | bytes 196608 | tf_op jit(solution)/shard_map/all_to_all | solution.py:284
  28.4 0.0 copy-done.19
  28.4 0.0 copy-start.14
  28.4 0.2 shard_map.259.hit
  28.5 6.5 %all-to-all-done.1.heads = bf16[16,24,128]{2,1,0:T(8,128)(2,1)S(1)} async-done(((bf16[16,24,128]{2,1,0:T(8,128)(2,1)}), bf16[16,24,128]{2,1,0:T(8,128)(2,1)S(1)}, u32[]{:S(2)}, u32[]{:S(2)}) %all-to-all-start.1) | async-done | bytes 98336 | tf_op jit(solution)/shard_map/all_to_all | solution.py:284
  35.0 0.0 copy-done.7
  35.0 0.0 copy-done.14
  35.0 0.3 shard_map.260
  35.3 30.6 %all_to_all.31 = bf16[32,4,128]{2,1,0:T(4,128)(2,1)S(1)} all-to-all(bf16[32,4,128]{2,1,0:T(4,128)(2,1)S(1)} %bitcast.29), channel_id=1, replica_groups=mesh['ep'=32,'tp'=16] {'ep'}, dimensions={0} | all-to-all | bytes 65536 | tf_op jit(solution)/shard_map/all_to_all | solution.py:284
  66.0 0.1 shard_map.261
  66.1 0.0 copy-start.4
  66.1 0.0 copy-start.5
  66.1 0.0 copy-start.8
  66.1 14.3 %all_to_all.32.arrived = bf16[16,152,128]{2,1,0:T(8,128)(2,1)S(1)} all-to-all(bf16[16,152,128]{2,1,0:T(8,128)(2,1)S(1)} %shard_map.261), channel_id=1, replica_groups=mesh['ep'=32,'tp'=16] {'tp'}, dimensions={0} | all-to-all | bytes 1245184 | tf_op jit(solution)/shard_map/all_to_all | solution.py:284
  80.4 0.0 copy-done.10
  80.4 0.0 copy-done.6
  80.4 0.0 copy-done.9
  80.4 0.0 copy-done.4
  80.4 0.0 copy-done.5
  80.4 0.0 copy-done.8
  80.4 0.6 copy-done.20
  81.1 1.1 shard_map.262
  82.2 12.8 %all_to_all.33.partial = bf16[16,152,128]{2,1,0:T(8,128)(2,1)S(1)} all-to-all(bf16[16,152,128]{2,1,0:T(8,128)(2,1)S(1)} %get-tuple-element.13), channel_id=1, replica_groups=mesh['ep'=32,'tp'=16] {'tp'}, dimensions={0} | all-to-all | bytes 1245184 | tf_op jit(solution)/shard_map/all_to_all | solution.py:284
  94.9 0.7 shard_map.263
  95.6 7.4 %all-to-all-start.5 = ((bf16[32,4,128]{2,1,0:T(4,128)(2,1)}), bf16[32,4,128]{2,1,0:T(4,128)(2,1)S(1)}, u32[]{:S(2)}, u32[]{:S(2)}) async-start(bf16[32,4,128]{2,1,0:T(4,128)(2,1)} %bitcast.18), calls=%async_computation.5 | async-start | bytes 65536 | tf_op jit(solution)/shard_map/all_to_all | solution.py:284
  103.1 0.0 copy-done.22
  103.1 0.2 shard_map.264.weights
  103.2 0.0 copy-start.21
  103.2 2.0 %shard_map.268 = f32[24,64,128]{2,1,0:T(8,128)} custom-call(f32[24,64,128]{2,1,0:T(8,128)S(1)} %copy-done, f32[5,24,128]{2,1,0:T(8,128)S(1)} %get-tuple-element.17.vectors), custom_call_target="tpu_custom_call" | custom-call | tf_op jit(solution)/shard_map/pallas_call | solution.py:30
  105.2 0.0 copy-done.21
  105.2 0.1 shard_map.265.mix
  105.3 9.8 %all-to-all-done.5 = bf16[32,4,128]{2,1,0:T(4,128)(2,1)S(1)} async-done(((bf16[32,4,128]{2,1,0:T(4,128)(2,1)}), bf16[32,4,128]{2,1,0:T(4,128)(2,1)S(1)}, u32[]{:S(2)}, u32[]{:S(2)}) %all-to-all-start.5) | async-done | bytes 32800 | tf_op jit(solution)/shard_map/all_to_all | solution.py:284
  115.1 0.8 shard_map.267
  (12 shorter events, 0.0 us)
Async XLA Ops:
  0.6 18.4 %copy-start = (f32[24,64,128]{2,1,0:T(8,128)S(1)}, f32[24,64,128]{2,1,0:T(8,128)}, u32[]{:S(2)}) copy-start(f32[24,64,128]{2,1,0:T(8,128)} %state.3) | copy-start | bytes 2359300
  0.6 0.8 copy-start.13
  1.4 0.7 copy-start.15
  2.1 0.7 copy-start.16
  2.9 0.7 copy-start.17
  3.7 15.3 %copy-start.11 = (bf16[96,128]{1,0:T(8,128)(2,1)S(1)}, bf16[96,128]{1,0:T(8,128)(2,1)}, u32[]{:S(2)}) copy-start(bf16[96,128]{1,0:T(8,128)(2,1)} %decay_up.1) | copy-start | bytes 73732
  3.8 15.3 %copy-start.12 = (bf16[96,128]{1,0:T(8,128)(2,1)S(1)}, bf16[96,128]{1,0:T(8,128)(2,1)}, u32[]{:S(2)}) copy-start(bf16[96,128]{1,0:T(8,128)(2,1)} %iclr_up.1) | copy-start | bytes 73732
  3.8 15.3 %copy-start.26 = (bf16[128]{0:T(256)(128)(2,1)S(1)}, bf16[128]{0:T(256)(128)(2,1)}, u32[]{:S(2)}) copy-start(bf16[128]{0:T(256)(128)(2,1)} %param.39) | copy-start | bytes 772
  3.8 15.3 %copy-start.27 = (bf16[128]{0:T(256)(128)(2,1)S(1)}, bf16[128]{0:T(256)(128)(2,1)}, u32[]{:S(2)}) copy-start(bf16[128]{0:T(256)(128)(2,1)} %param.40) | copy-start | bytes 772
  19.0 0.7 copy-start.18
  19.0 0.7 copy-start.23
  19.0 0.7 copy-start.24
  19.0 0.7 copy-start.25
  19.7 1.0 copy-start.1
  20.8 1.0 copy-start.2
  21.8 1.0 copy-start.3
  22.8 12.1 %copy-start.7 = (bf16[2048,128]{1,0:T(8,128)(2,1)S(1)}, bf16[2048,128]{1,0:T(8,128)(2,1)}, u32[]{:S(2)}) copy-start(bf16[2048,128]{1,0:T(8,128)(2,1)} %w_out.1) | copy-start | bytes 1572868
  24.7 3.7 %copy-start.19 = (s32[24,4]{0,1:T(4,128)S(1)}, s32[24,4]{0,1:T(4,128)}, u32[]{:S(2)}) copy-start(s32[24,4]{0,1:T(4,128)} %param.43) | copy-start | bytes 1156
  24.7 10.3 %all-to-all-start.1 = ((bf16[16,24,128]{2,1,0:T(8,128)(2,1)}), bf16[16,24,128]{2,1,0:T(8,128)(2,1)S(1)}, u32[]{:S(2)}, u32[]{:S(2)}) async-start(bf16[16,24,128]{2,1,0:T(8,128)(2,1)} %get-tuple-element.10), calls=%async_computation.1 | async-start | bytes 196608 | tf_op jit(solution)/shard_map/all_to_all | solution.py:284
  28.4 6.6 %copy-start.14 = (bf16[24,128]{1,0:T(8,128)(2,1)S(1)}, bf16[24,128]{1,0:T(8,128)(2,1)}, u32[]{:S(2)}) copy-start(bf16[24,128]{1,0:T(8,128)(2,1)} %tokens.3) | copy-start | bytes 18436
  35.3 45.1 %copy-start.10 = (bf16[32,2048]{1,0:T(8,128)(2,1)S(1)}, bf16[32,2048]{1,0:T(8,128)(2,1)}, u32[]{:S(2)}) copy-start(bf16[32,2048]{1,0:T(8,128)(2,1)} %dense_down.1) | copy-start | bytes 393220
  66.0 14.4 %copy-start.6 = (bf16[1,128,2048]{2,1,0:T(8,128)(2,1)S(1)}, bf16[1,128,2048]{2,1,0:T(8,128)(2,1)}, u32[]{:S(2)}) copy-start(bf16[1,128,2048]{2,1,0:T(8,128)(2,1)} %param.47) | copy-start | bytes 1572868
  66.0 14.4 %copy-start.9 = (bf16[2048,32]{0,1:T(8,128)(2,1)S(1)}, bf16[2048,32]{0,1:T(8,128)(2,1)}, u32[]{:S(2)}) copy-start(bf16[2048,32]{0,1:T(8,128)(2,1)} %param.49) | copy-start | bytes 393220
  66.1 14.3 %copy-start.4 = (bf16[1,2048,128]{2,1,0:T(8,128)(2,1)S(1)}, bf16[1,2048,128]{2,1,0:T(8,128)(2,1)}, u32[]{:S(2)}) copy-start(bf16[1,2048,128]{2,1,0:T(8,128)(2,1)} %param.45) | copy-start | bytes 1572868
  66.1 14.3 %copy-start.5 = (bf16[1,2048,128]{2,1,0:T(8,128)(2,1)S(1)}, bf16[1,2048,128]{2,1,0:T(8,128)(2,1)}, u32[]{:S(2)}) copy-start(bf16[1,2048,128]{2,1,0:T(8,128)(2,1)} %param.46) | copy-start | bytes 1572868
  66.1 14.3 %copy-start.8 = (bf16[2048,32]{0,1:T(8,128)(2,1)S(1)}, bf16[2048,32]{0,1:T(8,128)(2,1)}, u32[]{:S(2)}) copy-start(bf16[2048,32]{0,1:T(8,128)(2,1)} %param.48) | copy-start | bytes 393220
  80.4 0.7 copy-start.20
  94.9 8.1 %copy-start.22 = (f32[24,4]{0,1:T(4,128)S(1)}, f32[24,4]{0,1:T(4,128)}, u32[]{:S(2)}) copy-start(f32[24,4]{0,1:T(4,128)} %param.44) | copy-start | bytes 1156
  95.6 19.5 %all-to-all-start.5 = ((bf16[32,4,128]{2,1,0:T(4,128)(2,1)}), bf16[32,4,128]{2,1,0:T(4,128)(2,1)S(1)}, u32[]{:S(2)}, u32[]{:S(2)}) async-start(bf16[32,4,128]{2,1,0:T(4,128)(2,1)} %bitcast.18), calls=%async_computation.5 | async-start | bytes 65536 | tf_op jit(solution)/shard_map/all_to_all | solution.py:284
  103.2 2.0 %copy-start.21 = (bf16[2048]{0:T(1024)(128)(2,1)S(1)}, bf16[2048]{0:T(1024)(128)(2,1)}, u32[]{:S(2)}) copy-start(bf16[2048]{0:T(1024)(128)(2,1)} %param.51) | copy-start | bytes 12292

commit v2 on v1

--- a/solution.py
+++ b/solution.py
@@ -10,6 +10,8 @@
 f32 = jnp.float32
 bf16 = jnp.bfloat16
 
+FIRST = {"tp": 10, "ep": 17}
+
 norm_eps = 1e-06
 head_eps = 0.00064
 key_eps = 1e-06
@@ -27,7 +29,9 @@
 
 def call(kernel, outs, *args, **kwargs):
     params = pltpu.CompilerParams(vmem_limit_bytes=12 << 20)
-    return pl.pallas_call(kernel, out_shape=outs, compiler_params=params, **kwargs)(*args)
+    return pl.pallas_call(
+        kernel, out_shape=outs, compiler_params=params, **kwargs
+    )(*args)
 
 
 def shape(dims, dtype):
@@ -80,7 +84,7 @@
 
 def slot_table(routes, slots):
     top, seqs = routes.shape
-    expert = lax.broadcasted_iota(jnp.int32, (slots, seqs), 0) // 4
+    expert = (lax.broadcasted_iota(jnp.int32, (slots, seqs), 0) // 4 + FIRST["ep"]) % (slots // 4)
     matches = [routes[k : k + 1, :] == expert for k in range(top)]
     chosen = jnp.where(matches[0], 1.0, 0.0)
     for match in matches[1:]:
@@ -93,12 +97,44 @@
     return matches, jnp.where(before == place, chosen, 0.0)
 
 
-def routing_kernel(routes, hit_out):
+def prep_kernel(
+    w_recept,
+    w_key,
+    w_value,
+    decay_up,
+    iclr_up,
+    state,
+    routes,
+    gain,
+    decay_base,
+    iclr_base,
+    key_scale,
+    key_mix,
+    head_gain,
+    weights_out,
+    ups_out,
+    state_out,
+    hit_out,
+    gain_out,
+    rows_out,
+    sems,
+):
+    moves = [(w, weights_out.at[i]) for i, w in enumerate((w_recept, w_key, w_value))]
+    moves += [(decay_up, ups_out.at[0]), (iclr_up, ups_out.at[1]), (state, state_out)]
+    copies = [pltpu.make_async_copy(a, b, sems.at[i]) for i, (a, b) in enumerate(moves)]
+    for copy in copies:
+        copy.start()
     _, hit = slot_table(routes, hit_out.shape[0])
     hit_out[...] = hit.astype(bf16)
-
-
-def weights_kernel(routes, weights, out):
+    gain_out[...] = gain[...].astype(f32)
+    for i, row in enumerate((decay_base, iclr_base, key_scale, key_mix, head_gain)):
+        rows_out[i : i + 1, :] = row[...].astype(f32)
+    for copy in copies:
+        copy.wait()
+
+
+def weights_kernel(routes, weights, gain, out, gain_out):
+    gain_out[...] = gain[...].astype(f32)
     matches, hit = slot_table(routes, out.shape[0])
     total = jnp.zeros(out.shape, f32)
     for k, match in enumerate(matches):
@@ -107,26 +143,13 @@
 
 
 def mixer_in_kernel(
-    arrived,
-    state,
-    gain,
-    w_recept,
-    w_key,
-    w_value,
-    decay_up,
-    decay_base,
-    iclr_up,
-    iclr_base,
-    key_scale,
-    key_mix,
-    head_gain,
-    heads_out,
-    vectors_out,
+    arrived, state, gain, weights, ups, rows, heads_out, vectors_out
 ):
     count, seqs, width = arrived.shape
     piece = width // 3
-    rank = decay_up.shape[0]
-    tokens = [arrived[p, :, :piece].astype(f32) for p in range(count)]
+    rank = ups.shape[1]
+    decay_base, iclr_base, key_scale, key_mix, head_gain = (rows[i : i + 1, :] for i in range(5))
+    tokens = [x[:, :piece].astype(f32) for x in by_feature(arrived, count)]
     squares = tokens[0] * tokens[0]
     for x in tokens[1:]:
         squares = squares + x * x
@@ -135,7 +158,7 @@
     )
     first = jnp.concatenate(
         [
-            (x * scale * gain[p : p + 1, :].astype(f32)).astype(bf16)
+            (x * scale * gain[p : p + 1, :]).astype(bf16)
             for p, x in enumerate(tokens)
         ],
         axis=1,
@@ -146,16 +169,16 @@
     low = low * scale
     decay_act = jnp.tanh(low[:, :rank]).astype(bf16)
     rate_act = low[:, piece : piece + rank].astype(bf16)
-    recept = dot(first, w_recept[...]).astype(bf16).astype(f32)
-    key = dot(first, w_key[...]).astype(bf16).astype(f32)
-    value = dot(first, w_value[...]).astype(bf16).astype(f32)
-    decay_pre = -(decay_base[...] + dot(decay_act, decay_up[...]))
+    recept = dot(first, weights[0]).astype(bf16).astype(f32)
+    key = dot(first, weights[1]).astype(bf16).astype(f32)
+    value = dot(first, weights[2]).astype(bf16).astype(f32)
+    decay_pre = -(decay_base + dot(decay_act, ups[0]))
     softplus = jnp.maximum(decay_pre, 0.0) + jnp.log1p(jnp.exp(-jnp.abs(decay_pre)))
     decay = jnp.exp(-jnp.exp(-softplus - 0.5))
-    rate = jax.nn.sigmoid(iclr_base[...] + dot(rate_act, iclr_up[...]))
-    scaled = key * key_scale[...].astype(f32)
+    rate = jax.nn.sigmoid(iclr_base + dot(rate_act, ups[1]))
+    scaled = key * key_scale
     removal = scaled * lax.rsqrt(head_sum(scaled * scaled) + key_eps)
-    written = key * (1.0 + (rate - 1.0) * key_mix[...].astype(f32))
+    written = key * (1.0 + (rate - 1.0) * key_mix)
     scaled_removal = removal * rate
     together = same_head()
     own = own_channel()
@@ -173,7 +196,7 @@
     )
     centered = read - head_sum(read) * (1.0 / HEAD)
     variance = head_sum(centered * centered) * (1.0 / HEAD)
-    head_out = (centered * lax.rsqrt(variance + head_eps) * head_gain[...].astype(f32)).astype(bf16)
+    head_out = (centered * lax.rsqrt(variance + head_eps) * head_gain).astype(bf16)
     for p in range(count):
         heads_out[p] = head_out
     for i, v in enumerate((removal, decay, scaled_removal, value, written)):
@@ -199,7 +222,7 @@
 
 def dispatch_kernel(heads, w_out, tokens, hit, residual_out, outgoing):
     count = heads.shape[0]
-    rows = jnp.concatenate([heads[p] for p in range(count)], axis=1)
+    rows = jnp.concatenate([x[...] for x in by_feature(heads, count)], axis=1)
     mixed = dot(rows, w_out[...]).astype(bf16).astype(f32)
     residual = (tokens[...].astype(f32) + mixed).astype(bf16)
     residual_out[...] = residual
@@ -218,7 +241,7 @@
 ):
     count, rows, piece = arrived.shape
     slots = rows - dense_rows_out.shape[0]
-    pieces = [arrived[p].astype(f32) for p in range(count)]
+    pieces = [x[...].astype(f32) for x in by_feature(arrived, count)]
     squares = pieces[0] * pieces[0]
     for x in pieces[1:]:
         squares = squares + x * x
@@ -226,7 +249,7 @@
         jnp.sum(squares, axis=1, keepdims=True) * (1.0 / (count * piece)) + norm_eps
     )
     normed = [
-        (x * scale * gain[p : p + 1, :].astype(f32)).astype(bf16) for p, x in enumerate(pieces)
+        (x * scale * gain[p : p + 1, :]).astype(bf16) for p, x in enumerate(pieces)
     ]
     second = jnp.concatenate(normed, axis=1)
     routed, dense = second[:slots], second[slots:]
@@ -234,8 +257,8 @@
     dense_hidden = (
         jax.nn.silu(dot_t(dense, dense_gate[...])) * dot_t(dense, dense_up[...])
     ).astype(bf16)
-    for p in range(count):
-        cols = slice(p * piece, (p + 1) * piece)
+    for p, t in enumerate(member_order(count, "tp")):
+        cols = slice(t * piece, (t + 1) * piece)
         out[p, :slots] = dot(hidden, down[:, cols]).astype(bf16)
         out[p, slots:] = dot(dense_hidden, dense_down[:, cols]).astype(bf16)
     dense_rows_out[...] = dense
@@ -280,12 +303,25 @@
     out[...] = total.astype(bf16)
 
 
+def member_order(count, axis):
+    return [(i + FIRST[axis]) % count for i in range(count)]
+
+
+def by_feature(ref, count):
+    return [ref.at[(t - FIRST["tp"]) % count] for t in range(count)]
+
+
 def exchange(value, axis):
-    return lax.all_to_all(value, axis, 0, 0, tiled=True)
+    order = member_order(lax.axis_size(axis), axis)
+    return lax.all_to_all(value, axis, 0, 0, tiled=True, axis_index_groups=[order])
 
 
 def near(dims, dtype):
     return pltpu.VMEM(dims, dtype)
+
+
+def far(*values):
+    return [pltpu.with_memory_space_constraint(v, pltpu.HBM) for v in values]
 
 
 def held(*values):
@@ -332,39 +368,52 @@
     in_vmem = pl.BlockSpec(memory_space=pltpu.VMEM)
     message = call(
         message_kernel,
-        near((count, seqs, 3 * width), bf16),
+        shape((count, seqs, 3 * width), bf16),
         place,
-        *held(token_rows, pieces(first_gain), decay_down.T, iclr_down.T),
+        *far(token_rows, pieces(first_gain), decay_down.T, iclr_down.T),
         in_specs=[in_smem] + [in_vmem] * 4,
     )
     arrived = exchange(message, "tp")
-    hit = call(routing_kernel, near((slots, seqs), bf16), *held(routes.T))
-    heads, vectors = call(
-        mixer_in_kernel,
-        (near((count, seqs, width), bf16), near((5, seqs, width), f32)),
-        *held(
-            arrived,
-            prior_state,
-            pieces(first_gain),
+    weights, ups, state, hit, gain, rows_of = call(
+        prep_kernel,
+        (
+            near((3, *w_key.shape), bf16),
+            near((2, *decay_up.shape), bf16),
+            near(prior_state.shape, f32),
+            near((slots, seqs), bf16),
+            near((count, width), f32),
+            near((8, width), f32),
+        ),
+        *far(
             w_recept,
             w_key,
             w_value,
             decay_up,
+            iclr_up,
+            prior_state,
+            routes.T,
+            pieces(first_gain),
             row(decay_base),
-            iclr_up,
             row(iclr_base),
             row(key_scale),
             row(key_mix),
             row(head_gain),
         ),
+        in_specs=[pl.BlockSpec(memory_space=pl.ANY)] * 6 + [in_vmem] * 7,
+        scratch_shapes=[pltpu.SemaphoreType.DMA((6,))],
+    )
+    heads, vectors = call(
+        mixer_in_kernel,
+        (near((count, seqs, width), bf16), near((5, seqs, width), f32)),
+        *held(arrived, state, gain, weights, ups, rows_of),
     )
     heads_all = exchange(heads, "tp")
     block = 8
     next_state = call(
         state_kernel,
         shape(prior_state.shape, f32),
-        prior_state,
-        vectors,
+        *far(prior_state),
+        *held(vectors),
         grid=(seqs // block,),
         in_specs=[
             pl.BlockSpec((block, HEAD, width), lambda i: (i, 0, 0)),
@@ -378,16 +427,21 @@
         *held(heads_all, w_out, token_rows, hit),
     )
     sent = exchange(outgoing.reshape(groups, 4, width), "ep").reshape(slots, width)
-    slot_weights = call(weights_kernel, near((slots, seqs), f32), *held(routes.T, route_weights.T))
+    slot_weights, second_scale = call(
+        weights_kernel,
+        (near((slots, seqs), f32), near((count, width), f32)),
+        *far(routes.T, route_weights.T, pieces(second_gain)),
+    )
     gathered = exchange(
-        call(spread_kernel, shape((count, rows, width), bf16), *held(sent, residual)), "tp"
+        call(spread_kernel, shape((count, rows, width), bf16), *held(sent, residual)),
+        "tp",
     )
     partial, dense_rows = call(
         expert_kernel,
         (shape((count, rows, width), bf16), near((seqs, count * width), bf16)),
         *held(
             gathered,
-            pieces(second_gain),
+            second_scale,
             exp_gate[0],
             exp_up[0],
             exp_down[0],
@@ -396,7 +450,9 @@
             dense_down,
         ),
     )
-    mix = call(mix_kernel, near((seqs, width), f32), *held(dense_rows, pieces(dense_mix)))
+    mix = call(
+        mix_kernel, near((seqs, width), f32), *held(dense_rows), *far(pieces(dense_mix))
+    )
     expert_out, dense_out = call(
         total_kernel,
         (shape((slots, width), bf16), near((seqs, width), f32)),

time: 117 us -> 102 us (0.87)
  blocking collectives: 72.9 us -> 49.1 us
  starting transfers between devices: 11.1 us -> 29.9 us
  waiting for transfers between devices: 16.2 us -> 7.59 us
  local copies, waits for them, and re-layouts: 7.42 us -> 0.05 us
  Pallas kernels: 7.35 us -> 14 us
    all_to_all x4 -> x3, blocking collectives: 72.9 us -> 49.1 us  [exchange(): lax.all_to_all(value, axis, 0, 0, tiled=True, axis_index_groups=[order])]
    all_to_all x2 -> x3, starting transfers between devices: 11.1 us -> 29.9 us  [exchange(): lax.all_to_all(value, axis, 0, 0, tiled=True, axis_index_groups=[order])]
    all_to_all x2 -> x3, waiting for transfers between devices: 16.2 us -> 7.59 us  [exchange(): lax.all_to_all(value, axis, 0, 0, tiled=True, axis_index_groups=[order])]
    unnamed x56 -> x16, local copies, waits for them, and re-layouts: 7.42 us -> 0.05 us
    pallas_call x12, Pallas kernels: 7.35 us -> 14 us  [call(): pl.pallas_call(kernel, out_shape=outs, compiler_params=params, **kwargs)]
  transfers between devices with their start and end apart: 2 -> 3, of which waited for: 2 -> 2; matrix products, arithmetic and copies ran while one was open for 0% -> 0% of each run, Pallas kernels for 2% -> 7%
where the time goes in v2:
time: 102 us; the launch traced here: 101 us
  blocking collectives  49.1 us (48%)
  starting transfers between devices  29.9 us (29%)
  Pallas kernels  14 us (14%)
  waiting for transfers between devices  7.59 us (7%)
    all_to_all x3, blocking collectives, exchange(): lax.all_to_all(value, axis, 0, 0, tiled=True, axis_index_groups=[order])  49.1 us
    all_to_all x3, starting transfers between devices, exchange(): lax.all_to_all(value, axis, 0, 0, tiled=True, axis_index_groups=[order])  29.9 us
    pallas_call x12, Pallas kernels, call(): pl.pallas_call(kernel, out_shape=outs, compiler_params=params, **kwargs)  14 us
    all_to_all x3, waiting for transfers between devices, exchange(): lax.all_to_all(value, axis, 0, 0, tiled=True, axis_index_groups=[order])  7.59 us
  transfers between devices with their start and end apart: 3, of which 2 were waited for; matrix products, arithmetic and copies ran while one was open for 0% of the time, Pallas kernels for 7%

profile of v2, /device:TPU:1, one launch (start us, length us, event | category | flops | bytes accessed | tf_op | source)
XLA Modules:
  0.0 101.4 jit_solution(2347654365367634477)
XLA Ops:
  0.6 1.7 %shard_map.257 = bf16[16,24,384]{2,1,0:T(8,128)(2,1)} custom-call(s32[1]{0:T(128)} %bitcast.place, bf16[24,128]{1,0:T(8,128)(2,1)} %tokens.3, bf16[16,128]{1,0:T(8,128)(2,1)} %bitcast.32, bf16[96,128]{1,0:T(8,128)(2,1)} %bitcast.30, bf16[96,128]{1,0:T(8,128)(2,1)} %bitcast.31), custom_call_target="tpu_custom_call" | custom-call | tf_op jit(solution)/shard_map/pallas_call | solution.py:32
  2.3 9.6 %all-to-all-start = ((bf16[16,24,384]{2,1,0:T(8,128)(2,1)}), bf16[16,24,384]{2,1,0:T(8,128)(2,1)S(1)}, u32[]{:S(2)}, u32[]{:S(2)}) async-start(bf16[16,24,384]{2,1,0:T(8,128)(2,1)} %shard_map.257), calls=%async_computation | async-start | bytes 589824 | tf_op jit(solution)/shard_map/all_to_all | solution.py:316
  11.9 2.5 %shard_map.258 = (bf16[3,2048,128]{2,1,0:T(8,128)(2,1)S(1)}, bf16[2,96,128]{2,1,0:T(8,128)(2,1)S(1)}, f32[24,64,128]{2,1,0:T(8,128)S(1)}, bf16[128,24]{1,0:T(8,1...) custom-call(bf16[2048,128]{1,0:T(8,128)(2,1)} %w_recept.1, bf16[2048,128]{1,0:T(8,128)(2,1)} %w_key.1, ...), custom_call_target="tpu_custom_call" | custom-call | tf_op jit(solution)/shard_map/pallas_call | solution.py:32
  14.3 0.0 copy-start.3
  14.3 0.0 copy-start.7
  14.3 0.6 all-to-all-done.arrived
  14.9 1.2 %shard_map.259 = (bf16[16,24,128]{2,1,0:T(8,128)(2,1)S(1)}, f32[5,24,128]{2,1,0:T(8,128)S(1)}) custom-call(bf16[16,24,384]{2,1,0:T(8,128)(2,1)S(1)} %all-to-all-done.arrived, f32[24,64,128]{2,1,0:T(8,128)S(1)} %get-tuple-element.18.state, f32[16,128]{1,0:T(8,128)S(1)} %get-tuple-element.19.gain, bf16[3,2048,128]{2,1,0:T(8,128)(2,1)S(1)} %get-tuple-element.20.weights, ...), custom_call_target="tpu_custom_call" | custom-call | tf_op jit(solution)/shard_map/pallas_call | solution.py:32
  16.1 0.0 copy-start
  16.1 0.0 copy-start.1
  16.1 0.0 copy-start.2
  16.2 0.0 copy-start.4
  16.2 0.0 copy-start.5
  16.2 0.0 copy-start.6
  16.2 9.0 %all_to_all.30.heads = bf16[16,24,128]{2,1,0:T(8,128)(2,1)S(1)} all-to-all(bf16[16,24,128]{2,1,0:T(8,128)(2,1)S(1)} %get-tuple-element.23), channel_id=1, replica_groups={{10,11,12,13,14,15,0,1,2,3,4,5,6,7,8,9},{26,27,28,29,30,31,16,17,18,19,..., dimensions={0} | all-to-all | bytes 196608 | tf_op jit(solution)/shard_map/all_to_all | solution.py:316
  25.2 0.0 copy-done.3
  25.2 0.0 copy-done.7
  25.2 0.3 shard_map.260
  25.5 25.0 %all_to_all.31 = bf16[32,4,128]{2,1,0:T(4,128)(2,1)S(1)} all-to-all(bf16[32,4,128]{2,1,0:T(4,128)(2,1)S(1)} %bitcast.29), channel_id=1, replica_groups={{272,288,304,320,336,352,368,384,400,416,432,448,464,480,496,0,16,32,48..., dimensions={0} | all-to-all | bytes 65536 | tf_op jit(solution)/shard_map/all_to_all | solution.py:316
  50.4 0.9 shard_map.261
  51.4 8.1 %all-to-all-start.3 = ((bf16[16,152,128]{2,1,0:T(8,128)(2,1)}), bf16[16,152,128]{2,1,0:T(8,128)(2,1)S(1)}, u32[]{:S(2)}, u32[]{:S(2)}) async-start(bf16[16,152,128]{2,1,0:T(8,128)(2,1)} %shard_map.261), calls=%async_computation.3 | async-start | bytes 1245184 | tf_op jit(solution)/shard_map/all_to_all | solution.py:316
  59.5 0.9 shard_map.262
  60.3 7.0 %all-to-all-done.3.arrived = bf16[16,152,128]{2,1,0:T(8,128)(2,1)S(1)} async-done(((bf16[16,152,128]{2,1,0:T(8,128)(2,1)}), bf16[16,152,128]{2,1,0:T(8,128)(2,1)S(1)}, u32[]{:S(2)}, u32[]{:S(2)}) %all-to-all-start.3) | async-done | bytes 622624 | tf_op jit(solution)/shard_map/all_to_all | solution.py:316
  67.4 0.0 copy-done
  67.4 0.0 copy-done.1
  67.4 0.0 copy-done.2
  67.4 0.0 copy-done.4
  67.4 0.0 copy-done.5
  67.4 0.0 copy-done.6
  67.4 1.1 %shard_map.263 = (bf16[16,152,128]{2,1,0:T(8,128)(2,1)S(1)}, bf16[24,2048]{1,0:T(8,128)(2,1)S(1)}) custom-call(bf16[16,152,128]{2,1,0:T(8,128)(2,1)S(1)} %all-to-all-done.3.arrived, f32[16,128]{1,0:T(8,128)S(1)} %get-tuple-element.27.gain, bf16[2048,128]{1,0:T(8,128)(2,1)S(1)} %bitcast.22, bf16[2048,128]{1,0:T(8,128)(2,1)S(1)} %bitcast.23, ...), custom_call_target="tpu_custom_call" | custom-call | tf_op jit(solution)/shard_map/pallas_call | solution.py:32
  68.5 15.2 %all_to_all.32.partial = bf16[16,152,128]{2,1,0:T(8,128)(2,1)S(1)} all-to-all(bf16[16,152,128]{2,1,0:T(8,128)(2,1)S(1)} %get-tuple-element.28), channel_id=1, replica_groups={{10,11,12,13,14,15,0,1,2,3,4,5,6,7,8,9},{26,27,28,29,30,31,16,17,18,19,..., dimensions={0} | all-to-all | bytes 1245184 | tf_op jit(solution)/shard_map/all_to_all | solution.py:316
  83.7 0.7 shard_map.264
  84.4 12.2 %all-to-all-start.5 = ((bf16[32,4,128]{2,1,0:T(4,128)(2,1)}), bf16[32,4,128]{2,1,0:T(4,128)(2,1)S(1)}, u32[]{:S(2)}, u32[]{:S(2)}) async-start(bf16[32,4,128]{2,1,0:T(4,128)(2,1)} %bitcast.19), calls=%async_computation.5 | async-start | bytes 65536 | tf_op jit(solution)/shard_map/all_to_all | solution.py:316
  96.6 3.2 %shard_map.268 = f32[24,64,128]{2,1,0:T(8,128)} custom-call(f32[24,64,128]{2,1,0:T(8,128)} %state.3, f32[5,24,128]{2,1,0:T(8,128)S(1)} %get-tuple-element.33.vectors), custom_call_target="tpu_custom_call" | custom-call | tf_op jit(solution)/shard_map/pallas_call | solution.py:32
  99.8 0.8 shard_map.265.mix
  100.6 0.0 all-to-all-done.5
  100.6 0.8 shard_map.267
  (1 shorter events, 0.0 us)
Async XLA Ops:
  2.3 12.6 %all-to-all-start = ((bf16[16,24,384]{2,1,0:T(8,128)(2,1)}), bf16[16,24,384]{2,1,0:T(8,128)(2,1)S(1)}, u32[]{:S(2)}, u32[]{:S(2)}) async-start(bf16[16,24,384]{2,1,0:T(8,128)(2,1)} %shard_map.257), calls=%async_computation | async-start | bytes 589824 | tf_op jit(solution)/shard_map/all_to_all | solution.py:316
  14.3 10.8 %copy-start.3 = (bf16[2048,128]{1,0:T(8,128)(2,1)S(1)}, bf16[2048,128]{1,0:T(8,128)(2,1)}, u32[]{:S(2)}) copy-start(bf16[2048,128]{1,0:T(8,128)(2,1)} %w_out.1) | copy-start | bytes 1572868
  14.3 10.8 %copy-start.7 = (bf16[24,128]{1,0:T(8,128)(2,1)S(1)}, bf16[24,128]{1,0:T(8,128)(2,1)}, u32[]{:S(2)}) copy-start(bf16[24,128]{1,0:T(8,128)(2,1)} %tokens.3) | copy-start | bytes 18436
  16.1 51.3 %copy-start = (bf16[1,2048,128]{2,1,0:T(8,128)(2,1)S(1)}, bf16[1,2048,128]{2,1,0:T(8,128)(2,1)}, u32[]{:S(2)}) copy-start(bf16[1,2048,128]{2,1,0:T(8,128)(2,1)} %param.45) | copy-start | bytes 1572868
  16.1 51.2 %copy-start.1 = (bf16[1,2048,128]{2,1,0:T(8,128)(2,1)S(1)}, bf16[1,2048,128]{2,1,0:T(8,128)(2,1)}, u32[]{:S(2)}) copy-start(bf16[1,2048,128]{2,1,0:T(8,128)(2,1)} %param.46) | copy-start | bytes 1572868
  16.1 51.2 %copy-start.2 = (bf16[1,128,2048]{2,1,0:T(8,128)(2,1)S(1)}, bf16[1,128,2048]{2,1,0:T(8,128)(2,1)}, u32[]{:S(2)}) copy-start(bf16[1,128,2048]{2,1,0:T(8,128)(2,1)} %param.47) | copy-start | bytes 1572868
  16.2 51.2 %copy-start.4 = (bf16[2048,32]{0,1:T(8,128)(2,1)S(1)}, bf16[2048,32]{0,1:T(8,128)(2,1)}, u32[]{:S(2)}) copy-start(bf16[2048,32]{0,1:T(8,128)(2,1)} %param.48) | copy-start | bytes 393220
  16.2 51.2 %copy-start.5 = (bf16[2048,32]{0,1:T(8,128)(2,1)S(1)}, bf16[2048,32]{0,1:T(8,128)(2,1)}, u32[]{:S(2)}) copy-start(bf16[2048,32]{0,1:T(8,128)(2,1)} %param.49) | copy-start | bytes 393220
  16.2 51.2 %copy-start.6 = (bf16[32,2048]{1,0:T(8,128)(2,1)S(1)}, bf16[32,2048]{1,0:T(8,128)(2,1)}, u32[]{:S(2)}) copy-start(bf16[32,2048]{1,0:T(8,128)(2,1)} %dense_down.1) | copy-start | bytes 393220
  51.4 16.0 %all-to-all-start.3 = ((bf16[16,152,128]{2,1,0:T(8,128)(2,1)}), bf16[16,152,128]{2,1,0:T(8,128)(2,1)S(1)}, u32[]{:S(2)}, u32[]{:S(2)}) async-start(bf16[16,152,128]{2,1,0:T(8,128)(2,1)} %shard_map.261), calls=%async_computation.3 | async-start | bytes 1245184 | tf_op jit(solution)/shard_map/all_to_all | solution.py:316
  84.4 16.2 %all-to-all-start.5 = ((bf16[32,4,128]{2,1,0:T(4,128)(2,1)}), bf16[32,4,128]{2,1,0:T(4,128)(2,1)S(1)}, u32[]{:S(2)}, u32[]{:S(2)}) async-start(bf16[32,4,128]{2,1,0:T(4,128)(2,1)} %bitcast.19), calls=%async_computation.5 | async-start | bytes 65536 | tf_op jit(solution)/shard_map/all_to_all | solution.py:316

commit v3 on v2

--- a/solution.py
+++ b/solution.py
@@ -82,19 +82,25 @@
         out[p] = whole
 
 
-def slot_table(routes, slots):
+def slot_table(routes, slots, stride):
     top, seqs = routes.shape
-    expert = (lax.broadcasted_iota(jnp.int32, (slots, seqs), 0) // 4 + FIRST["ep"]) % (slots // 4)
-    matches = [routes[k : k + 1, :] == expert for k in range(top)]
-    chosen = jnp.where(matches[0], 1.0, 0.0)
+    index = lax.broadcasted_iota(jnp.int32, (slots, seqs), 0)
+    expert = (index // stride + FIRST["ep"]) % (slots // stride)
+    matches = [jnp.where(routes[k : k + 1, :] == expert, 1.0, 0.0) for k in range(top)]
+    chosen = matches[0]
     for match in matches[1:]:
-        chosen = chosen + jnp.where(match, 1.0, 0.0)
+        chosen = chosen + match
     earlier = lax.broadcasted_iota(jnp.int32, (seqs, seqs), 0) < lax.broadcasted_iota(
         jnp.int32, (seqs, seqs), 1
     )
     before = dot(chosen.astype(bf16), jnp.where(earlier, 1.0, 0.0).astype(bf16))
-    place = (lax.broadcasted_iota(jnp.int32, (slots, seqs), 0) % 4).astype(f32)
-    return matches, jnp.where(before == place, chosen, 0.0)
+    return matches, chosen, before - (index % stride).astype(f32)
+
+
+def in_three(x):
+    high = x.astype(bf16).astype(f32)
+    middle = (x - high).astype(bf16).astype(f32)
+    return high, middle, x - high - middle
 
 
 def prep_kernel(
@@ -105,6 +111,7 @@
     iclr_up,
     state,
     routes,
+    route_weights,
     gain,
     decay_base,
     iclr_base,
@@ -115,6 +122,7 @@
     ups_out,
     state_out,
     hit_out,
+    notes_out,
     gain_out,
     rows_out,
     sems,
@@ -124,8 +132,19 @@
     copies = [pltpu.make_async_copy(a, b, sems.at[i]) for i, (a, b) in enumerate(moves)]
     for copy in copies:
         copy.start()
-    _, hit = slot_table(routes, hit_out.shape[0])
-    hit_out[...] = hit.astype(bf16)
+    matches, chosen, offset = slot_table(routes, hit_out.shape[0], 8)
+    hit_out[...] = jnp.where(offset == 0.0, chosen, 0.0).astype(bf16)
+    noted = offset == -4.0
+    weighted = matches[0] * route_weights[0:1, :]
+    for k in range(1, len(matches)):
+        weighted = weighted + matches[k] * route_weights[k : k + 1, :]
+    weight = jnp.sum(jnp.where(noted, weighted, 0.0), axis=1, keepdims=True)
+    main = jnp.sum(jnp.where(noted, matches[0], 0.0), axis=1, keepdims=True)
+    lanes = lax.broadcasted_iota(jnp.int32, notes_out.shape, 1)
+    notes = jnp.zeros(notes_out.shape, f32)
+    for i, column in enumerate((*in_three(weight), main)):
+        notes = jnp.where(lanes == i, column, notes)
+    notes_out[...] = notes.astype(bf16)
     gain_out[...] = gain[...].astype(f32)
     for i, row in enumerate((decay_base, iclr_base, key_scale, key_mix, head_gain)):
         rows_out[i : i + 1, :] = row[...].astype(f32)
@@ -133,13 +152,14 @@
         copy.wait()
 
 
-def weights_kernel(routes, weights, gain, out, gain_out):
+def gains_kernel(gain, mix, gain_out, mix_out):
     gain_out[...] = gain[...].astype(f32)
-    matches, hit = slot_table(routes, out.shape[0])
-    total = jnp.zeros(out.shape, f32)
-    for k, match in enumerate(matches):
-        total = total + jnp.where(match, weights[k : k + 1, :], 0.0)
-    out[...] = total * hit
+    mix_out[...] = mix[...].astype(f32)
+
+
+def table_kernel(routes, out):
+    _, chosen, offset = slot_table(routes, out.shape[0], 4)
+    out[...] = jnp.where(offset == 0.0, chosen, 0.0).astype(bf16)
 
 
 def mixer_in_kernel(
@@ -220,27 +240,29 @@
     )
 
 
-def dispatch_kernel(heads, w_out, tokens, hit, residual_out, outgoing):
+def dispatch_kernel(heads, w_out, tokens, hit, notes, residual_out, outgoing):
     count = heads.shape[0]
     rows = jnp.concatenate([x[...] for x in by_feature(heads, count)], axis=1)
     mixed = dot(rows, w_out[...]).astype(bf16).astype(f32)
     residual = (tokens[...].astype(f32) + mixed).astype(bf16)
     residual_out[...] = residual
-    outgoing[...] = dot(hit[...], residual).astype(bf16)
-
-
-def spread_kernel(arrived, residual, out):
-    slots = arrived.shape[0]
-    for p in range(out.shape[0]):
-        out[p, :slots] = arrived[...]
-        out[p, slots:] = residual[...]
+    outgoing[...] = (dot(hit[...], residual) + notes[...].astype(f32)).astype(bf16)
+
+
+def spread_kernel(arrived, out, notes_out):
+    count, slots, _ = out.shape
+    slot = lax.broadcasted_iota(jnp.int32, (slots, 2 * slots), 0)
+    place = lax.broadcasted_iota(jnp.int32, (slots, 2 * slots), 1) - (slot // 4 * 8 + slot % 4)
+    rows = dot(jnp.where(place == 0, 1.0, 0.0).astype(bf16), arrived[...]).astype(bf16)
+    for p in range(count):
+        out[p] = rows
+    notes_out[...] = dot(jnp.where(place == 4, 1.0, 0.0).astype(bf16), arrived[...])
 
 
 def expert_kernel(
-    arrived, gain, gate, up, down, dense_gate, dense_up, dense_down, out, dense_rows_out
+    arrived, notes, gain, mix, gate, up, down, dense_gate, dense_up, dense_down, out
 ):
-    count, rows, piece = arrived.shape
-    slots = rows - dense_rows_out.shape[0]
+    count, _, piece = arrived.shape
     pieces = [x[...].astype(f32) for x in by_feature(arrived, count)]
     squares = pieces[0] * pieces[0]
     for x in pieces[1:]:
@@ -251,56 +273,41 @@
     normed = [
         (x * scale * gain[p : p + 1, :]).astype(bf16) for p, x in enumerate(pieces)
     ]
+    mixed = normed[0].astype(f32) * mix[0:1, :]
+    for p in range(1, count):
+        mixed = mixed + normed[p].astype(f32) * mix[p : p + 1, :]
+    mix_gate = jax.nn.sigmoid(jnp.sum(mixed, axis=1, keepdims=True))
+    weight = notes[:, 0:1] + notes[:, 1:2] + notes[:, 2:3]
+    dense_weight = mix_gate * notes[:, 3:4]
     second = jnp.concatenate(normed, axis=1)
-    routed, dense = second[:slots], second[slots:]
-    hidden = (jax.nn.silu(dot(routed, gate[...])) * dot(routed, up[...])).astype(bf16)
+    hidden = (jax.nn.silu(dot(second, gate[...])) * dot(second, up[...])).astype(bf16)
     dense_hidden = (
-        jax.nn.silu(dot_t(dense, dense_gate[...])) * dot_t(dense, dense_up[...])
+        jax.nn.silu(dot_t(second, dense_gate[...])) * dot_t(second, dense_up[...])
     ).astype(bf16)
     for p, t in enumerate(member_order(count, "tp")):
         cols = slice(t * piece, (t + 1) * piece)
-        out[p, :slots] = dot(hidden, down[:, cols]).astype(bf16)
-        out[p, slots:] = dot(dense_hidden, dense_down[:, cols]).astype(bf16)
-    dense_rows_out[...] = dense
-
-
-def mix_kernel(rows, weights, out):
-    count, width = weights.shape
-    mix = jnp.zeros(out.shape, f32)
-    for p in range(count):
-        mix = mix + rows[:, p * width : (p + 1) * width].astype(f32) * weights[
-            p : p + 1, :
-        ].astype(f32)
-    mix = jax.nn.sigmoid(jnp.sum(mix, axis=1, keepdims=True))
-    out[...] = jnp.broadcast_to(mix, out.shape)
-
-
-def total_kernel(partial, expert_out, dense_out):
-    count = partial.shape[0]
-    slots = expert_out.shape[0]
+        out[p] = (
+            weight * dot(hidden, down[:, cols])
+            + dense_weight * dot(dense_hidden, dense_down[:, cols])
+        ).astype(bf16)
+
+
+def total_kernel(partial, out):
     total = partial[0].astype(f32)
-    for p in range(1, count):
+    for p in range(1, partial.shape[0]):
         total = total + partial[p].astype(f32)
-    expert_out[...] = total[:slots].astype(bf16)
-    dense_out[...] = total[slots:]
-
-
-def base_kernel(residual, mix, dense, out):
-    out[...] = residual[...].astype(f32) + mix[...] * dense[...]
-
-
-def final_kernel(returned, weights, base, out):
-    high = weights[...].astype(bf16)
-    rest = weights[...] - high.astype(f32)
-    middle = rest.astype(bf16)
-    low = (rest - middle.astype(f32)).astype(bf16)
-    values = returned[...]
-    total = base[...]
-    for part in (low, middle, high):
-        total = total + lax.dot_general(
-            part, values, (((0,), (0,)), ((), ())), preferred_element_type=f32
-        )
     out[...] = total.astype(bf16)
+
+
+def base_kernel(residual, out):
+    out[...] = residual[...].astype(f32)
+
+
+def final_kernel(returned, table, base, out):
+    routed = lax.dot_general(
+        table[...], returned[...], (((0,), (0,)), ((), ())), preferred_element_type=f32
+    )
+    out[...] = (base[...] + routed).astype(bf16)
 
 
 def member_order(count, axis):
@@ -360,7 +367,6 @@
     count = lax.axis_size("tp")
     groups = lax.axis_size("ep")
     slots = groups * 4
-    rows = slots + seqs
     place = lax.axis_index("tp").reshape(1).astype(jnp.int32)
     row = lambda v: v.reshape(1, width)
     pieces = lambda v: v.reshape(count, width)
@@ -374,13 +380,14 @@
         in_specs=[in_smem] + [in_vmem] * 4,
     )
     arrived = exchange(message, "tp")
-    weights, ups, state, hit, gain, rows_of = call(
+    weights, ups, state, hit, notes, gain, rows_of = call(
         prep_kernel,
         (
             near((3, *w_key.shape), bf16),
             near((2, *decay_up.shape), bf16),
             near(prior_state.shape, f32),
-            near((slots, seqs), bf16),
+            near((2 * slots, seqs), bf16),
+            near((2 * slots, width), bf16),
             near((count, width), f32),
             near((8, width), f32),
         ),
@@ -392,6 +399,7 @@
             iclr_up,
             prior_state,
             routes.T,
+            route_weights.T,
             pieces(first_gain),
             row(decay_base),
             row(iclr_base),
@@ -399,7 +407,7 @@
             row(key_mix),
             row(head_gain),
         ),
-        in_specs=[pl.BlockSpec(memory_space=pl.ANY)] * 6 + [in_vmem] * 7,
+        in_specs=[pl.BlockSpec(memory_space=pl.ANY)] * 6 + [in_vmem] * 8,
         scratch_shapes=[pltpu.SemaphoreType.DMA((6,))],
     )
     heads, vectors = call(
@@ -423,25 +431,30 @@
     )
     residual, outgoing = call(
         dispatch_kernel,
-        (near((seqs, width), bf16), shape((slots, width), bf16)),
-        *held(heads_all, w_out, token_rows, hit),
-    )
-    sent = exchange(outgoing.reshape(groups, 4, width), "ep").reshape(slots, width)
-    slot_weights, second_scale = call(
-        weights_kernel,
-        (near((slots, seqs), f32), near((count, width), f32)),
-        *far(routes.T, route_weights.T, pieces(second_gain)),
-    )
-    gathered = exchange(
-        call(spread_kernel, shape((count, rows, width), bf16), *held(sent, residual)),
-        "tp",
-    )
-    partial, dense_rows = call(
+        (near((seqs, width), bf16), shape((2 * slots, width), bf16)),
+        *held(heads_all, w_out, token_rows, hit, notes),
+    )
+    sent = exchange(outgoing.reshape(groups, 8, width), "ep")
+    second_scale, mix_scale = call(
+        gains_kernel,
+        (near((count, width), f32), near((count, width), f32)),
+        *far(pieces(second_gain), pieces(dense_mix)),
+    )
+    rows, slot_notes = call(
+        spread_kernel,
+        (shape((count, slots, width), bf16), near((slots, width), f32)),
+        *held(sent.reshape(2 * slots, width)),
+    )
+    gathered = exchange(rows, "tp")
+    table = call(table_kernel, near((slots, seqs), bf16), *far(routes.T))
+    partial = call(
         expert_kernel,
-        (shape((count, rows, width), bf16), near((seqs, count * width), bf16)),
+        shape((count, slots, width), bf16),
         *held(
             gathered,
+            slot_notes,
             second_scale,
+            mix_scale,
             exp_gate[0],
             exp_up[0],
             exp_down[0],
@@ -450,20 +463,15 @@
             dense_down,
         ),
     )
-    mix = call(
-        mix_kernel, near((seqs, width), f32), *held(dense_rows), *far(pieces(dense_mix))
-    )
-    expert_out, dense_out = call(
-        total_kernel,
-        (shape((slots, width), bf16), near((seqs, width), f32)),
-        *held(exchange(partial, "tp")),
-    )
-    base = call(base_kernel, near((seqs, width), f32), *held(residual, mix, dense_out))
+    expert_out = call(
+        total_kernel, shape((slots, width), bf16), *held(exchange(partial, "tp"))
+    )
     returned = exchange(expert_out.reshape(groups, 4, width), "ep")
+    base = call(base_kernel, near((seqs, width), f32), *held(residual))
     layer_out = call(
         final_kernel,
         shape((seqs, width), bf16),
-        *held(returned.reshape(slots, width), slot_weights, base),
+        *held(returned.reshape(slots, width), table, base),
     )
     return (layer_out, next_state)
 

time: 102 us -> 102 us (level)
  no operation moved by 1% of the time
where the time goes in v3:
time: 102 us; the launch traced here: 101 us
  blocking collectives  49.1 us (48%)
  starting transfers between devices  30.1 us (30%)
  Pallas kernels  14.4 us (14%)
  waiting for transfers between devices  6.72 us (7%)
    all_to_all x3, blocking collectives, exchange(): lax.all_to_all(value, axis, 0, 0, tiled=True, axis_index_groups=[order])  49.1 us
    all_to_all x3, starting transfers between devices, exchange(): lax.all_to_all(value, axis, 0, 0, tiled=True, axis_index_groups=[order])  30.1 us
    pallas_call x12, Pallas kernels, call(): pl.pallas_call(kernel, out_shape=outs, compiler_params=params, **kwargs)  14.4 us
    all_to_all x3, waiting for transfers between devices, exchange(): lax.all_to_all(value, axis, 0, 0, tiled=True, axis_index_groups=[order])  6.72 us
  transfers between devices with their start and end apart: 3, of which 2 were waited for; matrix products, arithmetic and copies ran while one was open for 0% of the time, Pallas kernels for 7%

profile of v3, /device:TPU:1, one launch (start us, length us, event | category | flops | bytes accessed | tf_op | source)
XLA Modules:
  0.0 101.1 jit_solution(12772919041087806424)
XLA Ops:
  0.6 1.7 %shard_map.257 = bf16[16,24,384]{2,1,0:T(8,128)(2,1)} custom-call(s32[1]{0:T(128)} %bitcast.place, bf16[24,128]{1,0:T(8,128)(2,1)} %tokens.3, bf16[16,128]{1,0:T(8,128)(2,1)} %bitcast.32, bf16[96,128]{1,0:T(8,128)(2,1)} %bitcast.30, bf16[96,128]{1,0:T(8,128)(2,1)} %bitcast.31), custom_call_target="tpu_custom_call" | custom-call | tf_op jit(solution)/shard_map/pallas_call | solution.py:32
  2.3 9.6 %all-to-all-start = ((bf16[16,24,384]{2,1,0:T(8,128)(2,1)}), bf16[16,24,384]{2,1,0:T(8,128)(2,1)S(1)}, u32[]{:S(2)}, u32[]{:S(2)}) async-start(bf16[16,24,384]{2,1,0:T(8,128)(2,1)} %shard_map.257), calls=%async_computation | async-start | bytes 589824 | tf_op jit(solution)/shard_map/all_to_all | solution.py:323
  11.9 2.5 %shard_map.258 = (bf16[3,2048,128]{2,1,0:T(8,128)(2,1)S(1)}, bf16[2,96,128]{2,1,0:T(8,128)(2,1)S(1)}, f32[24,64,128]{2,1,0:T(8,128)S(1)}, bf16[256,24]{1,0:T(8,1...) custom-call(bf16[2048,128]{1,0:T(8,128)(2,1)} %w_recept.1, ...), custom_call_target="tpu_custom_call" | custom-call | tf_op jit(solution)/shard_map/pallas_call | solution.py:32
  14.4 0.0 copy-start
  14.4 0.0 copy-start.7
  14.4 0.5 all-to-all-done.arrived
  14.9 1.2 %shard_map.259 = (bf16[16,24,128]{2,1,0:T(8,128)(2,1)S(1)}, f32[5,24,128]{2,1,0:T(8,128)S(1)}) custom-call(bf16[16,24,384]{2,1,0:T(8,128)(2,1)S(1)} %all-to-all-done.arrived, f32[24,64,128]{2,1,0:T(8,128)S(1)} %get-tuple-element.17.state, f32[16,128]{1,0:T(8,128)S(1)} %get-tuple-element.18.gain, bf16[3,2048,128]{2,1,0:T(8,128)(2,1)S(1)} %get-tuple-element.19.weights, ...), custom_call_target="tpu_custom_call" | custom-call | tf_op jit(solution)/shard_map/pallas_call | solution.py:32
  16.1 0.0 copy-start.1
  16.1 0.0 copy-start.2
  16.1 0.0 copy-start.3
  16.2 0.0 copy-start.4
  16.2 0.0 copy-start.5
  16.2 0.0 copy-start.6
  16.2 9.0 %all_to_all.30.heads = bf16[16,24,128]{2,1,0:T(8,128)(2,1)S(1)} all-to-all(bf16[16,24,128]{2,1,0:T(8,128)(2,1)S(1)} %get-tuple-element.22), channel_id=1, replica_groups={{10,11,12,13,14,15,0,1,2,3,4,5,6,7,8,9},{26,27,28,29,30,31,16,17,18,19,..., dimensions={0} | all-to-all | bytes 196608 | tf_op jit(solution)/shard_map/all_to_all | solution.py:323
  25.2 0.0 copy-done
  25.2 0.0 copy-done.7
  25.2 0.4 shard_map.260
  25.5 26.4 %all_to_all.31 = bf16[32,8,128]{2,1,0:T(8,128)(2,1)S(1)} all-to-all(bf16[32,8,128]{2,1,0:T(8,128)(2,1)S(1)} %bitcast.29), channel_id=1, replica_groups={{272,288,304,320,336,352,368,384,400,416,432,448,464,480,496,0,16,32,48..., dimensions={0} | all-to-all | bytes 131072 | tf_op jit(solution)/shard_map/all_to_all | solution.py:323
  51.9 1.0 shard_map.261
  52.9 8.1 %all-to-all-start.3 = ((bf16[16,128,128]{2,1,0:T(8,128)(2,1)}), bf16[16,128,128]{2,1,0:T(8,128)(2,1)S(1)}, u32[]{:S(2)}, u32[]{:S(2)}) async-start(bf16[16,128,128]{2,1,0:T(8,128)(2,1)} %get-tuple-element.26), calls=%async_computation.3 | async-start | bytes 1048576 | tf_op jit(solution)/shard_map/all_to_all | solution.py:323
  61.0 0.7 shard_map.262
  61.7 6.2 %all-to-all-done.3.arrived = bf16[16,128,128]{2,1,0:T(8,128)(2,1)S(1)} async-done(((bf16[16,128,128]{2,1,0:T(8,128)(2,1)}), bf16[16,128,128]{2,1,0:T(8,128)(2,1)S(1)}, u32[]{:S(2)}, u32[]{:S(2)}) %all-to-all-start.3) | async-done | bytes 524320 | tf_op jit(solution)/shard_map/all_to_all | solution.py:323
  67.9 0.0 copy-done.1
  67.9 0.0 copy-done.2
  67.9 0.0 copy-done.3
  67.9 0.0 copy-done.4
  67.9 0.0 copy-done.5
  67.9 0.0 copy-done.6
  67.9 1.4 %shard_map.263 = bf16[16,128,128]{2,1,0:T(8,128)(2,1)S(1)} custom-call(bf16[16,128,128]{2,1,0:T(8,128)(2,1)S(1)} %all-to-all-done.3.arrived, f32[128,128]{1,0:T(8,128)S(1)} %get-tuple-element.27.notes, f32[16,128]{1,0:T(8,128)S(1)} %get-tuple-element.28.gain, f32[16,128]{1,0:T(8,128)S(1)} %get-tuple-element.29.mix, bf16[2048,128]{1,0:T(8,128)(2,1)S(1)} %bitcast.22, ...), custom_call_target="tpu_custom_call" | custom-call | tf_op jit(solution)/shard_map/pallas_call | solution.py:32
  69.3 13.8 %all_to_all.32.partial = bf16[16,128,128]{2,1,0:T(8,128)(2,1)S(1)} all-to-all(bf16[16,128,128]{2,1,0:T(8,128)(2,1)S(1)} %shard_map.263), channel_id=1, replica_groups={{10,11,12,13,14,15,0,1,2,3,4,5,6,7,8,9},{26,27,28,29,30,31,16,17,18,19,..., dimensions={0} | all-to-all | bytes 1048576 | tf_op jit(solution)/shard_map/all_to_all | solution.py:323
  83.1 0.7 shard_map.264
  83.8 12.5 %all-to-all-start.5 = ((bf16[32,4,128]{2,1,0:T(4,128)(2,1)}), bf16[32,4,128]{2,1,0:T(4,128)(2,1)S(1)}, u32[]{:S(2)}, u32[]{:S(2)}) async-start(bf16[32,4,128]{2,1,0:T(4,128)(2,1)} %bitcast.20), calls=%async_computation.5 | async-start | bytes 65536 | tf_op jit(solution)/shard_map/all_to_all | solution.py:323
  96.3 0.9 shard_map.265.table
  97.1 3.2 %shard_map.268 = f32[24,64,128]{2,1,0:T(8,128)} custom-call(f32[24,64,128]{2,1,0:T(8,128)} %state.3, f32[5,24,128]{2,1,0:T(8,128)S(1)} %get-tuple-element.31.vectors), custom_call_target="tpu_custom_call" | custom-call | tf_op jit(solution)/shard_map/pallas_call | solution.py:32
  100.4 0.0 all-to-all-done.5
  100.4 0.8 shard_map.267
  (1 shorter events, 0.0 us)
Async XLA Ops:
  2.3 12.6 %all-to-all-start = ((bf16[16,24,384]{2,1,0:T(8,128)(2,1)}), bf16[16,24,384]{2,1,0:T(8,128)(2,1)S(1)}, u32[]{:S(2)}, u32[]{:S(2)}) async-start(bf16[16,24,384]{2,1,0:T(8,128)(2,1)} %shard_map.257), calls=%async_computation | async-start | bytes 589824 | tf_op jit(solution)/shard_map/all_to_all | solution.py:323
  14.4 10.8 %copy-start = (bf16[2048,128]{1,0:T(8,128)(2,1)S(1)}, bf16[2048,128]{1,0:T(8,128)(2,1)}, u32[]{:S(2)}) copy-start(bf16[2048,128]{1,0:T(8,128)(2,1)} %w_out.1) | copy-start | bytes 1572868
  14.4 10.8 %copy-start.7 = (bf16[24,128]{1,0:T(8,128)(2,1)S(1)}, bf16[24,128]{1,0:T(8,128)(2,1)}, u32[]{:S(2)}) copy-start(bf16[24,128]{1,0:T(8,128)(2,1)} %tokens.3) | copy-start | bytes 18436
  16.1 51.8 %copy-start.1 = (bf16[1,2048,128]{2,1,0:T(8,128)(2,1)S(1)}, bf16[1,2048,128]{2,1,0:T(8,128)(2,1)}, u32[]{:S(2)}) copy-start(bf16[1,2048,128]{2,1,0:T(8,128)(2,1)} %param.45) | copy-start | bytes 1572868
  16.1 51.8 %copy-start.2 = (bf16[1,2048,128]{2,1,0:T(8,128)(2,1)S(1)}, bf16[1,2048,128]{2,1,0:T(8,128)(2,1)}, u32[]{:S(2)}) copy-start(bf16[1,2048,128]{2,1,0:T(8,128)(2,1)} %param.46) | copy-start | bytes 1572868
  16.1 51.8 %copy-start.3 = (bf16[1,128,2048]{2,1,0:T(8,128)(2,1)S(1)}, bf16[1,128,2048]{2,1,0:T(8,128)(2,1)}, u32[]{:S(2)}) copy-start(bf16[1,128,2048]{2,1,0:T(8,128)(2,1)} %param.47) | copy-start | bytes 1572868
  16.2 51.8 %copy-start.4 = (bf16[2048,32]{0,1:T(8,128)(2,1)S(1)}, bf16[2048,32]{0,1:T(8,128)(2,1)}, u32[]{:S(2)}) copy-start(bf16[2048,32]{0,1:T(8,128)(2,1)} %param.48) | copy-start | bytes 393220
  16.2 51.8 %copy-start.5 = (bf16[2048,32]{0,1:T(8,128)(2,1)S(1)}, bf16[2048,32]{0,1:T(8,128)(2,1)}, u32[]{:S(2)}) copy-start(bf16[2048,32]{0,1:T(8,128)(2,1)} %param.49) | copy-start | bytes 393220
  16.2 51.8 %copy-start.6 = (bf16[32,2048]{1,0:T(8,128)(2,1)S(1)}, bf16[32,2048]{1,0:T(8,128)(2,1)}, u32[]{:S(2)}) copy-start(bf16[32,2048]{1,0:T(8,128)(2,1)} %dense_down.1) | copy-start | bytes 393220
  52.9 15.0 %all-to-all-start.3 = ((bf16[16,128,128]{2,1,0:T(8,128)(2,1)}), bf16[16,128,128]{2,1,0:T(8,128)(2,1)S(1)}, u32[]{:S(2)}, u32[]{:S(2)}) async-start(bf16[16,128,128]{2,1,0:T(8,128)(2,1)} %get-tuple-element.26), calls=%async_computation.3 | async-start | bytes 1048576 | tf_op jit(solution)/shard_map/all_to_all | solution.py:323
  83.8 16.6 %all-to-all-start.5 = ((bf16[32,4,128]{2,1,0:T(4,128)(2,1)}), bf16[32,4,128]{2,1,0:T(4,128)(2,1)S(1)}, u32[]{:S(2)}, u32[]{:S(2)}) async-start(bf16[32,4,128]{2,1,0:T(4,128)(2,1)} %bitcast.20), calls=%async_computation.5 | async-start | bytes 65536 | tf_op jit(solution)/shard_map/all_to_all | solution.py:323

commit v4 on v3

--- a/solution.py
+++ b/solution.py
@@ -10,7 +10,9 @@
 f32 = jnp.float32
 bf16 = jnp.bfloat16
 
-FIRST = {"tp": 10, "ep": 17}
+FIRST = {"tokens": 10, "heads": 10, "spread_out": 10, "sums": 10, "send": 21, "back": 21}
+
+PIECE = 6
 
 norm_eps = 1e-06
 head_eps = 0.00064
@@ -82,10 +84,10 @@
         out[p] = whole
 
 
-def slot_table(routes, slots, stride):
+def slot_table(routes, slots, stride, first):
     top, seqs = routes.shape
     index = lax.broadcasted_iota(jnp.int32, (slots, seqs), 0)
-    expert = (index // stride + FIRST["ep"]) % (slots // stride)
+    expert = (index // stride + first) % (slots // stride)
     matches = [jnp.where(routes[k : k + 1, :] == expert, 1.0, 0.0) for k in range(top)]
     chosen = matches[0]
     for match in matches[1:]:
@@ -132,19 +134,21 @@
     copies = [pltpu.make_async_copy(a, b, sems.at[i]) for i, (a, b) in enumerate(moves)]
     for copy in copies:
         copy.start()
-    matches, chosen, offset = slot_table(routes, hit_out.shape[0], 8)
+    matches, chosen, offset = slot_table(routes, hit_out.shape[0], PIECE, FIRST["send"])
     hit_out[...] = jnp.where(offset == 0.0, chosen, 0.0).astype(bf16)
-    noted = offset == -4.0
     weighted = matches[0] * route_weights[0:1, :]
     for k in range(1, len(matches)):
         weighted = weighted + matches[k] * route_weights[k : k + 1, :]
-    weight = jnp.sum(jnp.where(noted, weighted, 0.0), axis=1, keepdims=True)
-    main = jnp.sum(jnp.where(noted, matches[0], 0.0), axis=1, keepdims=True)
     lanes = lax.broadcasted_iota(jnp.int32, notes_out.shape, 1)
     notes = jnp.zeros(notes_out.shape, f32)
-    for i, column in enumerate((*in_three(weight), main)):
-        notes = jnp.where(lanes == i, column, notes)
-    notes_out[...] = notes.astype(bf16)
+    for c in range(4):
+        noted = offset == c - 4.0
+        weight = jnp.sum(jnp.where(noted, weighted, 0.0), axis=1, keepdims=True)
+        main = jnp.sum(jnp.where(noted, matches[0], 0.0), axis=1, keepdims=True)
+        for i, column in enumerate((*in_three(weight), main)):
+            notes = jnp.where(lanes == 4 * c + i, column, notes)
+    rows = lax.broadcasted_iota(jnp.int32, notes_out.shape, 0)
+    notes_out[...] = jnp.where(rows % PIECE == 4, notes, 0.0).astype(bf16)
     gain_out[...] = gain[...].astype(f32)
     for i, row in enumerate((decay_base, iclr_base, key_scale, key_mix, head_gain)):
         rows_out[i : i + 1, :] = row[...].astype(f32)
@@ -158,7 +162,7 @@
 
 
 def table_kernel(routes, out):
-    _, chosen, offset = slot_table(routes, out.shape[0], 4)
+    _, chosen, offset = slot_table(routes, out.shape[0], 4, FIRST["back"])
     out[...] = jnp.where(offset == 0.0, chosen, 0.0).astype(bf16)
 
 
@@ -169,7 +173,7 @@
     piece = width // 3
     rank = ups.shape[1]
     decay_base, iclr_base, key_scale, key_mix, head_gain = (rows[i : i + 1, :] for i in range(5))
-    tokens = [x[:, :piece].astype(f32) for x in by_feature(arrived, count)]
+    tokens = [x[:, :piece].astype(f32) for x in by_feature(arrived, count, "tokens")]
     squares = tokens[0] * tokens[0]
     for x in tokens[1:]:
         squares = squares + x * x
@@ -189,9 +193,9 @@
     low = low * scale
     decay_act = jnp.tanh(low[:, :rank]).astype(bf16)
     rate_act = low[:, piece : piece + rank].astype(bf16)
-    recept = dot(first, weights[0]).astype(bf16).astype(f32)
-    key = dot(first, weights[1]).astype(bf16).astype(f32)
-    value = dot(first, weights[2]).astype(bf16).astype(f32)
+    projected = dot(first, jnp.concatenate([weights[i] for i in range(3)], axis=1))
+    projected = projected.astype(bf16).astype(f32)
+    recept, key, value = (projected[:, i * piece : (i + 1) * piece] for i in range(3))
     decay_pre = -(decay_base + dot(decay_act, ups[0]))
     softplus = jnp.maximum(decay_pre, 0.0) + jnp.log1p(jnp.exp(-jnp.abs(decay_pre)))
     decay = jnp.exp(-jnp.exp(-softplus - 0.5))
@@ -242,7 +246,7 @@
 
 def dispatch_kernel(heads, w_out, tokens, hit, notes, residual_out, outgoing):
     count = heads.shape[0]
-    rows = jnp.concatenate([x[...] for x in by_feature(heads, count)], axis=1)
+    rows = jnp.concatenate([x[...] for x in by_feature(heads, count, "heads")], axis=1)
     mixed = dot(rows, w_out[...]).astype(bf16).astype(f32)
     residual = (tokens[...].astype(f32) + mixed).astype(bf16)
     residual_out[...] = residual
@@ -250,20 +254,24 @@
 
 
 def spread_kernel(arrived, out, notes_out):
-    count, slots, _ = out.shape
-    slot = lax.broadcasted_iota(jnp.int32, (slots, 2 * slots), 0)
-    place = lax.broadcasted_iota(jnp.int32, (slots, 2 * slots), 1) - (slot // 4 * 8 + slot % 4)
-    rows = dot(jnp.where(place == 0, 1.0, 0.0).astype(bf16), arrived[...]).astype(bf16)
+    count, slots, width = out.shape
+    size = arrived.shape[0]
+    slot = lax.broadcasted_iota(jnp.int32, (slots, size), 0)
+    place = lax.broadcasted_iota(jnp.int32, (slots, size), 1) - slot // 4 * PIECE
+    rows = dot(jnp.where(place == slot % 4, 1.0, 0.0).astype(bf16), arrived[...]).astype(bf16)
     for p in range(count):
         out[p] = rows
-    notes_out[...] = dot(jnp.where(place == 4, 1.0, 0.0).astype(bf16), arrived[...])
+    notes = dot(jnp.where(place == 4, 1.0, 0.0).astype(bf16), arrived[...])
+    lane = lax.broadcasted_iota(jnp.int32, (slots, width), 1)
+    own = lax.broadcasted_iota(jnp.int32, (slots, width), 0) % 4
+    notes_out[...] = jnp.where(lane // 4 == own, notes, 0.0)
 
 
 def expert_kernel(
     arrived, notes, gain, mix, gate, up, down, dense_gate, dense_up, dense_down, out
 ):
     count, _, piece = arrived.shape
-    pieces = [x[...].astype(f32) for x in by_feature(arrived, count)]
+    pieces = [x[...].astype(f32) for x in by_feature(arrived, count, "spread_out")]
     squares = pieces[0] * pieces[0]
     for x in pieces[1:]:
         squares = squares + x * x
@@ -277,25 +285,32 @@
     for p in range(1, count):
         mixed = mixed + normed[p].astype(f32) * mix[p : p + 1, :]
     mix_gate = jax.nn.sigmoid(jnp.sum(mixed, axis=1, keepdims=True))
-    weight = notes[:, 0:1] + notes[:, 1:2] + notes[:, 2:3]
-    dense_weight = mix_gate * notes[:, 3:4]
+    flagged = lax.broadcasted_iota(jnp.int32, notes.shape, 1) % 4 == 3
+    weight = jnp.sum(jnp.where(flagged, 0.0, notes[...]), axis=1, keepdims=True)
+    main = jnp.sum(jnp.where(flagged, notes[...], 0.0), axis=1, keepdims=True)
     second = jnp.concatenate(normed, axis=1)
-    hidden = (jax.nn.silu(dot(second, gate[...])) * dot(second, up[...])).astype(bf16)
-    dense_hidden = (
-        jax.nn.silu(dot_t(second, dense_gate[...])) * dot_t(second, dense_up[...])
-    ).astype(bf16)
-    for p, t in enumerate(member_order(count, "tp")):
-        cols = slice(t * piece, (t + 1) * piece)
-        out[p] = (
-            weight * dot(hidden, down[:, cols])
-            + dense_weight * dot(dense_hidden, dense_down[:, cols])
-        ).astype(bf16)
+    units = gate.shape[1]
+    both = dot(second, jnp.concatenate([gate[...], up[...]], axis=1))
+    hidden = jax.nn.silu(both[:, :units]) * both[:, units:] * weight
+    small = dense_gate.shape[0]
+    dense = dot_t(second, jnp.concatenate([dense_gate[...], dense_up[...]], axis=0))
+    dense_hidden = jax.nn.silu(dense[:, :small]) * dense[:, small:] * (mix_gate * main)
+    joined = jnp.concatenate([hidden, dense_hidden], axis=1).astype(bf16)
+    order = member_order(count, "sums")
+    for t in range(0, count, 2):
+        cols = slice(t * piece, (t + 2) * piece)
+        block = dot(joined, jnp.concatenate([down[:, cols], dense_down[:, cols]], axis=0))
+        for i in range(2):
+            out[order.index(t + i)] = block[:, i * piece : (i + 1) * piece].astype(bf16)
 
 
 def total_kernel(partial, out):
     total = partial[0].astype(f32)
     for p in range(1, partial.shape[0]):
         total = total + partial[p].astype(f32)
+    turn = (FIRST["back"] - FIRST["send"]) * 4 % out.shape[0]
+    if turn:
+        total = jnp.concatenate([total[turn:], total[:turn]], axis=0)
     out[...] = total.astype(bf16)
 
 
@@ -310,16 +325,16 @@
     out[...] = (base[...] + routed).astype(bf16)
 
 
-def member_order(count, axis):
-    return [(i + FIRST[axis]) % count for i in range(count)]
-
-
-def by_feature(ref, count):
-    return [ref.at[(t - FIRST["tp"]) % count] for t in range(count)]
-
-
-def exchange(value, axis):
-    order = member_order(lax.axis_size(axis), axis)
+def member_order(count, name):
+    return [(i + FIRST[name]) % count for i in range(count)]
+
+
+def by_feature(ref, count, name):
+    return [ref.at[(t - FIRST[name]) % count] for t in range(count)]
+
+
+def exchange(value, axis, name):
+    order = member_order(lax.axis_size(axis), name)
     return lax.all_to_all(value, axis, 0, 0, tiled=True, axis_index_groups=[order])
 
 
@@ -367,6 +382,7 @@
     count = lax.axis_size("tp")
     groups = lax.axis_size("ep")
     slots = groups * 4
+    sent_rows = groups * PIECE
     place = lax.axis_index("tp").reshape(1).astype(jnp.int32)
     row = lambda v: v.reshape(1, width)
     pieces = lambda v: v.reshape(count, width)
@@ -379,15 +395,15 @@
         *far(token_rows, pieces(first_gain), decay_down.T, iclr_down.T),
         in_specs=[in_smem] + [in_vmem] * 4,
     )
-    arrived = exchange(message, "tp")
+    arrived = exchange(message, "tp", "tokens")
     weights, ups, state, hit, notes, gain, rows_of = call(
         prep_kernel,
         (
             near((3, *w_key.shape), bf16),
             near((2, *decay_up.shape), bf16),
             near(prior_state.shape, f32),
-            near((2 * slots, seqs), bf16),
-            near((2 * slots, width), bf16),
+            near((sent_rows, seqs), bf16),
+            near((sent_rows, width), bf16),
             near((count, width), f32),
             near((8, width), f32),
         ),
@@ -415,7 +431,7 @@
         (near((count, seqs, width), bf16), near((5, seqs, width), f32)),
         *held(arrived, state, gain, weights, ups, rows_of),
     )
-    heads_all = exchange(heads, "tp")
+    heads_all = exchange(heads, "tp", "heads")
     block = 8
     next_state = call(
         state_kernel,
@@ -431,10 +447,10 @@
     )
     residual, outgoing = call(
         dispatch_kernel,
-        (near((seqs, width), bf16), shape((2 * slots, width), bf16)),
+        (near((seqs, width), bf16), shape((sent_rows, width), bf16)),
         *held(heads_all, w_out, token_rows, hit, notes),
     )
-    sent = exchange(outgoing.reshape(groups, 8, width), "ep")
+    sent = exchange(outgoing.reshape(groups, PIECE // 2, 2, width), "ep", "send")
     second_scale, mix_scale = call(
         gains_kernel,
         (near((count, width), f32), near((count, width), f32)),
@@ -443,9 +459,9 @@
     rows, slot_notes = call(
         spread_kernel,
         (shape((count, slots, width), bf16), near((slots, width), f32)),
-        *held(sent.reshape(2 * slots, width)),
-    )
-    gathered = exchange(rows, "tp")
+        *held(sent.reshape(sent_rows, width)),
+    )
+    gathered = exchange(rows, "tp", "spread_out")
     table = call(table_kernel, near((slots, seqs), bf16), *far(routes.T))
     partial = call(
         expert_kernel,
@@ -464,9 +480,11 @@
         ),
     )
     expert_out = call(
-        total_kernel, shape((slots, width), bf16), *held(exchange(partial, "tp"))
-    )
-    returned = exchange(expert_out.reshape(groups, 4, width), "ep")
+        total_kernel,
+        shape((slots, width), bf16),
+        *held(exchange(partial, "tp", "sums")),
+    )
+    returned = exchange(expert_out.reshape(groups, 4, width), "ep", "back")
     base = call(base_kernel, near((seqs, width), f32), *held(residual))
     layer_out = call(
         final_kernel,

time: 102 us -> 99.7 us (0.977)
  starting transfers between devices: 30.1 us -> 28.7 us
    all_to_all x3, starting transfers between devices: 30.1 us -> 28.7 us  [exchange(): lax.all_to_all(value, axis, 0, 0, tiled=True, axis_index_groups=[order])]
    all_to_all x3, blocking collectives: 49.1 us -> 48.1 us  [exchange(): lax.all_to_all(value, axis, 0, 0, tiled=True, axis_index_groups=[order])]
  transfers between devices with their start and end apart: 3 -> 3, of which waited for: 2 -> 3; matrix products, arithmetic and copies ran while one was open for 0% -> 0% of each run, Pallas kernels for 7% -> 7%
where the time goes in v4:
time: 99.7 us; the launch traced here: 99 us
  blocking collectives  48.1 us (48%)
  starting transfers between devices  28.7 us (29%)
  Pallas kernels  14.1 us (14%)
  waiting for transfers between devices  7.25 us (7%)
    all_to_all x3, blocking collectives, exchange(): lax.all_to_all(value, axis, 0, 0, tiled=True, axis_index_groups=[order])  48.1 us
    all_to_all x3, starting transfers between devices, exchange(): lax.all_to_all(value, axis, 0, 0, tiled=True, axis_index_groups=[order])  28.7 us
    pallas_call x12, Pallas kernels, call(): pl.pallas_call(kernel, out_shape=outs, compiler_params=params, **kwargs)  14.1 us
    all_to_all x3, waiting for transfers between devices, exchange(): lax.all_to_all(value, axis, 0, 0, tiled=True, axis_index_groups=[order])  7.25 us
  transfers between devices with their start and end apart: 3, of which 3 were waited for; matrix products, arithmetic and copies ran while one was open for 0% of the time, Pallas kernels for 7%

profile of v4, /device:TPU:1, one launch (start us, length us, event | category | flops | bytes accessed | tf_op | source)
XLA Modules:
  0.0 99.0 jit_solution(16910352122136784415)
XLA Ops:
  0.6 1.7 %shard_map.257 = bf16[16,24,384]{2,1,0:T(8,128)(2,1)} custom-call(s32[1]{0:T(128)} %bitcast.place, bf16[24,128]{1,0:T(8,128)(2,1)} %tokens.3, bf16[16,128]{1,0:T(8,128)(2,1)} %bitcast.32, bf16[96,128]{1,0:T(8,128)(2,1)} %bitcast.30, bf16[96,128]{1,0:T(8,128)(2,1)} %bitcast.31), custom_call_target="tpu_custom_call" | custom-call | tf_op jit(solution)/shard_map/pallas_call | solution.py:34
  2.3 9.6 %all-to-all-start = ((bf16[16,24,384]{2,1,0:T(8,128)(2,1)}), bf16[16,24,384]{2,1,0:T(8,128)(2,1)S(1)}, u32[]{:S(2)}, u32[]{:S(2)}) async-start(bf16[16,24,384]{2,1,0:T(8,128)(2,1)} %shard_map.257), calls=%async_computation | async-start | bytes 589824 | tf_op jit(solution)/shard_map/all_to_all | solution.py:338
  11.9 2.5 %shard_map.258 = (bf16[3,2048,128]{2,1,0:T(8,128)(2,1)S(1)}, bf16[2,96,128]{2,1,0:T(8,128)(2,1)S(1)}, f32[24,64,128]{2,1,0:T(8,128)S(1)}, bf16[192,24]{1,0:T(8,1...) custom-call(bf16[2048,128]{1,0:T(8,128)(2,1)} %w_recept.1, ...), custom_call_target="tpu_custom_call" | custom-call | tf_op jit(solution)/shard_map/pallas_call | solution.py:34
  14.3 0.0 copy-start
  14.3 0.0 copy-start.7
  14.4 0.5 all-to-all-done.arrived
  14.9 1.3 %shard_map.259 = (bf16[16,24,128]{2,1,0:T(8,128)(2,1)S(1)}, f32[5,24,128]{2,1,0:T(8,128)S(1)}) custom-call(bf16[16,24,384]{2,1,0:T(8,128)(2,1)S(1)} %all-to-all-done.arrived, f32[24,64,128]{2,1,0:T(8,128)S(1)} %get-tuple-element.17.state, f32[16,128]{1,0:T(8,128)S(1)} %get-tuple-element.18.gain, bf16[3,2048,128]{2,1,0:T(8,128)(2,1)S(1)} %get-tuple-element.19.weights, ...), custom_call_target="tpu_custom_call" | custom-call | tf_op jit(solution)/shard_map/pallas_call | solution.py:34
  16.3 0.0 copy-start.1
  16.3 0.0 copy-start.2
  16.3 0.0 copy-start.3
  16.3 0.0 copy-start.4
  16.3 0.0 copy-start.5
  16.3 0.0 copy-start.6
  16.3 9.0 %all_to_all.30.heads = bf16[16,24,128]{2,1,0:T(8,128)(2,1)S(1)} all-to-all(bf16[16,24,128]{2,1,0:T(8,128)(2,1)S(1)} %get-tuple-element.22), channel_id=1, replica_groups={{10,11,12,13,14,15,0,1,2,3,4,5,6,7,8,9},{26,27,28,29,30,31,16,17,18,19,..., dimensions={0} | all-to-all | bytes 196608 | tf_op jit(solution)/shard_map/all_to_all | solution.py:338
  25.3 0.0 copy-done
  25.3 0.0 copy-done.7
  25.3 0.3 shard_map.260
  25.6 25.5 %all_to_all.31 = bf16[32,3,2,128]{3,2,1,0:T(2,128)(2,1)S(1)} all-to-all(bf16[32,3,2,128]{3,2,1,0:T(2,128)(2,1)S(1)} %bitcast.29), channel_id=1, replica_groups={{336,352,368,384,400,416,432,448,464,480,496,0,16,32,48,64,80,96,112,12..., dimensions={0} | all-to-all | bytes 98304 | tf_op jit(solution)/shard_map/all_to_all | solution.py:338
  51.1 1.0 %shard_map.261 = (bf16[16,128,128]{2,1,0:T(8,128)(2,1)}, f32[128,128]{1,0:T(8,128)S(1)}) custom-call(bf16[192,128]{1,0:T(8,128)(2,1)S(1)} %bitcast.25), custom_call_target="tpu_custom_call" | custom-call | tf_op jit(solution)/shard_map/pallas_call | solution.py:34
  52.1 8.1 %all-to-all-start.3 = ((bf16[16,128,128]{2,1,0:T(8,128)(2,1)}), bf16[16,128,128]{2,1,0:T(8,128)(2,1)S(1)}, u32[]{:S(2)}, u32[]{:S(2)}) async-start(bf16[16,128,128]{2,1,0:T(8,128)(2,1)} %get-tuple-element.26), calls=%async_computation.3 | async-start | bytes 1048576 | tf_op jit(solution)/shard_map/all_to_all | solution.py:338
  60.2 0.7 shard_map.262
  60.9 6.2 %all-to-all-done.3.arrived = bf16[16,128,128]{2,1,0:T(8,128)(2,1)S(1)} async-done(((bf16[16,128,128]{2,1,0:T(8,128)(2,1)}), bf16[16,128,128]{2,1,0:T(8,128)(2,1)S(1)}, u32[]{:S(2)}, u32[]{:S(2)}) %all-to-all-start.3) | async-done | bytes 524320 | tf_op jit(solution)/shard_map/all_to_all | solution.py:338
  67.1 0.0 copy-done.1
  67.1 0.0 copy-done.2
  67.1 0.0 copy-done.3
  67.1 0.0 copy-done.4
  67.1 0.0 copy-done.5
  67.1 0.0 copy-done.6
  67.2 1.1 %shard_map.263 = bf16[16,128,128]{2,1,0:T(8,128)(2,1)S(1)} custom-call(bf16[16,128,128]{2,1,0:T(8,128)(2,1)S(1)} %all-to-all-done.3.arrived, f32[128,128]{1,0:T(8,128)S(1)} %get-tuple-element.27.notes, f32[16,128]{1,0:T(8,128)S(1)} %get-tuple-element.28.gain, f32[16,128]{1,0:T(8,128)S(1)} %get-tuple-element.29.mix, bf16[2048,128]{1,0:T(8,128)(2,1)S(1)} %bitcast.22, ...), custom_call_target="tpu_custom_call" | custom-call | tf_op jit(solution)/shard_map/pallas_call | solution.py:34
  68.2 13.6 %all_to_all.32.partial = bf16[16,128,128]{2,1,0:T(8,128)(2,1)S(1)} all-to-all(bf16[16,128,128]{2,1,0:T(8,128)(2,1)S(1)} %shard_map.263), channel_id=1, replica_groups={{10,11,12,13,14,15,0,1,2,3,4,5,6,7,8,9},{26,27,28,29,30,31,16,17,18,19,..., dimensions={0} | all-to-all | bytes 1048576 | tf_op jit(solution)/shard_map/all_to_all | solution.py:338
  81.9 0.7 shard_map.264
  82.6 11.1 %all-to-all-start.5 = ((bf16[32,4,128]{2,1,0:T(4,128)(2,1)}), bf16[32,4,128]{2,1,0:T(4,128)(2,1)S(1)}, u32[]{:S(2)}, u32[]{:S(2)}) async-start(bf16[32,4,128]{2,1,0:T(4,128)(2,1)} %bitcast.20), calls=%async_computation.5 | async-start | bytes 65536 | tf_op jit(solution)/shard_map/all_to_all | solution.py:338
  93.6 0.9 shard_map.265.table
  94.5 3.2 %shard_map.268 = f32[24,64,128]{2,1,0:T(8,128)} custom-call(f32[24,64,128]{2,1,0:T(8,128)} %state.3, f32[5,24,128]{2,1,0:T(8,128)S(1)} %get-tuple-element.31.vectors), custom_call_target="tpu_custom_call" | custom-call | tf_op jit(solution)/shard_map/pallas_call | solution.py:34
  97.7 0.5 all-to-all-done.5
  98.2 0.8 shard_map.267
  (1 shorter events, 0.0 us)
Async XLA Ops:
  2.3 12.6 %all-to-all-start = ((bf16[16,24,384]{2,1,0:T(8,128)(2,1)}), bf16[16,24,384]{2,1,0:T(8,128)(2,1)S(1)}, u32[]{:S(2)}, u32[]{:S(2)}) async-start(bf16[16,24,384]{2,1,0:T(8,128)(2,1)} %shard_map.257), calls=%async_computation | async-start | bytes 589824 | tf_op jit(solution)/shard_map/all_to_all | solution.py:338
  14.3 10.9 %copy-start = (bf16[2048,128]{1,0:T(8,128)(2,1)S(1)}, bf16[2048,128]{1,0:T(8,128)(2,1)}, u32[]{:S(2)}) copy-start(bf16[2048,128]{1,0:T(8,128)(2,1)} %w_out.1) | copy-start | bytes 1572868
  14.3 10.9 %copy-start.7 = (bf16[24,128]{1,0:T(8,128)(2,1)S(1)}, bf16[24,128]{1,0:T(8,128)(2,1)}, u32[]{:S(2)}) copy-start(bf16[24,128]{1,0:T(8,128)(2,1)} %tokens.3) | copy-start | bytes 18436
  16.3 50.9 %copy-start.1 = (bf16[1,2048,128]{2,1,0:T(8,128)(2,1)S(1)}, bf16[1,2048,128]{2,1,0:T(8,128)(2,1)}, u32[]{:S(2)}) copy-start(bf16[1,2048,128]{2,1,0:T(8,128)(2,1)} %param.45) | copy-start | bytes 1572868
  16.3 50.9 %copy-start.2 = (bf16[1,2048,128]{2,1,0:T(8,128)(2,1)S(1)}, bf16[1,2048,128]{2,1,0:T(8,128)(2,1)}, u32[]{:S(2)}) copy-start(bf16[1,2048,128]{2,1,0:T(8,128)(2,1)} %param.46) | copy-start | bytes 1572868
  16.3 50.8 %copy-start.3 = (bf16[1,128,2048]{2,1,0:T(8,128)(2,1)S(1)}, bf16[1,128,2048]{2,1,0:T(8,128)(2,1)}, u32[]{:S(2)}) copy-start(bf16[1,128,2048]{2,1,0:T(8,128)(2,1)} %param.47) | copy-start | bytes 1572868
  16.3 50.8 %copy-start.4 = (bf16[2048,32]{0,1:T(8,128)(2,1)S(1)}, bf16[2048,32]{0,1:T(8,128)(2,1)}, u32[]{:S(2)}) copy-start(bf16[2048,32]{0,1:T(8,128)(2,1)} %param.48) | copy-start | bytes 393220
  16.3 50.8 %copy-start.5 = (bf16[2048,32]{0,1:T(8,128)(2,1)S(1)}, bf16[2048,32]{0,1:T(8,128)(2,1)}, u32[]{:S(2)}) copy-start(bf16[2048,32]{0,1:T(8,128)(2,1)} %param.49) | copy-start | bytes 393220
  16.3 50.8 %copy-start.6 = (bf16[32,2048]{1,0:T(8,128)(2,1)S(1)}, bf16[32,2048]{1,0:T(8,128)(2,1)}, u32[]{:S(2)}) copy-start(bf16[32,2048]{1,0:T(8,128)(2,1)} %dense_down.1) | copy-start | bytes 393220
  52.1 15.0 %all-to-all-start.3 = ((bf16[16,128,128]{2,1,0:T(8,128)(2,1)}), bf16[16,128,128]{2,1,0:T(8,128)(2,1)S(1)}, u32[]{:S(2)}, u32[]{:S(2)}) async-start(bf16[16,128,128]{2,1,0:T(8,128)(2,1)} %get-tuple-element.26), calls=%async_computation.3 | async-start | bytes 1048576 | tf_op jit(solution)/shard_map/all_to_all | solution.py:338
  82.6 15.6 %all-to-all-start.5 = ((bf16[32,4,128]{2,1,0:T(4,128)(2,1)}), bf16[32,4,128]{2,1,0:T(4,128)(2,1)S(1)}, u32[]{:S(2)}, u32[]{:S(2)}) async-start(bf16[32,4,128]{2,1,0:T(4,128)(2,1)} %bitcast.20), calls=%async_computation.5 | async-start | bytes 65536 | tf_op jit(solution)/shard_map/all_to_all | solution.py:338

commit v5 on v4

--- a/solution.py
+++ b/solution.py
@@ -31,9 +31,7 @@
 
 def call(kernel, outs, *args, **kwargs):
     params = pltpu.CompilerParams(vmem_limit_bytes=12 << 20)
-    return pl.pallas_call(
-        kernel, out_shape=outs, compiler_params=params, **kwargs
-    )(*args)
+    return pl.pallas_call(kernel, out_shape=outs, compiler_params=params, **kwargs)(*args)
 
 
 def shape(dims, dtype):
@@ -66,21 +64,20 @@
 def message_kernel(place, tokens, gain, decay_down, iclr_down, out):
     rows = lax.broadcasted_iota(jnp.int32, gain.shape, 0)
     own = jnp.sum(jnp.where(rows == place[0], gain[...].astype(f32), 0.0), axis=0, keepdims=True)
-    scaled = (tokens[...].astype(f32) * own).astype(bf16)
-    count, seqs, width = out.shape
-    rank = decay_down.shape[0]
-    pad = jnp.zeros((seqs, width // 3 - rank), f32)
-    whole = jnp.concatenate(
-        [
-            tokens[...].astype(f32),
-            dot_t(scaled, decay_down[...]),
-            pad,
-            dot_t(scaled, iclr_down[...]),
-            pad,
-        ],
-        axis=1,
-    ).astype(bf16)
-    for p in range(count):
+    values = tokens[...].astype(f32)
+    scaled = (values * own).astype(bf16)
+    width = tokens.shape[1]
+    low = dot_t(scaled, jnp.concatenate([decay_down[...], iclr_down[...]], axis=0))
+    squares = in_three(jnp.sum(values * values, axis=1, keepdims=True))
+    lanes = lax.broadcasted_iota(jnp.int32, (8, width - HEAD), 1)
+    corner = jnp.zeros(lanes.shape, f32)
+    for g in range(3):
+        for i in range(3):
+            corner = jnp.where(lanes == 3 * g + i, squares[i][8 * g : 8 * g + 8], corner)
+    rest = low[:, width:]
+    tail = jnp.concatenate([rest[:16], jnp.concatenate([rest[16:], corner], axis=0)], axis=1)
+    whole = jnp.concatenate([scaled.astype(f32), low[:, :width], tail], axis=0).astype(bf16)
+    for p in range(out.shape[0]):
         out[p] = whole
 
 
@@ -114,7 +111,6 @@
     state,
     routes,
     route_weights,
-    gain,
     decay_base,
     iclr_base,
     key_scale,
@@ -125,7 +121,6 @@
     state_out,
     hit_out,
     notes_out,
-    gain_out,
     rows_out,
     sems,
 ):
@@ -149,7 +144,6 @@
             notes = jnp.where(lanes == 4 * c + i, column, notes)
     rows = lax.broadcasted_iota(jnp.int32, notes_out.shape, 0)
     notes_out[...] = jnp.where(rows % PIECE == 4, notes, 0.0).astype(bf16)
-    gain_out[...] = gain[...].astype(f32)
     for i, row in enumerate((decay_base, iclr_base, key_scale, key_mix, head_gain)):
         rows_out[i : i + 1, :] = row[...].astype(f32)
     for copy in copies:
@@ -166,40 +160,42 @@
     out[...] = jnp.where(offset == 0.0, chosen, 0.0).astype(bf16)
 
 
-def mixer_in_kernel(
-    arrived, state, gain, weights, ups, rows, heads_out, vectors_out
-):
-    count, seqs, width = arrived.shape
-    piece = width // 3
+def mixer_in_kernel(arrived, state, weights, ups, rows, heads_out, vectors_out):
+    count, _, piece = arrived.shape
+    seqs = state.shape[0]
     rank = ups.shape[1]
+    split = piece - rank
     decay_base, iclr_base, key_scale, key_mix, head_gain = (rows[i : i + 1, :] for i in range(5))
-    tokens = [x[:, :piece].astype(f32) for x in by_feature(arrived, count, "tokens")]
-    squares = tokens[0] * tokens[0]
-    for x in tokens[1:]:
-        squares = squares + x * x
-    scale = lax.rsqrt(
-        jnp.sum(squares, axis=1, keepdims=True) * (1.0 / (count * piece)) + norm_eps
-    )
-    first = jnp.concatenate(
+    first = jnp.concatenate([x[:seqs] for x in by_feature(arrived, count, "tokens")], axis=1)
+    low = arrived[0, seqs:].astype(f32)
+    for p in range(1, count):
+        low = low + arrived[p, seqs:].astype(f32)
+    tail = low[seqs:]
+    lanes = lax.broadcasted_iota(jnp.int32, (8, piece), 1) - HEAD
+    squares = jnp.concatenate(
         [
-            (x * scale * gain[p : p + 1, :]).astype(bf16)
-            for p, x in enumerate(tokens)
+            jnp.sum(
+                jnp.where((lanes >= 3 * g) & (lanes < 3 * g + 3), tail[8:], 0.0),
+                axis=1,
+                keepdims=True,
+            )
+            for g in range(3)
         ],
-        axis=1,
-    )
-    low = arrived[0, :, piece:].astype(f32)
-    for p in range(1, count):
-        low = low + arrived[p, :, piece:].astype(f32)
-    low = low * scale
-    decay_act = jnp.tanh(low[:, :rank]).astype(bf16)
-    rate_act = low[:, piece : piece + rank].astype(bf16)
-    projected = dot(first, jnp.concatenate([weights[i] for i in range(3)], axis=1))
-    projected = projected.astype(bf16).astype(f32)
-    recept, key, value = (projected[:, i * piece : (i + 1) * piece] for i in range(3))
+        axis=0,
+    )
+    scale = lax.rsqrt(squares * (1.0 / (count * piece)) + norm_eps)
+    near_low = low[:seqs] * scale
+    far_low = jnp.concatenate([tail[:, :HEAD], tail[:8, HEAD:]], axis=0) * scale
+    decay_act = jnp.tanh(near_low[:, :rank]).astype(bf16)
+    rate_near = near_low[:, rank:].astype(bf16)
+    rate_far = far_low.astype(bf16)
+    recept, key, value = (
+        (dot(first, weights[i]) * scale).astype(bf16).astype(f32) for i in range(3)
+    )
     decay_pre = -(decay_base + dot(decay_act, ups[0]))
     softplus = jnp.maximum(decay_pre, 0.0) + jnp.log1p(jnp.exp(-jnp.abs(decay_pre)))
     decay = jnp.exp(-jnp.exp(-softplus - 0.5))
-    rate = jax.nn.sigmoid(iclr_base + dot(rate_act, ups[1]))
+    rate = jax.nn.sigmoid(iclr_base + dot(rate_near, ups[1, :split]) + dot(rate_far, ups[1, split:]))
     scaled = key * key_scale
     removal = scaled * lax.rsqrt(head_sum(scaled * scaled) + key_eps)
     written = key * (1.0 + (rate - 1.0) * key_mix)
@@ -268,7 +264,19 @@
 
 
 def expert_kernel(
-    arrived, notes, gain, mix, gate, up, down, dense_gate, dense_up, dense_down, out
+    arrived,
+    notes,
+    gain,
+    mix,
+    gate,
+    up,
+    down,
+    dense_gate,
+    dense_up,
+    dense_down,
+    out,
+    made,
+    sems,
 ):
     count, _, piece = arrived.shape
     pieces = [x[...].astype(f32) for x in by_feature(arrived, count, "spread_out")]
@@ -297,11 +305,18 @@
     dense_hidden = jax.nn.silu(dense[:, :small]) * dense[:, small:] * (mix_gate * main)
     joined = jnp.concatenate([hidden, dense_hidden], axis=1).astype(bf16)
     order = member_order(count, "sums")
-    for t in range(0, count, 2):
-        cols = slice(t * piece, (t + 2) * piece)
+    copies = []
+    for p in range(0, count, 2):
+        cols = slice(order[p] * piece, (order[p] + 2) * piece)
         block = dot(joined, jnp.concatenate([down[:, cols], dense_down[:, cols]], axis=0))
         for i in range(2):
-            out[order.index(t + i)] = block[:, i * piece : (i + 1) * piece].astype(bf16)
+            made[p + i] = block[:, i * piece : (i + 1) * piece].astype(bf16)
+        if p % 8 == 6:
+            part = pl.ds(p - 6, 8)
+            copies.append(pltpu.make_async_copy(made.at[part], out.at[part], sems.at[p // 8]))
+            copies[-1].start()
+    for copy in copies:
+        copy.wait()
 
 
 def total_kernel(partial, out):
@@ -390,13 +405,13 @@
     in_vmem = pl.BlockSpec(memory_space=pltpu.VMEM)
     message = call(
         message_kernel,
-        shape((count, seqs, 3 * width), bf16),
+        shape((count, 2 * seqs + 16, width), bf16),
         place,
         *far(token_rows, pieces(first_gain), decay_down.T, iclr_down.T),
         in_specs=[in_smem] + [in_vmem] * 4,
     )
     arrived = exchange(message, "tp", "tokens")
-    weights, ups, state, hit, notes, gain, rows_of = call(
+    weights, ups, state, hit, notes, rows_of = call(
         prep_kernel,
         (
             near((3, *w_key.shape), bf16),
@@ -404,7 +419,6 @@
             near(prior_state.shape, f32),
             near((sent_rows, seqs), bf16),
             near((sent_rows, width), bf16),
-            near((count, width), f32),
             near((8, width), f32),
         ),
         *far(
@@ -416,20 +430,19 @@
             prior_state,
             routes.T,
             route_weights.T,
-            pieces(first_gain),
             row(decay_base),
             row(iclr_base),
             row(key_scale),
             row(key_mix),
             row(head_gain),
         ),
-        in_specs=[pl.BlockSpec(memory_space=pl.ANY)] * 6 + [in_vmem] * 8,
+        in_specs=[pl.BlockSpec(memory_space=pl.ANY)] * 6 + [in_vmem] * 7,
         scratch_shapes=[pltpu.SemaphoreType.DMA((6,))],
     )
     heads, vectors = call(
         mixer_in_kernel,
         (near((count, seqs, width), bf16), near((5, seqs, width), f32)),
-        *held(arrived, state, gain, weights, ups, rows_of),
+        *held(arrived, state, weights, ups, rows_of),
     )
     heads_all = exchange(heads, "tp", "heads")
     block = 8
@@ -478,18 +491,19 @@
             dense_up.T,
             dense_down,
         ),
+        out_specs=pl.BlockSpec(memory_space=pl.ANY),
+        scratch_shapes=[
+            pltpu.VMEM((count, slots, width), bf16),
+            pltpu.SemaphoreType.DMA((2,)),
+        ],
     )
     expert_out = call(
-        total_kernel,
-        shape((slots, width), bf16),
-        *held(exchange(partial, "tp", "sums")),
+        total_kernel, shape((slots, width), bf16), *held(exchange(partial, "tp", "sums"))
     )
     returned = exchange(expert_out.reshape(groups, 4, width), "ep", "back")
     base = call(base_kernel, near((seqs, width), f32), *held(residual))
     layer_out = call(
-        final_kernel,
-        shape((seqs, width), bf16),
-        *held(returned.reshape(slots, width), table, base),
+        final_kernel, shape((seqs, width), bf16), *held(returned.reshape(slots, width), table, base)
     )
     return (layer_out, next_state)
 

time: 99.7 us -> 99.4 us (level)
  no operation moved by 1% of the time
where the time goes in v5:
time: 99.4 us; the launch traced here: 98.7 us
  blocking collectives  48 us (48%)
  starting transfers between devices  28.7 us (29%)
  Pallas kernels  14.2 us (14%)
  waiting for transfers between devices  7.05 us (7%)
    all_to_all x3, blocking collectives, exchange(): lax.all_to_all(value, axis, 0, 0, tiled=True, axis_index_groups=[order])  48 us
    all_to_all x3, starting transfers between devices, exchange(): lax.all_to_all(value, axis, 0, 0, tiled=True, axis_index_groups=[order])  28.7 us
    pallas_call x12, Pallas kernels, call(): pl.pallas_call(kernel, out_shape=outs, compiler_params=params, **kwargs)  14.2 us
    all_to_all x3, waiting for transfers between devices, exchange(): lax.all_to_all(value, axis, 0, 0, tiled=True, axis_index_groups=[order])  7.05 us
  transfers between devices with their start and end apart: 3, of which 3 were waited for; matrix products, arithmetic and copies ran while one was open for 0% of the time, Pallas kernels for 7%

profile of v5, /device:TPU:1, one launch (start us, length us, event | category | flops | bytes accessed | tf_op | source)
XLA Modules:
  0.0 98.7 jit_solution(1421894690139104544)
XLA Ops:
  0.6 1.7 %shard_map.257 = bf16[16,64,128]{2,1,0:T(8,128)(2,1)} custom-call(s32[1]{0:T(128)} %bitcast.place, bf16[24,128]{1,0:T(8,128)(2,1)} %tokens.3, bf16[16,128]{1,0:T(8,128)(2,1)} %bitcast.34, bf16[96,128]{1,0:T(8,128)(2,1)} %bitcast.30, bf16[96,128]{1,0:T(8,128)(2,1)} %bitcast.31), custom_call_target="tpu_custom_call" | custom-call | tf_op jit(solution)/shard_map/pallas_call | solution.py:34
  2.4 9.5 %all-to-all-start = ((bf16[16,64,128]{2,1,0:T(8,128)(2,1)}), bf16[16,64,128]{2,1,0:T(8,128)(2,1)S(1)}, u32[]{:S(2)}, u32[]{:S(2)}) async-start(bf16[16,64,128]{2,1,0:T(8,128)(2,1)} %shard_map.257), calls=%async_computation | async-start | bytes 524288 | tf_op jit(solution)/shard_map/all_to_all | solution.py:353
  11.9 2.5 %shard_map.258 = (bf16[3,2048,128]{2,1,0:T(8,128)(2,1)S(1)}, bf16[2,96,128]{2,1,0:T(8,128)(2,1)S(1)}, f32[24,64,128]{2,1,0:T(8,128)S(1)}, bf16[192,24]{1,0:T(8,1...) custom-call(bf16[2048,128]{1,0:T(8,128)(2,1)} %w_recept.1, bf16[2048,128]{1,0:T(8,128)(2,1)} %w_key.1, ...), custom_call_target="tpu_custom_call" | custom-call | tf_op jit(solution)/shard_map/pallas_call | solution.py:34
  14.4 0.0 copy-start
  14.4 0.0 copy-start.7
  14.4 0.3 all-to-all-done.arrived
  14.7 1.1 %shard_map.259 = (bf16[16,24,128]{2,1,0:T(8,128)(2,1)S(1)}, f32[5,24,128]{2,1,0:T(8,128)S(1)}) custom-call(bf16[16,64,128]{2,1,0:T(8,128)(2,1)S(1)} %all-to-all-done.arrived, f32[24,64,128]{2,1,0:T(8,128)S(1)} %get-tuple-element.16.state, bf16[3,2048,128]{2,1,0:T(8,128)(2,1)S(1)} %get-tuple-element.17.weights, ...), custom_call_target="tpu_custom_call" | custom-call | tf_op jit(solution)/shard_map/pallas_call | solution.py:34
  15.9 0.0 copy-start.1
  15.9 0.0 copy-start.2
  15.9 0.0 copy-start.3
  15.9 0.0 copy-start.4
  15.9 0.0 copy-start.5
  16.0 0.0 copy-start.6
  16.0 9.1 %all_to_all.30.heads = bf16[16,24,128]{2,1,0:T(8,128)(2,1)S(1)} all-to-all(bf16[16,24,128]{2,1,0:T(8,128)(2,1)S(1)} %get-tuple-element.20), channel_id=1, replica_groups={{10,11,12,13,14,15,0,1,2,3,4,5,6,7,8,9},{26,27,28,29,30,31,16,17,18,19,..., dimensions={0} | all-to-all | bytes 196608 | tf_op jit(solution)/shard_map/all_to_all | solution.py:353
  25.1 0.0 copy-done
  25.1 0.0 copy-done.7
  25.1 0.3 shard_map.260
  25.4 25.3 %all_to_all.31 = bf16[32,3,2,128]{3,2,1,0:T(2,128)(2,1)S(1)} all-to-all(bf16[32,3,2,128]{3,2,1,0:T(2,128)(2,1)S(1)} %bitcast.29), channel_id=1, replica_groups={{336,352,368,384,400,416,432,448,464,480,496,0,16,32,48,64,80,96,112,12..., dimensions={0} | all-to-all | bytes 98304 | tf_op jit(solution)/shard_map/all_to_all | solution.py:353
  50.7 1.0 %shard_map.261 = (bf16[16,128,128]{2,1,0:T(8,128)(2,1)}, f32[128,128]{1,0:T(8,128)S(1)}) custom-call(bf16[192,128]{1,0:T(8,128)(2,1)S(1)} %bitcast.25), custom_call_target="tpu_custom_call" | custom-call | tf_op jit(solution)/shard_map/pallas_call | solution.py:34
  51.7 8.1 %all-to-all-start.3 = ((bf16[16,128,128]{2,1,0:T(8,128)(2,1)}), bf16[16,128,128]{2,1,0:T(8,128)(2,1)S(1)}, u32[]{:S(2)}, u32[]{:S(2)}) async-start(bf16[16,128,128]{2,1,0:T(8,128)(2,1)} %get-tuple-element.24), calls=%async_computation.3 | async-start | bytes 1048576 | tf_op jit(solution)/shard_map/all_to_all | solution.py:353
  59.8 0.7 shard_map.262
  60.5 6.2 %all-to-all-done.3.arrived = bf16[16,128,128]{2,1,0:T(8,128)(2,1)S(1)} async-done(((bf16[16,128,128]{2,1,0:T(8,128)(2,1)}), bf16[16,128,128]{2,1,0:T(8,128)(2,1)S(1)}, u32[]{:S(2)}, u32[]{:S(2)}) %all-to-all-start.3) | async-done | bytes 524320 | tf_op jit(solution)/shard_map/all_to_all | solution.py:353
  66.7 0.0 copy-done.1
  66.7 0.0 copy-done.2
  66.7 0.0 copy-done.3
  66.7 0.0 copy-done.4
  66.7 0.0 copy-done.5
  66.7 0.0 copy-done.6
  66.7 1.3 %shard_map.263 = bf16[16,128,128]{2,1,0:T(8,128)(2,1)S(1)} custom-call(bf16[16,128,128]{2,1,0:T(8,128)(2,1)S(1)} %all-to-all-done.3.arrived, f32[128,128]{1,0:T(8,128)S(1)} %get-tuple-element.25.notes, f32[16,128]{1,0:T(8,128)S(1)} %get-tuple-element.26.gain, f32[16,128]{1,0:T(8,128)S(1)} %get-tuple-element.27.mix, bf16[2048,128]{1,0:T(8,128)(2,1)S(1)} %bitcast.22, ...), custom_call_target="tpu_custom_call" | custom-call | tf_op jit(solution)/shard_map/pallas_call | solution.py:34
  68.0 13.7 %all_to_all.32.partial = bf16[16,128,128]{2,1,0:T(8,128)(2,1)S(1)} all-to-all(bf16[16,128,128]{2,1,0:T(8,128)(2,1)S(1)} %shard_map.263), channel_id=1, replica_groups={{10,11,12,13,14,15,0,1,2,3,4,5,6,7,8,9},{26,27,28,29,30,31,16,17,18,19,..., dimensions={0} | all-to-all | bytes 1048576 | tf_op jit(solution)/shard_map/all_to_all | solution.py:353
  81.7 0.7 shard_map.264
  82.3 11.0 %all-to-all-start.5 = ((bf16[32,4,128]{2,1,0:T(4,128)(2,1)}), bf16[32,4,128]{2,1,0:T(4,128)(2,1)S(1)}, u32[]{:S(2)}, u32[]{:S(2)}) async-start(bf16[32,4,128]{2,1,0:T(4,128)(2,1)} %bitcast.20), calls=%async_computation.5 | async-start | bytes 65536 | tf_op jit(solution)/shard_map/all_to_all | solution.py:353
  93.4 0.9 shard_map.265.table
  94.2 3.2 %shard_map.268 = f32[24,64,128]{2,1,0:T(8,128)} custom-call(f32[24,64,128]{2,1,0:T(8,128)} %state.3, f32[5,24,128]{2,1,0:T(8,128)S(1)} %get-tuple-element.29.vectors), custom_call_target="tpu_custom_call" | custom-call | tf_op jit(solution)/shard_map/pallas_call | solution.py:34
  97.5 0.5 all-to-all-done.5
  98.0 0.8 shard_map.267
  (1 shorter events, 0.0 us)
Async XLA Ops:
  2.4 12.4 %all-to-all-start = ((bf16[16,64,128]{2,1,0:T(8,128)(2,1)}), bf16[16,64,128]{2,1,0:T(8,128)(2,1)S(1)}, u32[]{:S(2)}, u32[]{:S(2)}) async-start(bf16[16,64,128]{2,1,0:T(8,128)(2,1)} %shard_map.257), calls=%async_computation | async-start | bytes 524288 | tf_op jit(solution)/shard_map/all_to_all | solution.py:353
  14.4 10.7 %copy-start = (bf16[2048,128]{1,0:T(8,128)(2,1)S(1)}, bf16[2048,128]{1,0:T(8,128)(2,1)}, u32[]{:S(2)}) copy-start(bf16[2048,128]{1,0:T(8,128)(2,1)} %w_out.1) | copy-start | bytes 1572868
  14.4 10.7 %copy-start.7 = (bf16[24,128]{1,0:T(8,128)(2,1)S(1)}, bf16[24,128]{1,0:T(8,128)(2,1)}, u32[]{:S(2)}) copy-start(bf16[24,128]{1,0:T(8,128)(2,1)} %tokens.3) | copy-start | bytes 18436
  15.9 50.8 %copy-start.1 = (bf16[1,2048,128]{2,1,0:T(8,128)(2,1)S(1)}, bf16[1,2048,128]{2,1,0:T(8,128)(2,1)}, u32[]{:S(2)}) copy-start(bf16[1,2048,128]{2,1,0:T(8,128)(2,1)} %param.45) | copy-start | bytes 1572868
  15.9 50.8 %copy-start.2 = (bf16[1,2048,128]{2,1,0:T(8,128)(2,1)S(1)}, bf16[1,2048,128]{2,1,0:T(8,128)(2,1)}, u32[]{:S(2)}) copy-start(bf16[1,2048,128]{2,1,0:T(8,128)(2,1)} %param.46) | copy-start | bytes 1572868
  15.9 50.8 %copy-start.3 = (bf16[1,128,2048]{2,1,0:T(8,128)(2,1)S(1)}, bf16[1,128,2048]{2,1,0:T(8,128)(2,1)}, u32[]{:S(2)}) copy-start(bf16[1,128,2048]{2,1,0:T(8,128)(2,1)} %param.47) | copy-start | bytes 1572868
  15.9 50.8 %copy-start.4 = (bf16[2048,32]{0,1:T(8,128)(2,1)S(1)}, bf16[2048,32]{0,1:T(8,128)(2,1)}, u32[]{:S(2)}) copy-start(bf16[2048,32]{0,1:T(8,128)(2,1)} %param.48) | copy-start | bytes 393220
  15.9 50.8 %copy-start.5 = (bf16[2048,32]{0,1:T(8,128)(2,1)S(1)}, bf16[2048,32]{0,1:T(8,128)(2,1)}, u32[]{:S(2)}) copy-start(bf16[2048,32]{0,1:T(8,128)(2,1)} %param.49) | copy-start | bytes 393220
  16.0 50.8 %copy-start.6 = (bf16[32,2048]{1,0:T(8,128)(2,1)S(1)}, bf16[32,2048]{1,0:T(8,128)(2,1)}, u32[]{:S(2)}) copy-start(bf16[32,2048]{1,0:T(8,128)(2,1)} %dense_down.1) | copy-start | bytes 393220
  51.7 15.0 %all-to-all-start.3 = ((bf16[16,128,128]{2,1,0:T(8,128)(2,1)}), bf16[16,128,128]{2,1,0:T(8,128)(2,1)S(1)}, u32[]{:S(2)}, u32[]{:S(2)}) async-start(bf16[16,128,128]{2,1,0:T(8,128)(2,1)} %get-tuple-element.24), calls=%async_computation.3 | async-start | bytes 1048576 | tf_op jit(solution)/shard_map/all_to_all | solution.py:353
  82.3 15.6 %all-to-all-start.5 = ((bf16[32,4,128]{2,1,0:T(4,128)(2,1)}), bf16[32,4,128]{2,1,0:T(4,128)(2,1)S(1)}, u32[]{:S(2)}, u32[]{:S(2)}) async-start(bf16[32,4,128]{2,1,0:T(4,128)(2,1)} %bitcast.20), calls=%async_computation.5 | async-start | bytes 65536 | tf_op jit(solution)/shard_map/all_to_all | solution.py:353

commit v6 on v5

--- a/solution.py
+++ b/solution.py
@@ -10,7 +10,7 @@
 f32 = jnp.float32
 bf16 = jnp.bfloat16
 
-FIRST = {"tokens": 10, "heads": 10, "spread_out": 10, "sums": 10, "send": 21, "back": 21}
+FIRST = {"tokens": 10, "heads": 10, "spread_out": 10, "sums": 10, "send": 23, "back": 23}
 
 PIECE = 6
 
@@ -152,7 +152,7 @@
 
 def gains_kernel(gain, mix, gain_out, mix_out):
     gain_out[...] = gain[...].astype(f32)
-    mix_out[...] = mix[...].astype(f32)
+    mix_out[...] = jnp.broadcast_to(mix[...].astype(f32), mix_out.shape).astype(bf16)
 
 
 def table_kernel(routes, out):
@@ -249,23 +249,36 @@
     outgoing[...] = (dot(hit[...], residual) + notes[...].astype(f32)).astype(bf16)
 
 
-def spread_kernel(arrived, out, notes_out):
-    count, slots, width = out.shape
-    size = arrived.shape[0]
+def place_in_piece(slots, size):
     slot = lax.broadcasted_iota(jnp.int32, (slots, size), 0)
-    place = lax.broadcasted_iota(jnp.int32, (slots, size), 1) - slot // 4 * PIECE
-    rows = dot(jnp.where(place == slot % 4, 1.0, 0.0).astype(bf16), arrived[...]).astype(bf16)
-    for p in range(count):
+    return slot % 4, lax.broadcasted_iota(jnp.int32, (slots, size), 1) - slot // 4 * PIECE
+
+
+def spread_kernel(arrived, out):
+    own, place = place_in_piece(out.shape[1], arrived.shape[0])
+    rows = dot(jnp.where(place == own, 1.0, 0.0).astype(bf16), arrived[...]).astype(bf16)
+    for p in range(out.shape[0]):
         out[p] = rows
+
+
+def notes_kernel(arrived, weight_out, main_out):
+    slots, width = weight_out.shape
+    _, place = place_in_piece(slots, arrived.shape[0])
     notes = dot(jnp.where(place == 4, 1.0, 0.0).astype(bf16), arrived[...])
     lane = lax.broadcasted_iota(jnp.int32, (slots, width), 1)
     own = lax.broadcasted_iota(jnp.int32, (slots, width), 0) % 4
-    notes_out[...] = jnp.where(lane // 4 == own, notes, 0.0)
+    notes = jnp.where(lane // 4 == own, notes, 0.0)
+    flagged = lane % 4 == 3
+    weight = jnp.sum(jnp.where(flagged, 0.0, notes), axis=1, keepdims=True)
+    main = jnp.sum(jnp.where(flagged, notes, 0.0), axis=1, keepdims=True)
+    weight_out[...] = jnp.broadcast_to(weight, weight_out.shape)
+    main_out[...] = jnp.broadcast_to(main, main_out.shape)
 
 
 def expert_kernel(
     arrived,
-    notes,
+    weight,
+    main,
     gain,
     mix,
     gate,
@@ -289,20 +302,14 @@
     normed = [
         (x * scale * gain[p : p + 1, :]).astype(bf16) for p, x in enumerate(pieces)
     ]
-    mixed = normed[0].astype(f32) * mix[0:1, :]
-    for p in range(1, count):
-        mixed = mixed + normed[p].astype(f32) * mix[p : p + 1, :]
-    mix_gate = jax.nn.sigmoid(jnp.sum(mixed, axis=1, keepdims=True))
-    flagged = lax.broadcasted_iota(jnp.int32, notes.shape, 1) % 4 == 3
-    weight = jnp.sum(jnp.where(flagged, 0.0, notes[...]), axis=1, keepdims=True)
-    main = jnp.sum(jnp.where(flagged, notes[...], 0.0), axis=1, keepdims=True)
     second = jnp.concatenate(normed, axis=1)
     units = gate.shape[1]
     both = dot(second, jnp.concatenate([gate[...], up[...]], axis=1))
-    hidden = jax.nn.silu(both[:, :units]) * both[:, units:] * weight
+    hidden = jax.nn.silu(both[:, :units]) * both[:, units:] * weight[...]
     small = dense_gate.shape[0]
-    dense = dot_t(second, jnp.concatenate([dense_gate[...], dense_up[...]], axis=0))
-    dense_hidden = jax.nn.silu(dense[:, :small]) * dense[:, small:] * (mix_gate * main)
+    dense = dot_t(second, jnp.concatenate([dense_gate[...], dense_up[...], mix[...]], axis=0))
+    mix_gate = jax.nn.sigmoid(dense[:, 2 * small : 2 * small + 1]) * main[:, 0:1]
+    dense_hidden = jax.nn.silu(dense[:, :small]) * dense[:, small : 2 * small] * mix_gate
     joined = jnp.concatenate([hidden, dense_hidden], axis=1).astype(bf16)
     order = member_order(count, "sums")
     copies = []
@@ -466,22 +473,23 @@
     sent = exchange(outgoing.reshape(groups, PIECE // 2, 2, width), "ep", "send")
     second_scale, mix_scale = call(
         gains_kernel,
-        (near((count, width), f32), near((count, width), f32)),
-        *far(pieces(second_gain), pieces(dense_mix)),
-    )
-    rows, slot_notes = call(
-        spread_kernel,
-        (shape((count, slots, width), bf16), near((slots, width), f32)),
-        *held(sent.reshape(sent_rows, width)),
-    )
+        (near((count, width), f32), near((8, count * width), bf16)),
+        *far(pieces(second_gain), dense_mix.reshape(1, count * width)),
+    )
+    sent = sent.reshape(sent_rows, width)
+    rows = call(spread_kernel, shape((count, slots, width), bf16), *held(sent))
     gathered = exchange(rows, "tp", "spread_out")
     table = call(table_kernel, near((slots, seqs), bf16), *far(routes.T))
+    slot_weight, slot_main = call(
+        notes_kernel, (near((slots, width), f32), near((slots, width), f32)), *held(sent)
+    )
     partial = call(
         expert_kernel,
         shape((count, slots, width), bf16),
         *held(
             gathered,
-            slot_notes,
+            slot_weight,
+            slot_main,
             second_scale,
             mix_scale,
             exp_gate[0],

time: 99.4 us -> 99.3 us (level)
  starting transfers between devices: 28.7 us -> 27.5 us
    all_to_all x3, starting transfers between devices: 28.7 us -> 27.5 us  [exchange(): lax.all_to_all(value, axis, 0, 0, tiled=True, axis_index_groups=[order])]
    pallas_call x12 -> x13, Pallas kernels: 14.2 us -> 14.3 us  [call(): pl.pallas_call(kernel, out_shape=outs, compiler_params=params, **kwargs)]
  transfers between devices with their start and end apart: 3 -> 3, of which waited for: 3 -> 3; matrix products, arithmetic and copies ran while one was open for 0% -> 1% of each run, Pallas kernels for 7% -> 8%
where the time goes in v6:
time: 99.3 us; the launch traced here: 98.6 us
  blocking collectives  48.3 us (49%)
  starting transfers between devices  27.5 us (28%)
  Pallas kernels  14.3 us (14%)
  waiting for transfers between devices  7.13 us (7%)
    all_to_all x3, blocking collectives, exchange(): lax.all_to_all(value, axis, 0, 0, tiled=True, axis_index_groups=[order])  48.3 us
    all_to_all x3, starting transfers between devices, exchange(): lax.all_to_all(value, axis, 0, 0, tiled=True, axis_index_groups=[order])  27.5 us
    pallas_call x13, Pallas kernels, call(): pl.pallas_call(kernel, out_shape=outs, compiler_params=params, **kwargs)  14.3 us
    all_to_all x3, waiting for transfers between devices, exchange(): lax.all_to_all(value, axis, 0, 0, tiled=True, axis_index_groups=[order])  7.13 us
  transfers between devices with their start and end apart: 3, of which 3 were waited for; matrix products, arithmetic and copies ran while one was open for 1% of the time, Pallas kernels for 8%

profile of v6, /device:TPU:1, one launch (start us, length us, event | category | flops | bytes accessed | tf_op | source)
XLA Modules:
  0.0 98.6 jit_solution(1041084059074879887)
XLA Ops:
  0.6 1.7 %shard_map.257 = bf16[16,64,128]{2,1,0:T(8,128)(2,1)} custom-call(s32[1]{0:T(128)} %bitcast.place, bf16[24,128]{1,0:T(8,128)(2,1)} %tokens.3, bf16[16,128]{1,0:T(8,128)(2,1)} %bitcast.34, bf16[96,128]{1,0:T(8,128)(2,1)} %bitcast.30, bf16[96,128]{1,0:T(8,128)(2,1)} %bitcast.31), custom_call_target="tpu_custom_call" | custom-call | tf_op jit(solution)/shard_map/pallas_call | solution.py:34
  2.4 9.5 %all-to-all-start = ((bf16[16,64,128]{2,1,0:T(8,128)(2,1)}), bf16[16,64,128]{2,1,0:T(8,128)(2,1)S(1)}, u32[]{:S(2)}, u32[]{:S(2)}) async-start(bf16[16,64,128]{2,1,0:T(8,128)(2,1)} %shard_map.257), calls=%async_computation | async-start | bytes 524288 | tf_op jit(solution)/shard_map/all_to_all | solution.py:360
  11.9 2.5 %shard_map.258 = (bf16[3,2048,128]{2,1,0:T(8,128)(2,1)S(1)}, bf16[2,96,128]{2,1,0:T(8,128)(2,1)S(1)}, f32[24,64,128]{2,1,0:T(8,128)S(1)}, bf16[192,24]{1,0:T(8,1...) custom-call(bf16[2048,128]{1,0:T(8,128)(2,1)} %w_recept.1, bf16[2048,128]{1,0:T(8,128)(2,1)} %w_key.1, ...), custom_call_target="tpu_custom_call" | custom-call | tf_op jit(solution)/shard_map/pallas_call | solution.py:34
  14.4 0.0 copy-start.3
  14.4 0.0 copy-start.7
  14.4 0.3 all-to-all-done.arrived
  14.7 1.1 %shard_map.259 = (bf16[16,24,128]{2,1,0:T(8,128)(2,1)S(1)}, f32[5,24,128]{2,1,0:T(8,128)S(1)}) custom-call(bf16[16,64,128]{2,1,0:T(8,128)(2,1)S(1)} %all-to-all-done.arrived, f32[24,64,128]{2,1,0:T(8,128)S(1)} %get-tuple-element.16.state, bf16[3,2048,128]{2,1,0:T(8,128)(2,1)S(1)} %get-tuple-element.17.weights, ...), custom_call_target="tpu_custom_call" | custom-call | tf_op jit(solution)/shard_map/pallas_call | solution.py:34
  15.9 0.0 copy-start.8
  15.9 0.0 copy-start
  15.9 0.0 copy-start.1
  15.9 0.0 copy-start.2
  15.9 0.0 copy-start.4
  16.0 0.0 copy-start.5
  16.0 0.0 copy-start.6
  16.0 9.1 %all_to_all.30.heads = bf16[16,24,128]{2,1,0:T(8,128)(2,1)S(1)} all-to-all(bf16[16,24,128]{2,1,0:T(8,128)(2,1)S(1)} %get-tuple-element.20), channel_id=1, replica_groups={{10,11,12,13,14,15,0,1,2,3,4,5,6,7,8,9},{26,27,28,29,30,31,16,17,18,19,..., dimensions={0} | all-to-all | bytes 196608 | tf_op jit(solution)/shard_map/all_to_all | solution.py:360
  25.1 0.0 copy-done.3
  25.1 0.0 copy-done.7
  25.1 0.3 shard_map.260
  25.4 25.4 %all_to_all.31 = bf16[32,3,2,128]{3,2,1,0:T(2,128)(2,1)S(1)} all-to-all(bf16[32,3,2,128]{3,2,1,0:T(2,128)(2,1)S(1)} %bitcast.29), channel_id=1, replica_groups={{368,384,400,416,432,448,464,480,496,0,16,32,48,64,80,96,112,128,144,16..., dimensions={0} | all-to-all | bytes 98304 | tf_op jit(solution)/shard_map/all_to_all | solution.py:360
  50.8 1.0 %shard_map.261 = bf16[16,128,128]{2,1,0:T(8,128)(2,1)} custom-call(bf16[192,128]{1,0:T(8,128)(2,1)S(1)} %bitcast.24), custom_call_target="tpu_custom_call" | custom-call | tf_op jit(solution)/shard_map/pallas_call | solution.py:34
  51.8 8.1 %all-to-all-start.3 = ((bf16[16,128,128]{2,1,0:T(8,128)(2,1)}), bf16[16,128,128]{2,1,0:T(8,128)(2,1)S(1)}, u32[]{:S(2)}, u32[]{:S(2)}) async-start(bf16[16,128,128]{2,1,0:T(8,128)(2,1)} %shard_map.261), calls=%async_computation.3 | async-start | bytes 1048576 | tf_op jit(solution)/shard_map/all_to_all | solution.py:360
  59.9 0.0 copy-done.8
  59.9 0.6 reshape.53.mix
  60.5 0.7 shard_map.263
  61.2 0.2 shard_map.262
  61.5 5.3 %all-to-all-done.3.arrived = bf16[16,128,128]{2,1,0:T(8,128)(2,1)S(1)} async-done(((bf16[16,128,128]{2,1,0:T(8,128)(2,1)}), bf16[16,128,128]{2,1,0:T(8,128)(2,1)S(1)}, u32[]{:S(2)}, u32[]{:S(2)}) %all-to-all-start.3) | async-done | bytes 524320 | tf_op jit(solution)/shard_map/all_to_all | solution.py:360
  66.8 0.0 copy-done
  66.8 0.0 copy-done.1
  66.8 0.0 copy-done.2
  66.8 0.0 copy-done.4
  66.8 0.0 copy-done.5
  66.9 0.0 copy-done.6
  66.9 1.1 %shard_map.264 = bf16[16,128,128]{2,1,0:T(8,128)(2,1)S(1)} custom-call(bf16[16,128,128]{2,1,0:T(8,128)(2,1)S(1)} %all-to-all-done.3.arrived, f32[128,128]{1,0:T(8,128)S(1)} %get-tuple-element.24.weight, f32[128,128]{1,0:T(8,128)S(1)} %get-tuple-element.25.main, f32[16,128]{1,0:T(8,128)S(1)} %get-tuple-element.26.gain, ...), custom_call_target="tpu_custom_call" | custom-call | tf_op jit(solution)/shard_map/pallas_call | solution.py:34
  68.0 13.8 %all_to_all.32.partial = bf16[16,128,128]{2,1,0:T(8,128)(2,1)S(1)} all-to-all(bf16[16,128,128]{2,1,0:T(8,128)(2,1)S(1)} %shard_map.264), channel_id=1, replica_groups={{10,11,12,13,14,15,0,1,2,3,4,5,6,7,8,9},{26,27,28,29,30,31,16,17,18,19,..., dimensions={0} | all-to-all | bytes 1048576 | tf_op jit(solution)/shard_map/all_to_all | solution.py:360
  81.7 0.7 shard_map.265
  82.4 9.9 %all-to-all-start.5 = ((bf16[32,4,128]{2,1,0:T(4,128)(2,1)}), bf16[32,4,128]{2,1,0:T(4,128)(2,1)S(1)}, u32[]{:S(2)}, u32[]{:S(2)}) async-start(bf16[32,4,128]{2,1,0:T(4,128)(2,1)} %bitcast.19), calls=%async_computation.5 | async-start | bytes 65536 | tf_op jit(solution)/shard_map/all_to_all | solution.py:360
  92.3 0.9 shard_map.266.table
  93.2 3.2 %shard_map.269 = f32[24,64,128]{2,1,0:T(8,128)} custom-call(f32[24,64,128]{2,1,0:T(8,128)} %state.3, f32[5,24,128]{2,1,0:T(8,128)S(1)} %get-tuple-element.29.vectors), custom_call_target="tpu_custom_call" | custom-call | tf_op jit(solution)/shard_map/pallas_call | solution.py:34
  96.4 1.4 %all-to-all-done.5 = bf16[32,4,128]{2,1,0:T(4,128)(2,1)S(1)} async-done(((bf16[32,4,128]{2,1,0:T(4,128)(2,1)}), bf16[32,4,128]{2,1,0:T(4,128)(2,1)S(1)}, u32[]{:S(2)}, u32[]{:S(2)}) %all-to-all-start.5) | async-done | bytes 32800 | tf_op jit(solution)/shard_map/all_to_all | solution.py:360
  97.8 0.8 shard_map.268
  (1 shorter events, 0.0 us)
Async XLA Ops:
  2.4 12.4 %all-to-all-start = ((bf16[16,64,128]{2,1,0:T(8,128)(2,1)}), bf16[16,64,128]{2,1,0:T(8,128)(2,1)S(1)}, u32[]{:S(2)}, u32[]{:S(2)}) async-start(bf16[16,64,128]{2,1,0:T(8,128)(2,1)} %shard_map.257), calls=%async_computation | async-start | bytes 524288 | tf_op jit(solution)/shard_map/all_to_all | solution.py:360
  14.4 10.7 %copy-start.3 = (bf16[2048,128]{1,0:T(8,128)(2,1)S(1)}, bf16[2048,128]{1,0:T(8,128)(2,1)}, u32[]{:S(2)}) copy-start(bf16[2048,128]{1,0:T(8,128)(2,1)} %w_out.1) | copy-start | bytes 1572868
  14.4 10.7 %copy-start.7 = (bf16[24,128]{1,0:T(8,128)(2,1)S(1)}, bf16[24,128]{1,0:T(8,128)(2,1)}, u32[]{:S(2)}) copy-start(bf16[24,128]{1,0:T(8,128)(2,1)} %tokens.3) | copy-start | bytes 18436
  15.9 44.0 %copy-start.8 = (bf16[2048]{0:T(1024)(128)(2,1)S(1)}, bf16[2048]{0:T(1024)(128)(2,1)}, u32[]{:S(2)}) copy-start(bf16[2048]{0:T(1024)(128)(2,1)} %param.51) | copy-start | bytes 12292
  15.9 50.9 %copy-start = (bf16[1,2048,128]{2,1,0:T(8,128)(2,1)S(1)}, bf16[1,2048,128]{2,1,0:T(8,128)(2,1)}, u32[]{:S(2)}) copy-start(bf16[1,2048,128]{2,1,0:T(8,128)(2,1)} %param.45) | copy-start | bytes 1572868
  15.9 50.9 %copy-start.1 = (bf16[1,2048,128]{2,1,0:T(8,128)(2,1)S(1)}, bf16[1,2048,128]{2,1,0:T(8,128)(2,1)}, u32[]{:S(2)}) copy-start(bf16[1,2048,128]{2,1,0:T(8,128)(2,1)} %param.46) | copy-start | bytes 1572868
  15.9 50.9 %copy-start.2 = (bf16[1,128,2048]{2,1,0:T(8,128)(2,1)S(1)}, bf16[1,128,2048]{2,1,0:T(8,128)(2,1)}, u32[]{:S(2)}) copy-start(bf16[1,128,2048]{2,1,0:T(8,128)(2,1)} %param.47) | copy-start | bytes 1572868
  15.9 50.9 %copy-start.4 = (bf16[2048,32]{0,1:T(8,128)(2,1)S(1)}, bf16[2048,32]{0,1:T(8,128)(2,1)}, u32[]{:S(2)}) copy-start(bf16[2048,32]{0,1:T(8,128)(2,1)} %param.48) | copy-start | bytes 393220
  16.0 50.9 %copy-start.5 = (bf16[2048,32]{0,1:T(8,128)(2,1)S(1)}, bf16[2048,32]{0,1:T(8,128)(2,1)}, u32[]{:S(2)}) copy-start(bf16[2048,32]{0,1:T(8,128)(2,1)} %param.49) | copy-start | bytes 393220
  16.0 50.9 %copy-start.6 = (bf16[32,2048]{1,0:T(8,128)(2,1)S(1)}, bf16[32,2048]{1,0:T(8,128)(2,1)}, u32[]{:S(2)}) copy-start(bf16[32,2048]{1,0:T(8,128)(2,1)} %dense_down.1) | copy-start | bytes 393220
  51.8 15.0 %all-to-all-start.3 = ((bf16[16,128,128]{2,1,0:T(8,128)(2,1)}), bf16[16,128,128]{2,1,0:T(8,128)(2,1)S(1)}, u32[]{:S(2)}, u32[]{:S(2)}) async-start(bf16[16,128,128]{2,1,0:T(8,128)(2,1)} %shard_map.261), calls=%async_computation.3 | async-start | bytes 1048576 | tf_op jit(solution)/shard_map/all_to_all | solution.py:360
  82.4 15.4 %all-to-all-start.5 = ((bf16[32,4,128]{2,1,0:T(4,128)(2,1)}), bf16[32,4,128]{2,1,0:T(4,128)(2,1)S(1)}, u32[]{:S(2)}, u32[]{:S(2)}) async-start(bf16[32,4,128]{2,1,0:T(4,128)(2,1)} %bitcast.19), calls=%async_computation.5 | async-start | bytes 65536 | tf_op jit(solution)/shard_map/all_to_all | solution.py:360
